TPU v7x, 256 devices: a 8x8x2 block of a 8x8x16 slice. The times are simulated.
256 devices in a mesh: grp: 2 (over z), sp: 16 (over y, core), tp: 8 (over x).
Axes of the slice: x: 8, y: 8, z: 2, core: 2. Of those that a mesh axis runs over, the one named last changes fastest.
The devices are a block of a 8x8x16 slice.
Arguments:
- residual: bfloat16 [3072, 8, 2048], P(('sp', 'tp'), 'grp'), parts along dimension 1, may hold values from -6 to 6
- query: bfloat16 [3072, 8, 1536], P('sp', 'grp', 'tp'), parts along dimension 1, may hold values from -64 to 64
- latent: bfloat16 [3072, 8, 512], P('sp', 'grp'), parts along dimension 1, may hold values from -6 to 6
- rope_key: bfloat16 [3072, 8, 64], P('sp', 'grp'), parts along dimension 1, may hold values from -8 to 8
- latent_gain: float32 [512], replicated, may hold values from 0.1 to 1.9
- key_up: bfloat16 [512, 1024], P(None, 'tp'), may hold values from -0.25 to 0.25
- value_up: bfloat16 [512, 1024], P(None, 'tp'), may hold values from -0.25 to 0.25
- out_weight: bfloat16 [1024, 2048], P('tp'), may hold values from -0.375 to 0.375
- norm_gain: float32 [2048], replicated, may hold values from 0.1 to 1.9
- group_prob: float32 [3072, 8], P(('sp', 'tp'), 'grp'), parts along dimension 1, may hold values from 0.25 to 1
- pair_logits: float32 [3072, 8, 2], P(('sp', 'tp'), 'grp'), parts along dimension 1, may hold values from -8 to 8
- routes: int32 [3072, 8, 2], P(('sp', 'tp'), 'grp'), parts along dimension 1, may hold values from 0 to 127, all different within a row; in each aligned block of 96 rows (0 to 95, 96 to 191, ..., all dimensions but the last counted through in order) at most 2 rows name the same one
- w_gate: bfloat16 [128, 2048, 768], P(('sp', 'tp')), may hold values from -0.125 to 0.125
- w_up: bfloat16 [128, 2048, 768], P(('sp', 'tp')), may hold values from -0.125 to 0.125
- w_down: bfloat16 [128, 768, 2048], P(('sp', 'tp')), may hold values from -0.4375 to 0.4375
Outputs:
- layer_out: bfloat16 [3072, 8, 2048], P(('sp', 'tp'), 'grp'), parts along dimension 1
There are 2 independent parts, one for each index of `grp`. A program takes and returns all parts, laid end to end along the dimension named above; an argument that names none is the same for every part. Nothing has to cross between parts.
Inputs may be any that keep to these rules, and one draw needn't show every extreme that they name: `routes`: A token's 2 experts differ. Among the tokens of one device (aligned blocks of 96 rows in position-then-sequence order), no expert is named more than 2 times, a bound that some block reaches.
All inputs are finite; a program needn't handle non-finite values.
Results may differ from a plain program's by a relative error of at most 0.013.
Values may be sent and summed in bfloat16 or wider, within the bound.
No kernel may reach another device: no remote copies, remote signals or barrier semaphores. Data moves between devices by JAX's collectives and lax.ppermute only.
A program may use at most 128 MiB of HBM per device.

v0:
```python
import jax
import jax.numpy as jnp
import numpy as np
from jax import lax
from jax.experimental import pallas as pl
from jax.experimental.pallas import tpu as pltpu
from jax.sharding import Mesh, PartitionSpec as P


D = 2048
NOPE = 128
VDIM = 128
QK = 192
SEQS = 4
LANE = 256
BANDS = D // LANE

epsilon = 1e-06
rotary_base = 10000.0
score_scale = QK ** (-0.5) * 1.4426950408889634

Y = ("half", "quad")
ALL = ("half", "quad", "core", "tp")


def rotate(values, positions):
    halfway = values.shape[-1] // 2
    inverse = rotary_base ** (-jnp.arange(halfway, dtype=jnp.float32) / halfway)
    angles = positions.astype(jnp.float32)[:, None] * inverse[None, :]
    angles = angles.reshape((1, angles.shape[0], halfway))
    cosine_values = jnp.cos(angles)
    sine_values = jnp.sin(angles)
    first_half = values[..., :halfway]
    second_half = values[..., halfway:]
    return jnp.concatenate(
        [
            first_half * cosine_values - second_half * sine_values,
            second_half * cosine_values + first_half * sine_values,
        ],
        axis=-1,
    )


def shift(x, axis, by, size):
    if by == 0:
        return x
    return lax.ppermute(x, axis, [(i, (i + by) % size) for i in range(size)])


def swap(x):
    return lax.ppermute(x, "core", [(0, 1), (1, 0)])


def spread(x, by, size):
    pairs = []
    for i in range(size):
        pairs.append((i, (i + by) % size))
        pairs.append((size + i, size + (i - by) % size))
    return lax.ppermute(x, ("core", "tp"), pairs)


def dot(a, b):
    return lax.dot_general(a, b, (((1,), (0,)), ((), ())), preferred_element_type=jnp.float32)


def packing(inverse):
    i = lax.broadcasted_iota(jnp.int32, (256, 256), 1 if inverse else 0)
    k = lax.broadcasted_iota(jnp.int32, (256, 256), 0 if inverse else 1)
    d, r = i // 16, i % 16
    return (k == (r // 2) * 32 + (r % 2) * 16 + d).astype(jnp.bfloat16)


def pack_rows(rows_ref, out_ref, perm):
    for b in range(8):
        stack = []
        for j in range(BANDS):
            for slot in range(2):
                lo = slot * 128 + b * 16
                stack.append(rows_ref[lo : lo + 16, j * LANE : (j + 1) * LANE])
        out_ref[b * 256 : (b + 1) * 256, :] = dot(perm, jnp.concatenate(stack, axis=0)).astype(
            jnp.bfloat16
        )


def unpack_rows(in_ref, rows_ref, perm):
    for b in range(8):
        block = dot(perm, in_ref[b * 256 : (b + 1) * 256, :]).astype(jnp.bfloat16)
        for j in range(BANDS):
            for slot in range(2):
                lo = slot * 128 + b * 16
                at = j * 32 + slot * 16
                rows_ref[lo : lo + 16, j * LANE : (j + 1) * LANE] = block[at : at + 16, :]


def places(meta):
    rows = meta.shape[0]
    expert = lax.broadcasted_iota(jnp.int32, (rows, 128), 1).astype(jnp.float32)
    first = (meta[:, 0:1] == expert).astype(jnp.float32)
    second = (meta[:, 1:2] == expert).astype(jnp.float32)
    earlier = (
        lax.broadcasted_iota(jnp.int32, (rows, rows), 0)
        > lax.broadcasted_iota(jnp.int32, (rows, rows), 1)
    ).astype(jnp.bfloat16)
    before = dot(earlier, (first + second).astype(jnp.bfloat16))
    return first, second, before


def attention_body(at_ref, q_ref, a_ref, b_ref, o_ref, keys, values):
    quad = at_ref[2]
    for i in range(16):
        src = a_ref if i < 8 else b_ref
        j = i % 8
        lo, hi = i * 96, 1536 + i * 96
        keys[lo : lo + 96, 0:128] = src[j, 0:96, :]
        keys[hi : hi + 96, 0:128] = src[j, 96:192, :]
        values[lo : lo + 96, :] = src[j, 192:288, :]
        values[hi : hi + 96, :] = src[j, 288:384, :]
        rot = src[j, 384:480, :]
        keys[lo : lo + 96, 128:256] = rot
        keys[hi : hi + 96, 128:256] = pltpu.roll(rot.astype(jnp.float32), 64, 1).astype(
            jnp.bfloat16
        )
    for n in range(4):
        q = q_ref[n * 192 : (n + 1) * 192, :]
        scores = lax.dot_general(
            q, keys[...], (((1,), (1,)), ((), ())), preferred_element_type=jnp.float32
        )
        highest = jnp.max(scores, axis=-1, keepdims=True)
        weights = jnp.exp2((scores - highest) * score_scale)
        totals = jnp.sum(weights, axis=-1, keepdims=True)
        out = dot(weights.astype(jnp.bfloat16), values[...])
        o_ref[(quad + 4 - n) % 4] = (out / totals).astype(jnp.bfloat16)


def project_body(
    at_ref,
    att_ref,
    w0,
    w1,
    w2,
    w3,
    s1,
    s2,
    s3,
    w4,
    s4,
    res_ref,
    gain_ref,
    meta_ref,
    stream_ref,
    out_ref,
    rows,
):
    tp, core = at_ref[0], at_ref[1]
    turn = 1 - 2 * core
    projected = dot(att_ref[tp], w0[...])
    for k, w_ref in ((1, w1), (2, w2), (3, w3), (-1, s1), (-2, s2), (-3, s3)):
        projected += dot(att_ref[(tp + 8 - turn * k) % 8], w_ref[...])
    last = att_ref[(tp + 4) % 8]
    turned = pltpu.roll(last.astype(jnp.float32), 64, 1).astype(jnp.bfloat16)
    last = jnp.where(core == 0, last, turned)
    projected += dot(last[:, :64], w4[...]) + dot(last[:, 64:], s4[...])
    stream = (res_ref[...].astype(jnp.float32) + projected).astype(jnp.bfloat16)
    stream_ref[...] = stream
    wide = stream.astype(jnp.float32)
    normed = (
        wide * lax.rsqrt(jnp.mean(wide * wide, axis=-1, keepdims=True) + epsilon) * gain_ref[...]
    ).astype(jnp.bfloat16)
    first, second, before = places(meta_ref[...])
    both = first + second
    for slot in range(2):
        pick = (both * (before == slot).astype(jnp.float32)).T.astype(jnp.bfloat16)
        rows[slot * 128 : (slot + 1) * 128, :] = dot(pick, normed).astype(jnp.bfloat16)
    pack_rows(rows, out_ref, packing(False))


def expert_body(in_ref, gate_ref, up_ref, down_ref, out_ref, rows, acc):
    step = pl.program_id(0)

    @pl.when(step == 0)
    def _():
        unpack_rows(in_ref, rows, packing(True))

    x = rows[...]
    gate = dot(x, gate_ref[...])
    up = dot(x, up_ref[...])
    hidden = (gate / (1.0 + jnp.exp(-gate)) * up).astype(jnp.bfloat16)
    part = dot(hidden, down_ref[...])

    @pl.when(step == 0)
    def _():
        acc[...] = part

    @pl.when(step > 0)
    def _():
        acc[...] += part

    @pl.when(step == pl.num_programs(0) - 1)
    def _():
        rows[...] = acc[...].astype(jnp.bfloat16)
        pack_rows(rows, out_ref, packing(False))


def combine_body(in_ref, stream_ref, meta_ref, out_ref, rows):
    unpack_rows(in_ref, rows, packing(True))
    meta = meta_ref[...]
    first, second, before = places(meta)
    logits = meta[:, 2:4]
    weights = jnp.exp(logits - jnp.max(logits, axis=-1, keepdims=True))
    mixing = weights / jnp.sum(weights, axis=-1, keepdims=True) * meta[:, 4:5]
    slots = [(before == slot).astype(jnp.float32) for slot in range(2)]
    total = stream_ref[...].astype(jnp.float32)
    r = rows[...]
    added = None
    for k, hot in enumerate((first, second)):
        pick = jnp.concatenate([hot * slots[0], hot * slots[1]], axis=-1).astype(jnp.bfloat16)
        term = dot(pick, r) * mixing[:, k : k + 1]
        added = term if added is None else added + term
    out_ref[...] = (total + added).astype(jnp.bfloat16)


def vmem(*shape):
    return pltpu.VMEM(shape, jnp.bfloat16)


def params():
    return pltpu.CompilerParams(vmem_limit_bytes=56 * 1024 * 1024)


def kernel_call(body, **options):
    return pl.pallas_call(body, compiler_params=params(), **options)


VM = pl.BlockSpec(memory_space=pltpu.VMEM)
SM = pl.BlockSpec(memory_space=pltpu.SMEM)


def layer(
    residual,
    query,
    latent,
    rope_key,
    latent_gain,
    key_up,
    value_up,
    out_weight,
    norm_gain,
    group_prob,
    pair_logits,
    routes,
    w_gate,
    w_up,
    w_down,
):
    tp = lax.axis_index("tp")
    core = lax.axis_index("core")
    block = query.shape[0]
    rows = residual.shape[0] * SEQS
    tp_size = lax.axis_size("tp")
    quad = lax.axis_index("quad")
    at = jnp.stack([tp, core, quad]).astype(jnp.int32)

    spot = (lax.axis_index("half") * 4 + lax.axis_index("quad")) * 2 + core
    positions = spot * block + jnp.arange(block, dtype=jnp.int32)
    q = jnp.swapaxes(query, 0, 1)
    q_rot = rotate(q[..., NOPE:].astype(jnp.float32), positions).astype(jnp.bfloat16)
    q = jnp.concatenate([q[..., :NOPE], q_rot, jnp.zeros_like(q_rot)], axis=-1)
    queries = []
    for k in range(4):
        piece = lax.dynamic_index_in_dim(q, (quad + k) % 4, 0, keepdims=False)
        queries.append(shift(piece, "quad", k, 4))
    queries = jnp.concatenate(queries, axis=0)

    lat = jnp.swapaxes(latent, 0, 1).astype(jnp.float32)
    lat = (
        lat * lax.rsqrt(jnp.mean(lat * lat, axis=-1, keepdims=True) + epsilon) * latent_gain
    ).astype(jnp.bfloat16)
    keys = jnp.einsum("spd,dc->spc", lat, key_up, preferred_element_type=jnp.float32)
    vals = jnp.einsum("spd,dc->spc", lat, value_up, preferred_element_type=jnp.float32)
    rot = rotate(jnp.swapaxes(rope_key, 0, 1).astype(jnp.float32), positions)
    rot = jnp.concatenate([rot[:, : block // 2], rot[:, block // 2 :]], axis=-1)
    kv = jnp.concatenate([keys, vals, rot], axis=1).astype(jnp.bfloat16)
    kv = jnp.concatenate([kv, kv], axis=0)
    half_rows = out_weight.shape[0] // 2
    one, two = spread(out_weight, 1, tp_size), spread(out_weight, 2, tp_size)
    three = spread(two, 1, tp_size)
    part = lax.dynamic_slice(two, (core * half_rows, 0), (half_rows, D))
    four = spread(part, 2, tp_size)
    weights = [out_weight, one, two, three, swap(one), swap(two)]
    weights += [swap(three), four, swap(four)]

    near = lax.all_to_all(kv, Y, split_axis=0, concat_axis=0, tiled=True)
    far = swap(near)

    attended = kernel_call(
        attention_body,
        out_shape=jax.ShapeDtypeStruct((4, block, VDIM), jnp.bfloat16),
        in_specs=[SM] + [VM] * 3,
        out_specs=VM,
        scratch_shapes=[vmem(16 * block, 256), vmem(16 * block, VDIM)],
    )(at, queries, near, far)
    attended = attended.reshape(4 * tp_size, block // tp_size, VDIM)
    attended = lax.all_to_all(attended, ("quad", "tp"), split_axis=0, concat_axis=0, tiled=True)
    attended = attended.reshape(SEQS, tp_size, block // tp_size, VDIM)
    attended = jnp.swapaxes(attended, 0, 1).reshape(tp_size, rows, VDIM)

    res = jnp.swapaxes(residual, 0, 1).reshape(rows, D)
    meta = jnp.concatenate(
        [routes.astype(jnp.float32), pair_logits, group_prob[..., None]], axis=-1
    )
    meta = jnp.swapaxes(meta, 0, 1).reshape(rows, 5)
    stream, outgoing = pl.pallas_call(
        project_body,
        out_shape=(
            jax.ShapeDtypeStruct((rows, D), jnp.bfloat16),
            jax.ShapeDtypeStruct((2048, LANE), jnp.bfloat16),
        ),
        in_specs=[SM] + [VM] * 13,
        out_specs=(VM, VM),
        scratch_shapes=[vmem(256, D)],
        compiler_params=params(),
        name="project",
    )(at, attended, *weights, res, norm_gain.reshape(1, D), meta)

    def exchange(x):
        x = x.reshape(128, 16, LANE)
        return lax.all_to_all(x, ALL, split_axis=0, concat_axis=0, tiled=True).reshape(2048, LANE)

    arrived = exchange(outgoing)
    hidden = w_gate.shape[2]
    step = 256
    served = pl.pallas_call(
        expert_body,
        out_shape=jax.ShapeDtypeStruct((2048, LANE), jnp.bfloat16),
        grid=(hidden // step,),
        in_specs=[
            pl.BlockSpec((2048, LANE), lambda i: (0, 0)),
            pl.BlockSpec((D, step), lambda i: (0, i)),
            pl.BlockSpec((D, step), lambda i: (0, i)),
            pl.BlockSpec((step, D), lambda i: (i, 0)),
        ],
        out_specs=pl.BlockSpec((2048, LANE), lambda i: (0, 0)),
        scratch_shapes=[vmem(256, D), pltpu.VMEM((256, D), jnp.float32)],
        compiler_params=params(),
        name="experts",
    )(arrived, w_gate[0], w_up[0], w_down[0])
    returned = exchange(served)
    combined = pl.pallas_call(
        combine_body,
        out_shape=jax.ShapeDtypeStruct((rows, D), jnp.bfloat16),
        in_specs=[VM] * 3,
        out_specs=VM,
        scratch_shapes=[vmem(256, D)],
        compiler_params=params(),
        name="combine",
    )(returned, stream, meta)
    return jnp.swapaxes(combined.reshape(SEQS, rows // SEQS, D), 0, 1)


def solution(mesh):
    shape = mesh.shape
    devices = np.asarray(mesh.devices).reshape(
        shape["grp"], 2, 4, shape["sp"] // 8, shape["tp"]
    )
    fine = Mesh(devices, ("grp", "half", "quad", "core", "tp"))
    sp = ("half", "quad", "core")
    both = ("half", "quad", "core", "tp")
    placed = (
        P(both, "grp", None),
        P(sp, "grp", "tp"),
        P(sp, "grp", None),
        P(sp, "grp", None),
        P(),
        P(None, "tp"),
        P(None, "tp"),
        P("tp", None),
        P(),
        P(both, "grp"),
        P(both, "grp", None),
        P(both, "grp", None),
        P(both, None, None),
        P(both, None, None),
        P(both, None, None),
    )
    return jax.shard_map(
        layer, mesh=fine, in_specs=placed, out_specs=P(both, "grp", None), check_vma=False
    )
```

profile of v0, /device:TPU:513, one launch (start us, length us, event | category | flops | bytes accessed | tf_op | source)
XLA Modules:
  0.0 191.0 jit_solution(7571506169690358380)
XLA Ops:
  0.1 1.1 copy.35
  3.2 1.2 maximum_maximum_fusion
  4.4 13.7 %all-to-all-start = ((bf16[8,480,128]{2,1,0:T(8,128)(2,1)}), bf16[8,480,128]{2,1,0:T(8,128)(2,1)S(1)}, u32[]{:S(2)}, u32[]{:S(2)}) async-start(bf16[8,480,128]{2,1,0:T(8,128)(2,1)} %maximum_maximum_fusion), calls=%async_computation | async-start | bytes 1966080 | tf_op jit(solution)/shard_map/all_to_all | solution.py:292
  18.1 4.3 %collective-permute-start.5 = (bf16[128,2048]{1,0:T(8,128)(2,1)}, bf16[128,2048]{1,0:T(8,128)(2,1)S(1)}, u32[]{:S(2)}, u32[]{:S(2)}) collective-permute-start(bf16[128,2048]{1,0:T(8,128)(2,1)} %w0.1), channel_id=1, source_target_pairs={{0,2},{8,14},{1,3},{9,15},{2,4},{10,8},{3,5},{11,9},{4,6},{12,10},... | collective-permute-start | bytes 1572872 | tf_op jit(solution)/shard_map/ppermute | solution.py:59
  22.4 1.0 collective-permute-start.4
  23.5 11.9 %all-to-all-done.a_ref = bf16[8,480,128]{2,1,0:T(8,128)(2,1)S(1)} async-done(((bf16[8,480,128]{2,1,0:T(8,128)(2,1)}), bf16[8,480,128]{2,1,0:T(8,128)(2,1)S(1)}, u32[]{:S(2)}, u32[]{:S(2)}) %all-to-all-start) | async-done | bytes 983072 | tf_op jit(solution)/shard_map/all_to_all | solution.py:292
  35.4 11.2 %collective-permute-start.3 = (bf16[8,480,128]{2,1,0:T(8,128)(2,1)S(1)}, bf16[8,480,128]{2,1,0:T(8,128)(2,1)S(1)}, u32[]{:S(2)}, u32[]{:S(2)}) collective-permute-start(bf16[8,480,128]{2,1,0:T(8,128)(2,1)S(1)} %all-to-all-done.a_ref), channel_id=1, source_target_pairs={{0,8},{8,0},{1,9},{9,1},{2,10},{10,2},{3,11},{11,3},{4,12},{12,4},... | collective-permute-start | bytes 2949128 | tf_op jit(solution)/shard_map/ppermute | solution.py:51
  46.6 1.1 subtract_convert_fusion
  47.8 3.4 %collective-permute-start.6 = (bf16[128,2048]{1,0:T(8,128)(2,1)S(1)}, bf16[128,2048]{1,0:T(8,128)(2,1)S(1)}, u32[]{:S(2)}, u32[]{:S(2)}) collective-permute-start(bf16[128,2048]{1,0:T(8,128)(2,1)S(1)} %collective-permute-done.5.w2), channel_id=1, source_target_pairs={{0,1},{8,15},{1,2},{9,8},{2,3},{10,9},{3,4},{11,10},{4,5},{12,11},... | collective-permute-start | bytes 1572872 | tf_op jit(solution)/shard_map/ppermute | solution.py:59
  52.5 6.3 %collective-permute-done = bf16[192,256]{1,0:T(8,128)(2,1)} collective-permute-done((bf16[192,256]{1,0:T(8,128)(2,1)}, bf16[192,256]{1,0:T(8,128)(2,1)}, u32[]{:S(2)}, u32[]{:S(2)}) %collective-permute-start) | collective-permute-done | bytes 98336 | tf_op jit(solution)/shard_map/ppermute | solution.py:47
  59.6 2.2 %collective-permute-done.1 = bf16[192,256]{1,0:T(8,128)(2,1)} collective-permute-done((bf16[192,256]{1,0:T(8,128)(2,1)}, bf16[192,256]{1,0:T(8,128)(2,1)}, u32[]{:S(2)}, u32[]{:S(2)}) %collective-permute-start.1) | collective-permute-done | bytes 98336 | tf_op jit(solution)/shard_map/ppermute | solution.py:47
  61.8 2.1 %collective-permute-start.10 = (bf16[64,2048]{1,0:T(8,128)(2,1)}, bf16[64,2048]{1,0:T(8,128)(2,1)}, u32[]{:S(2)}, u32[]{:S(2)}) collective-permute-start(bf16[64,2048]{1,0:T(8,128)(2,1)} %constant_dynamic-slice_fusion), channel_id=1, source_target_pairs={{0,2},{8,14},{1,3},{9,15},{2,4},{10,8},{3,5},{11,9},{4,6},{12,10},... | collective-permute-start | bytes 786440 | tf_op jit(solution)/shard_map/ppermute | solution.py:59
  65.4 1.8 pad_maximum_fusion.q_ref
  67.2 1.0 copy-done.3
  68.2 6.9 %shard_map.145 = bf16[4,192,128]{2,1,0:T(8,128)(2,1)} custom-call(s32[3]{0:T(128)} %pad_add_fusion.at_ref, bf16[768,256]{1,0:T(8,128)(2,1)} %pad_maximum_fusion.q_ref, bf16[8,480,128]{2,1,0:T(8,128)(2,1)} %copy-done.1, bf16[8,480,128]{2,1,0:T(8,128)(2,1)} %copy-done.3), custom_call_target="tpu_custom_call" | custom-call | tf_op jit(solution)/shard_map/pallas_call | solution.py:295
  75.0 7.2 %all-to-all-start.1 = ((bf16[32,24,128]{2,1,0:T(8,128)(2,1)}), bf16[32,24,128]{2,1,0:T(8,128)(2,1)S(1)}, u32[]{:S(2)}, u32[]{:S(2)}) async-start(bf16[32,24,128]{2,1,0:T(8,128)(2,1)} %bitcast.71), calls=%async_computation.1 | async-start | bytes 393216 | tf_op jit(solution)/shard_map/all_to_all | solution.py:303
  83.7 1.0 copy.37
  84.7 6.6 %all-to-all-done.1 = bf16[32,24,128]{2,1,0:T(8,128)(2,1)S(1)} async-done(((bf16[32,24,128]{2,1,0:T(8,128)(2,1)}), bf16[32,24,128]{2,1,0:T(8,128)(2,1)S(1)}, u32[]{:S(2)}, u32[]{:S(2)}) %all-to-all-start.1) | async-done | bytes 196640 | tf_op jit(solution)/shard_map/all_to_all | solution.py:303
  92.7 5.4 %project.1 = (bf16[96,2048]{1,0:T(8,128)(2,1)}, bf16[2048,256]{1,0:T(8,128)(2,1)}) custom-call(s32[3]{0:T(128)} %pad_add_fusion.at_ref, bf16[8,96,128]{2,1,0:T(8,128)(2,1)} %bitcast.69, bf16[128,2048]{1,0:T(8,128)(2,1)} %w0.1, bf16[128,2048]{1,0:T(8,128)(2,1)} %collective-permute-done.4.w1, bf16[128,2048]{1,0:T(8,128)(2,1)} %copy-done.2, ...), custom_call_target="tpu_custom_call" | custom-call | tf_op jit(solution)/shard_map/project/pallas_call | solution.py:312
  98.0 40.3 %all_to_all.20 = bf16[128,16,256]{2,1,0:T(8,128)(2,1)} all-to-all(bf16[128,16,256]{2,1,0:T(8,128)(2,1)} %bitcast.68), channel_id=1, replica_groups=mesh['grp'=2,'half'=2,'quad'=4,'core'=2,'tp'=8] {'half','quad','core','tp'}, dimensions={0} | all-to-all | bytes 2097152 | tf_op jit(solution)/shard_map/all_to_all | solution.py:327
  138.4 8.8 %experts.1 = bf16[2048,256]{1,0:T(8,128)(2,1)} custom-call(bf16[2048,256]{1,0:T(8,128)(2,1)} %bitcast.58, bf16[2048,768]{1,0:T(8,128)(2,1)} %bitcast.61, bf16[2048,768]{1,0:T(8,128)(2,1)} %bitcast.62, bf16[768,2048]{1,0:T(8,128)(2,1)} %bitcast.63), custom_call_target="tpu_custom_call" | custom-call | tf_op jit(solution)/shard_map/experts/pallas_call | solution.py:332
  147.2 38.7 %all_to_all.21 = bf16[128,16,256]{2,1,0:T(8,128)(2,1)} all-to-all(bf16[128,16,256]{2,1,0:T(8,128)(2,1)} %bitcast.59), channel_id=1, replica_groups=mesh['grp'=2,'half'=2,'quad'=4,'core'=2,'tp'=8] {'half','quad','core','tp'}, dimensions={0} | all-to-all | bytes 2097152 | tf_op jit(solution)/shard_map/all_to_all | solution.py:327
  185.9 3.1 %combine.1 = bf16[96,2048]{1,0:T(8,128)(2,1)} custom-call(bf16[2048,256]{1,0:T(8,128)(2,1)} %bitcast.57, bf16[96,2048]{1,0:T(8,128)(2,1)} %get-tuple-element.8.stream_ref, f32[96,5]{1,0:T(8,128)} %bitcast.73), custom_call_target="tpu_custom_call" | custom-call | tf_op jit(solution)/shard_map/combine/pallas_call | solution.py:348
  188.9 2.0 %copy.47 = bf16[4,24,2048]{2,0,1:T(4,128)(2,1)} copy(bf16[4,24,2048]{2,1,0:T(8,128)(2,1)} %bitcast.67) | data formatting | bytes 786432 | tf_op jit(solution)/shard_map/reshape | solution.py:357
  (69 shorter events, 8.5 us)
Async XLA Ops:
  0.0 2.3 %copy-start = (bf16[512,128]{1,0:T(8,128)(2,1)S(1)}, bf16[512,128]{1,0:T(8,128)(2,1)}, u32[]{:S(2)}) copy-start(bf16[512,128]{1,0:T(8,128)(2,1)} %param.21) | copy-start | bytes 393220
  0.0 2.3 %copy-start.14 = (f32[512]{0:T(512)S(1)}, f32[512]{0:T(512)}, u32[]{:S(2)}) copy-start(f32[512]{0:T(512)} %param.19) | copy-start | bytes 6148
  3.2 20.2 %copy-start.7 = (bf16[192,4,192]{2,1,0:T(4,128)(2,1)S(1)}, bf16[192,4,192]{2,1,0:T(4,128)(2,1)}, u32[]{:S(2)}) copy-start(bf16[192,4,192]{2,1,0:T(4,128)(2,1)} %param.16) | copy-start | bytes 884740
  4.4 31.0 %all-to-all-start = ((bf16[8,480,128]{2,1,0:T(8,128)(2,1)}), bf16[8,480,128]{2,1,0:T(8,128)(2,1)S(1)}, u32[]{:S(2)}, u32[]{:S(2)}) async-start(bf16[8,480,128]{2,1,0:T(8,128)(2,1)} %maximum_maximum_fusion), calls=%async_computation | async-start | bytes 1966080 | tf_op jit(solution)/shard_map/all_to_all | solution.py:292
  18.1 29.7 %collective-permute-start.5 = (bf16[128,2048]{1,0:T(8,128)(2,1)}, bf16[128,2048]{1,0:T(8,128)(2,1)S(1)}, u32[]{:S(2)}, u32[]{:S(2)}) collective-permute-start(bf16[128,2048]{1,0:T(8,128)(2,1)} %w0.1), channel_id=1, source_target_pairs={{0,2},{8,14},{1,3},{9,15},{2,4},{10,8},{3,5},{11,9},{4,6},{12,10},... | collective-permute-start | bytes 1572872 | tf_op jit(solution)/shard_map/ppermute | solution.py:59
  22.4 41.5 %collective-permute-start.4 = (bf16[128,2048]{1,0:T(8,128)(2,1)}, bf16[128,2048]{1,0:T(8,128)(2,1)}, u32[]{:S(2)}, u32[]{:S(2)}) collective-permute-start(bf16[128,2048]{1,0:T(8,128)(2,1)} %w0.1), channel_id=1, source_target_pairs={{0,1},{8,15},{1,2},{9,8},{2,3},{10,9},{3,4},{11,10},{4,5},{12,11},... | collective-permute-start | bytes 1572872 | tf_op jit(solution)/shard_map/ppermute | solution.py:59
  35.4 24.1 %copy-start.1 = (bf16[8,480,128]{2,1,0:T(8,128)(2,1)}, bf16[8,480,128]{2,1,0:T(8,128)(2,1)S(1)}, u32[]{:S(2)}) copy-start(bf16[8,480,128]{2,1,0:T(8,128)(2,1)S(1)} %all-to-all-done.a_ref) | copy-start | bytes 2949124
  35.4 31.8 %collective-permute-start.3 = (bf16[8,480,128]{2,1,0:T(8,128)(2,1)S(1)}, bf16[8,480,128]{2,1,0:T(8,128)(2,1)S(1)}, u32[]{:S(2)}, u32[]{:S(2)}) collective-permute-start(bf16[8,480,128]{2,1,0:T(8,128)(2,1)S(1)} %all-to-all-done.a_ref), channel_id=1, source_target_pairs={{0,8},{8,0},{1,9},{9,1},{2,10},{10,2},{3,11},{11,3},{4,12},{12,4},... | collective-permute-start | bytes 2949128 | tf_op jit(solution)/shard_map/ppermute | solution.py:51
  47.8 27.2 %copy-start.2 = (bf16[128,2048]{1,0:T(8,128)(2,1)}, bf16[128,2048]{1,0:T(8,128)(2,1)S(1)}, u32[]{:S(2)}) copy-start(bf16[128,2048]{1,0:T(8,128)(2,1)S(1)} %collective-permute-done.5.w2) | copy-start | bytes 1572868
  47.8 16.7 %collective-permute-start.6 = (bf16[128,2048]{1,0:T(8,128)(2,1)S(1)}, bf16[128,2048]{1,0:T(8,128)(2,1)S(1)}, u32[]{:S(2)}, u32[]{:S(2)}) collective-permute-start(bf16[128,2048]{1,0:T(8,128)(2,1)S(1)} %collective-permute-done.5.w2), channel_id=1, source_target_pairs={{0,1},{8,15},{1,2},{9,8},{2,3},{10,9},{3,4},{11,10},{4,5},{12,11},... | collective-permute-start | bytes 1572872 | tf_op jit(solution)/shard_map/ppermute | solution.py:59
  52.2 6.6 %collective-permute-start = (bf16[192,256]{1,0:T(8,128)(2,1)}, bf16[192,256]{1,0:T(8,128)(2,1)}, u32[]{:S(2)}, u32[]{:S(2)}) collective-permute-start(bf16[192,256]{1,0:T(8,128)(2,1)} %get-tuple-element.16), channel_id=1, source_target_pairs={{0,16},{16,32},{32,48},{48,0},{1,17},{17,33},{33,49},{49,1},{2,18}... | collective-permute-start | bytes 294920 | tf_op jit(solution)/shard_map/ppermute | solution.py:47
  52.5 9.3 %collective-permute-start.1 = (bf16[192,256]{1,0:T(8,128)(2,1)}, bf16[192,256]{1,0:T(8,128)(2,1)}, u32[]{:S(2)}, u32[]{:S(2)}) collective-permute-start(bf16[192,256]{1,0:T(8,128)(2,1)} %get-tuple-element.15), channel_id=1, source_target_pairs={{0,32},{16,48},{32,0},{48,16},{1,33},{17,49},{33,1},{49,17},{2,34}... | collective-permute-start | bytes 294920 | tf_op jit(solution)/shard_map/ppermute | solution.py:47
  58.8 5.1 %collective-permute-start.2 = (bf16[192,256]{1,0:T(8,128)(2,1)}, bf16[192,256]{1,0:T(8,128)(2,1)S(1)}, u32[]{:S(2)}, u32[]{:S(2)}) collective-permute-start(bf16[192,256]{1,0:T(8,128)(2,1)} %get-tuple-element.14), channel_id=1, source_target_pairs={{0,48},{16,0},{32,16},{48,32},{1,49},{17,1},{33,17},{49,33},{2,50}... | collective-permute-start | bytes 294920 | tf_op jit(solution)/shard_map/ppermute | solution.py:47
  59.6 23.4 %copy-start.10 = (s32[24,4,2]{0,2,1:T(2,128)S(1)}, s32[24,4,2]{0,2,1:T(2,128)}, u32[]{:S(2)}) copy-start(s32[24,4,2]{0,2,1:T(2,128)} %param.26) | copy-start | bytes 2308
  59.6 23.4 %copy-start.11 = (f32[24,4,2]{0,2,1:T(2,128)S(1)}, f32[24,4,2]{0,2,1:T(2,128)}, u32[]{:S(2)}) copy-start(f32[24,4,2]{0,2,1:T(2,128)} %param.25) | copy-start | bytes 2308
  59.6 23.4 %copy-start.12 = (f32[24,4]{0,1:T(4,128)S(1)}, f32[24,4]{0,1:T(4,128)}, u32[]{:S(2)}) copy-start(f32[24,4]{0,1:T(4,128)} %param.24) | copy-start | bytes 1156
  59.6 24.2 %copy-start.8 = (bf16[24,4,2048]{2,1,0:T(4,128)(2,1)S(1)}, bf16[24,4,2048]{2,1,0:T(4,128)(2,1)}, u32[]{:S(2)}) copy-start(bf16[24,4,2048]{2,1,0:T(4,128)(2,1)} %param.15) | copy-start | bytes 1179652
  61.8 20.4 %collective-permute-start.10 = (bf16[64,2048]{1,0:T(8,128)(2,1)}, bf16[64,2048]{1,0:T(8,128)(2,1)}, u32[]{:S(2)}, u32[]{:S(2)}) collective-permute-start(bf16[64,2048]{1,0:T(8,128)(2,1)} %constant_dynamic-slice_fusion), channel_id=1, source_target_pairs={{0,2},{8,14},{1,3},{9,15},{2,4},{10,8},{3,5},{11,9},{4,6},{12,10},... | collective-permute-start | bytes 786440 | tf_op jit(solution)/shard_map/ppermute | solution.py:59
  63.9 28.0 %collective-permute-start.8 = (bf16[128,2048]{1,0:T(8,128)(2,1)S(1)}, bf16[128,2048]{1,0:T(8,128)(2,1)}, u32[]{:S(2)}, u32[]{:S(2)}) collective-permute-start(bf16[128,2048]{1,0:T(8,128)(2,1)S(1)} %collective-permute-done.5.w2), channel_id=1, source_target_pairs={{0,8},{8,0},{1,9},{9,1},{2,10},{10,2},{3,11},{11,3},{4,12},{12,4},... | collective-permute-start | bytes 1572872 | tf_op jit(solution)/shard_map/ppermute | solution.py:51
  63.9 28.0 %collective-permute-start.7 = (bf16[128,2048]{1,0:T(8,128)(2,1)}, bf16[128,2048]{1,0:T(8,128)(2,1)}, u32[]{:S(2)}, u32[]{:S(2)}) collective-permute-start(bf16[128,2048]{1,0:T(8,128)(2,1)} %collective-permute-done.4.w1), channel_id=1, source_target_pairs={{0,8},{8,0},{1,9},{9,1},{2,10},{10,2},{3,11},{11,3},{4,12},{12,4},... | collective-permute-start | bytes 1572872 | tf_op jit(solution)/shard_map/ppermute | solution.py:51
  64.4 20.3 %copy-start.6 = (bf16[128,2048]{1,0:T(8,128)(2,1)}, bf16[128,2048]{1,0:T(8,128)(2,1)S(1)}, u32[]{:S(2)}) copy-start(bf16[128,2048]{1,0:T(8,128)(2,1)S(1)} %collective-permute-done.6.w3) | copy-start | bytes 1572868
  64.4 27.5 %collective-permute-start.9 = (bf16[128,2048]{1,0:T(8,128)(2,1)S(1)}, bf16[128,2048]{1,0:T(8,128)(2,1)}, u32[]{:S(2)}, u32[]{:S(2)}) collective-permute-start(bf16[128,2048]{1,0:T(8,128)(2,1)S(1)} %collective-permute-done.6.w3), channel_id=1, source_target_pairs={{0,8},{8,0},{1,9},{9,1},{2,10},{10,2},{3,11},{11,3},{4,12},{12,4},... | collective-permute-start | bytes 1572872 | tf_op jit(solution)/shard_map/ppermute | solution.py:51
  75.0 16.2 %all-to-all-start.1 = ((bf16[32,24,128]{2,1,0:T(8,128)(2,1)}), bf16[32,24,128]{2,1,0:T(8,128)(2,1)S(1)}, u32[]{:S(2)}, u32[]{:S(2)}) async-start(bf16[32,24,128]{2,1,0:T(8,128)(2,1)} %bitcast.71), calls=%async_computation.1 | async-start | bytes 393216 | tf_op jit(solution)/shard_map/all_to_all | solution.py:303
  82.3 9.7 %collective-permute-start.11 = (bf16[64,2048]{1,0:T(8,128)(2,1)}, bf16[64,2048]{1,0:T(8,128)(2,1)S(1)}, u32[]{:S(2)}, u32[]{:S(2)}) collective-permute-start(bf16[64,2048]{1,0:T(8,128)(2,1)} %collective-permute-done.10.w4), channel_id=1, source_target_pairs={{0,8},{8,0},{1,9},{9,1},{2,10},{10,2},{3,11},{11,3},{4,12},{12,4},... | collective-permute-start | bytes 786440 | tf_op jit(solution)/shard_map/ppermute | solution.py:51
  (5 other events, 5.8 us)
where the time goes:
time: 192 us; the launch traced here: 191 us
  blocking collectives  79 us (41%)
  starting transfers between devices  44.8 us (23%)
  waiting for transfers between devices  27.1 us (14%)
  Pallas kernels  24.1 us (13%)
  local copies, waits for them, and re-layouts  8.9 us (5%)
  other arithmetic  5.93 us (3%)
    all_to_all x2, blocking collectives, exchange(): lax.all_to_all(x, ALL, split_axis=0, concat_axis=0, tiled=True)  79 us
    all_to_all x1, starting transfers between devices, layer(): near = lax.all_to_all(kv, Y, split_axis=0, concat_axis=0, tiled=True)  13.7 us
    ppermute x5, starting transfers between devices, swap(): return lax.ppermute(x, 'core', [(0, 1), (1, 0)])  12.7 us
    all_to_all x1, waiting for transfers between devices, layer(): near = lax.all_to_all(kv, Y, split_axis=0, concat_axis=0, tiled=True)  11.9 us
    ppermute x4, starting transfers between devices, spread(): return lax.ppermute(x, ('core', 'tp'), pairs)  10.8 us
    pallas_call x1, Pallas kernels, layer(): pl.pallas_call(expert_body, out_shape=jax.ShapeDtypeStruct((2048, LANE),...  8.84 us
    ppermute x3, waiting for transfers between devices, shift(): return lax.ppermute(x, axis, [(i, (i + by) % size) for i in range(size)])  8.59 us
    all_to_all x1, starting transfers between devices, layer(): lax.all_to_all(attended, ('quad', 'tp'), split_axis=0, concat_axis=0, til...  7.23 us
  transfers between devices with their start and end apart: 14, of which 4 were waited for; matrix products, arithmetic and copies ran while one was open for 4% of the time, Pallas kernels for 4%

commit v1 on v0

--- a/solution.py
+++ b/solution.py
@@ -9,6 +9,7 @@
 
 D = 2048
 NOPE = 128
+ROPE = 64
 VDIM = 128
 QK = 192
 SEQS = 4
@@ -105,12 +106,9 @@
     return first, second, before
 
 
-def attention_body(at_ref, q_ref, a_ref, b_ref, o_ref, keys, values):
-    quad = at_ref[2]
-    for i in range(16):
-        src = a_ref if i < 8 else b_ref
-        j = i % 8
-        lo, hi = i * 96, 1536 + i * 96
+def load_keys(src, keys, values):
+    for j in range(8):
+        lo, hi = j * 96, 768 + j * 96
         keys[lo : lo + 96, 0:128] = src[j, 0:96, :]
         keys[hi : hi + 96, 0:128] = src[j, 96:192, :]
         values[lo : lo + 96, :] = src[j, 192:288, :]
@@ -120,16 +118,47 @@
         keys[hi : hi + 96, 128:256] = pltpu.roll(rot.astype(jnp.float32), 64, 1).astype(
             jnp.bfloat16
         )
+
+
+def load_query(q_ref, n):
+    base = n * 288
+    rot = q_ref[base + 192 : base + 288, :].astype(jnp.float32)
+    low = lax.broadcasted_iota(jnp.int32, rot.shape, 1) < ROPE
+    first = jnp.where(low, rot, 0.0).astype(jnp.bfloat16)
+    second = jnp.where(low, pltpu.roll(rot, 64, 1), 0.0).astype(jnp.bfloat16)
+    rot = jnp.concatenate([first, second], axis=0)
+    return jnp.concatenate([q_ref[base : base + 192, :], rot], axis=1)
+
+
+def attend(q, keys, values):
+    scores = lax.dot_general(
+        q, keys[...], (((1,), (1,)), ((), ())), preferred_element_type=jnp.float32
+    )
+    highest = jnp.max(scores, axis=-1, keepdims=True)
+    weights = jnp.exp2((scores - highest) * score_scale)
+    totals = jnp.sum(weights, axis=-1, keepdims=True)
+    return highest, totals, dot(weights.astype(jnp.bfloat16), values[...])
+
+
+def attention_near_body(q_ref, a_ref, acc_ref, stat_ref, keys, values):
+    load_keys(a_ref, keys, values)
     for n in range(4):
-        q = q_ref[n * 192 : (n + 1) * 192, :]
-        scores = lax.dot_general(
-            q, keys[...], (((1,), (1,)), ((), ())), preferred_element_type=jnp.float32
-        )
-        highest = jnp.max(scores, axis=-1, keepdims=True)
-        weights = jnp.exp2((scores - highest) * score_scale)
-        totals = jnp.sum(weights, axis=-1, keepdims=True)
-        out = dot(weights.astype(jnp.bfloat16), values[...])
-        o_ref[(quad + 4 - n) % 4] = (out / totals).astype(jnp.bfloat16)
+        highest, totals, out = attend(load_query(q_ref, n), keys, values)
+        acc_ref[n] = out
+        stat_ref[n] = jnp.concatenate([highest + jnp.zeros_like(out), totals + jnp.zeros_like(out)], axis=1)
+
+
+def attention_far_body(at_ref, q_ref, b_ref, acc_ref, stat_ref, o_ref, keys, values):
+    quad = at_ref[2]
+    load_keys(b_ref, keys, values)
+    for n in range(4):
+        highest, totals, out = attend(load_query(q_ref, n), keys, values)
+        before, sums = stat_ref[n, :, 0:128], stat_ref[n, :, 128:256]
+        top = jnp.maximum(highest, before)
+        old = jnp.exp2((before - top) * score_scale)
+        new = jnp.exp2((highest - top) * score_scale)
+        out = (acc_ref[n] * old + out * new) / (sums * old + totals * new)
+        o_ref[(quad + 4 - n) % 4] = out.astype(jnp.bfloat16)
 
 
 def project_body(
@@ -153,13 +182,16 @@
 ):
     tp, core = at_ref[0], at_ref[1]
     turn = 1 - 2 * core
-    projected = dot(att_ref[tp], w0[...])
-    for k, w_ref in ((1, w1), (2, w2), (3, w3), (-1, s1), (-2, s2), (-3, s3)):
-        projected += dot(att_ref[(tp + 8 - turn * k) % 8], w_ref[...])
     last = att_ref[(tp + 4) % 8]
     turned = pltpu.roll(last.astype(jnp.float32), 64, 1).astype(jnp.bfloat16)
     last = jnp.where(core == 0, last, turned)
-    projected += dot(last[:, :64], w4[...]) + dot(last[:, 64:], s4[...])
+    near = jnp.concatenate([att_ref[tp], last], axis=1)
+    projected = dot(near, jnp.concatenate([w0[...], w4[...], s4[...]], axis=0))
+    for k, w_ref, s_ref in ((1, w1, s1), (2, w2, s2), (3, w3, s3)):
+        pair = jnp.concatenate(
+            [att_ref[(tp + 8 - turn * k) % 8], att_ref[(tp + 8 + turn * k) % 8]], axis=1
+        )
+        projected += dot(pair, jnp.concatenate([w_ref[...], s_ref[...]], axis=0))
     stream = (res_ref[...].astype(jnp.float32) + projected).astype(jnp.bfloat16)
     stream_ref[...] = stream
     wide = stream.astype(jnp.float32)
@@ -264,7 +296,8 @@
     positions = spot * block + jnp.arange(block, dtype=jnp.int32)
     q = jnp.swapaxes(query, 0, 1)
     q_rot = rotate(q[..., NOPE:].astype(jnp.float32), positions).astype(jnp.bfloat16)
-    q = jnp.concatenate([q[..., :NOPE], q_rot, jnp.zeros_like(q_rot)], axis=-1)
+    q_rot = jnp.concatenate([q_rot[:, : block // 2], q_rot[:, block // 2 :]], axis=-1)
+    q = jnp.concatenate([q[..., :NOPE], q_rot], axis=1)
     queries = []
     for k in range(4):
         piece = lax.dynamic_index_in_dim(q, (quad + k) % 4, 0, keepdims=False)
@@ -292,13 +325,24 @@
     near = lax.all_to_all(kv, Y, split_axis=0, concat_axis=0, tiled=True)
     far = swap(near)
 
+    scratch = [vmem(8 * block, 256), vmem(8 * block, VDIM)]
+    partial, stats = kernel_call(
+        attention_near_body,
+        out_shape=(
+            jax.ShapeDtypeStruct((4, block, VDIM), jnp.float32),
+            jax.ShapeDtypeStruct((4, block, 2 * VDIM), jnp.float32),
+        ),
+        in_specs=[VM] * 2,
+        out_specs=(VM, VM),
+        scratch_shapes=scratch,
+    )(queries, near)
     attended = kernel_call(
-        attention_body,
+        attention_far_body,
         out_shape=jax.ShapeDtypeStruct((4, block, VDIM), jnp.bfloat16),
-        in_specs=[SM] + [VM] * 3,
+        in_specs=[SM] + [VM] * 4,
         out_specs=VM,
-        scratch_shapes=[vmem(16 * block, 256), vmem(16 * block, VDIM)],
-    )(at, queries, near, far)
+        scratch_shapes=scratch,
+    )(at, queries, far, partial, stats)
     attended = attended.reshape(4 * tp_size, block // tp_size, VDIM)
     attended = lax.all_to_all(attended, ("quad", "tp"), split_axis=0, concat_axis=0, tiled=True)
     attended = attended.reshape(SEQS, tp_size, block // tp_size, VDIM)

time: 192 us -> 190 us (0.990)
  waiting for transfers between devices: 27.1 us -> 23.4 us
  Pallas kernels: 24.1 us -> 26.9 us
    pallas_call x1 -> x2, Pallas kernels: 6.87 us -> 10 us  [the longest x1 5.1 us: layer(): kernel_call(attention_far_body, out_shape=jax.ShapeDtypeStruct((4, block,...]
    ppermute x3, waiting for transfers between devices: 8.59 us -> 6.04 us  [shift(): return lax.ppermute(x, axis, [(i, (i + by) % size) for i in range(size)])]
  transfers between devices with their start and end apart: 14 -> 14, of which waited for: 4 -> 4; matrix products, arithmetic and copies ran while one was open for 4% -> 4% of each run, Pallas kernels for 4% -> 5%
where the time goes in v1:
time: 190 us
  blocking collectives  79 us (42%)
  starting transfers between devices  45.5 us (24%)
  Pallas kernels  26.9 us (14%)
  waiting for transfers between devices  23.4 us (12%)
  local copies, waits for them, and re-layouts  8.65 us (5%)
  other arithmetic  5.03 us (3%)
    all_to_all x2, blocking collectives, exchange(): lax.all_to_all(x, ALL, split_axis=0, concat_axis=0, tiled=True)  79 us
    all_to_all x1, starting transfers between devices, layer(): near = lax.all_to_all(kv, Y, split_axis=0, concat_axis=0, tiled=True)  13.7 us
    ppermute x5, starting transfers between devices, swap(): return lax.ppermute(x, 'core', [(0, 1), (1, 0)])  12.7 us
    all_to_all x1, waiting for transfers between devices, layer(): near = lax.all_to_all(kv, Y, split_axis=0, concat_axis=0, tiled=True)  11.8 us
    ppermute x4, starting transfers between devices, spread(): return lax.ppermute(x, ('core', 'tp'), pairs)  11.2 us
    pallas_call x1, Pallas kernels, layer(): pl.pallas_call(expert_body, out_shape=jax.ShapeDtypeStruct((2048, LANE),...  8.83 us
    all_to_all x1, starting transfers between devices, layer(): lax.all_to_all(attended, ('quad', 'tp'), split_axis=0, concat_axis=0, til...  7.49 us
    ppermute x3, waiting for transfers between devices, shift(): return lax.ppermute(x, axis, [(i, (i + by) % size) for i in range(size)])  6.04 us
  transfers between devices with their start and end apart: 14, of which 4 were waited for; matrix products, arithmetic and copies ran while one was open for 4% of the time, Pallas kernels for 5%

profile of v1, /device:TPU:513, one launch (start us, length us, event | category | flops | bytes accessed | tf_op | source)
XLA Modules:
  0.0 189.8 jit_solution(12143860373285772142)
XLA Ops:
  0.1 1.1 copy.35
  3.2 1.2 maximum_maximum_fusion
  4.4 13.7 %all-to-all-start = ((bf16[8,480,128]{2,1,0:T(8,128)(2,1)}), bf16[8,480,128]{2,1,0:T(8,128)(2,1)S(1)}, u32[]{:S(2)}, u32[]{:S(2)}) async-start(bf16[8,480,128]{2,1,0:T(8,128)(2,1)} %maximum_maximum_fusion), calls=%async_computation | async-start | bytes 1966080 | tf_op jit(solution)/shard_map/all_to_all | solution.py:325
  18.1 4.4 %collective-permute-start.5 = (bf16[128,2048]{1,0:T(8,128)(2,1)S(1)}, bf16[128,2048]{1,0:T(8,128)(2,1)S(1)}, u32[]{:S(2)}, u32[]{:S(2)}) collective-permute-start(bf16[128,2048]{1,0:T(8,128)(2,1)S(1)} %copy-done.4), channel_id=1, source_target_pairs={{0,2},{8,14},{1,3},{9,15},{2,4},{10,8},{3,5},{11,9},{4,6},{12,10},... | collective-permute-start | bytes 1572872 | tf_op jit(solution)/shard_map/ppermute | solution.py:60
  22.5 1.0 collective-permute-start.4
  23.6 11.8 %all-to-all-done.a_ref = bf16[8,480,128]{2,1,0:T(8,128)(2,1)S(1)} async-done(((bf16[8,480,128]{2,1,0:T(8,128)(2,1)}), bf16[8,480,128]{2,1,0:T(8,128)(2,1)S(1)}, u32[]{:S(2)}, u32[]{:S(2)}) %all-to-all-start) | async-done | bytes 983072 | tf_op jit(solution)/shard_map/all_to_all | solution.py:325
  35.4 11.2 %collective-permute-start.3 = (bf16[8,480,128]{2,1,0:T(8,128)(2,1)S(1)}, bf16[8,480,128]{2,1,0:T(8,128)(2,1)}, u32[]{:S(2)}, u32[]{:S(2)}) collective-permute-start(bf16[8,480,128]{2,1,0:T(8,128)(2,1)S(1)} %all-to-all-done.a_ref), channel_id=1, source_target_pairs={{0,8},{8,0},{1,9},{9,1},{2,10},{10,2},{3,11},{11,3},{4,12},{12,4},... | collective-permute-start | bytes 2949128 | tf_op jit(solution)/shard_map/ppermute | solution.py:52
  47.0 3.5 %collective-permute-start.6 = (bf16[128,2048]{1,0:T(8,128)(2,1)S(1)}, bf16[128,2048]{1,0:T(8,128)(2,1)}, u32[]{:S(2)}, u32[]{:S(2)}) collective-permute-start(bf16[128,2048]{1,0:T(8,128)(2,1)S(1)} %collective-permute-done.5.w2), channel_id=1, source_target_pairs={{0,1},{8,15},{1,2},{9,8},{2,3},{10,9},{3,4},{11,10},{4,5},{12,11},... | collective-permute-start | bytes 1572872 | tf_op jit(solution)/shard_map/ppermute | solution.py:60
  51.7 4.3 %collective-permute-done = bf16[288,128]{1,0:T(8,128)(2,1)S(1)} collective-permute-done((bf16[288,128]{1,0:T(8,128)(2,1)S(1)}, bf16[288,128]{1,0:T(8,128)(2,1)S(1)}, u32[]{:S(2)}, u32[]{:S(2)}) %collective-permute-start) | collective-permute-done | bytes 73760 | tf_op jit(solution)/shard_map/ppermute | solution.py:48
  56.8 1.7 collective-permute-done.1
  58.5 2.3 %collective-permute-start.10 = (bf16[64,2048]{1,0:T(8,128)(2,1)}, bf16[64,2048]{1,0:T(8,128)(2,1)S(1)}, u32[]{:S(2)}, u32[]{:S(2)}) collective-permute-start(bf16[64,2048]{1,0:T(8,128)(2,1)} %constant_dynamic-slice_fusion), channel_id=1, source_target_pairs={{0,2},{8,14},{1,3},{9,15},{2,4},{10,8},{3,5},{11,9},{4,6},{12,10},... | collective-permute-start | bytes 786440 | tf_op jit(solution)/shard_map/ppermute | solution.py:60
  61.6 1.7 pad_maximum_fusion.q_ref
  63.3 4.9 %shard_map.145 = (f32[4,192,128]{2,1,0:T(8,128)}, f32[4,192,256]{2,1,0:T(8,128)}) custom-call(bf16[1152,128]{1,0:T(8,128)(2,1)} %pad_maximum_fusion.q_ref, bf16[8,480,128]{2,1,0:T(8,128)(2,1)} %copy-done.1), custom_call_target="tpu_custom_call" | custom-call | tf_op jit(solution)/shard_map/pallas_call | solution.py:329
  68.2 5.1 %shard_map.146 = bf16[4,192,128]{2,1,0:T(8,128)(2,1)} custom-call(s32[3]{0:T(128)} %pad_add_fusion.at_ref, bf16[1152,128]{1,0:T(8,128)(2,1)} %pad_maximum_fusion.q_ref, bf16[8,480,128]{2,1,0:T(8,128)(2,1)} %collective-permute-done.3.b_ref, f32[4,192,128]{2,1,0:T(8,128)} %get-tuple-element.9.acc_ref, f32[4,192,256]{2,1,0:T(8,128)} %get-tuple-element.10.stat_ref), custom_call_target="tpu_custom_call" | custom-call | tf_op jit(solution)/shard_map/pallas_call | solution.py:339
  73.3 7.5 %all-to-all-start.1 = ((bf16[32,24,128]{2,1,0:T(8,128)(2,1)}), bf16[32,24,128]{2,1,0:T(8,128)(2,1)S(1)}, u32[]{:S(2)}, u32[]{:S(2)}) async-start(bf16[32,24,128]{2,1,0:T(8,128)(2,1)} %bitcast.70), calls=%async_computation.1 | async-start | bytes 393216 | tf_op jit(solution)/shard_map/all_to_all | solution.py:347
  80.9 0.7 collective-permute-start.11
  82.3 2.0 %copy.37 = bf16[4,24,2048]{2,1,0:T(8,128)(2,1)} copy(bf16[4,24,2048]{2,0,1:T(4,128)(2,1)} %bitcast.74) | data formatting | bytes 786432 | tf_op jit(solution)/shard_map/transpose | solution.py:351
  84.3 5.5 %all-to-all-done.1 = bf16[32,24,128]{2,1,0:T(8,128)(2,1)S(1)} async-done(((bf16[32,24,128]{2,1,0:T(8,128)(2,1)}), bf16[32,24,128]{2,1,0:T(8,128)(2,1)S(1)}, u32[]{:S(2)}, u32[]{:S(2)}) %all-to-all-start.1) | async-done | bytes 196640 | tf_op jit(solution)/shard_map/all_to_all | solution.py:347
  91.8 5.1 %project.1 = (bf16[96,2048]{1,0:T(8,128)(2,1)}, bf16[2048,256]{1,0:T(8,128)(2,1)}) custom-call(s32[3]{0:T(128)} %pad_add_fusion.at_ref, bf16[8,96,128]{2,1,0:T(8,128)(2,1)} %bitcast.69, bf16[128,2048]{1,0:T(8,128)(2,1)} %w0.1, bf16[128,2048]{1,0:T(8,128)(2,1)} %collective-permute-done.4.w1, bf16[128,2048]{1,0:T(8,128)(2,1)} %copy-done.2, ...), custom_call_target="tpu_custom_call" | custom-call | tf_op jit(solution)/shard_map/project/pallas_call | solution.py:356
  96.9 40.3 %all_to_all.20 = bf16[128,16,256]{2,1,0:T(8,128)(2,1)} all-to-all(bf16[128,16,256]{2,1,0:T(8,128)(2,1)} %bitcast.68), channel_id=1, replica_groups=mesh['grp'=2,'half'=2,'quad'=4,'core'=2,'tp'=8] {'half','quad','core','tp'}, dimensions={0} | all-to-all | bytes 2097152 | tf_op jit(solution)/shard_map/all_to_all | solution.py:371
  137.2 8.8 %experts.1 = bf16[2048,256]{1,0:T(8,128)(2,1)} custom-call(bf16[2048,256]{1,0:T(8,128)(2,1)} %bitcast.58, bf16[2048,768]{1,0:T(8,128)(2,1)} %bitcast.61, bf16[2048,768]{1,0:T(8,128)(2,1)} %bitcast.62, bf16[768,2048]{1,0:T(8,128)(2,1)} %bitcast.63), custom_call_target="tpu_custom_call" | custom-call | tf_op jit(solution)/shard_map/experts/pallas_call | solution.py:376
  146.1 38.7 %all_to_all.21 = bf16[128,16,256]{2,1,0:T(8,128)(2,1)} all-to-all(bf16[128,16,256]{2,1,0:T(8,128)(2,1)} %bitcast.59), channel_id=1, replica_groups=mesh['grp'=2,'half'=2,'quad'=4,'core'=2,'tp'=8] {'half','quad','core','tp'}, dimensions={0} | all-to-all | bytes 2097152 | tf_op jit(solution)/shard_map/all_to_all | solution.py:371
  184.7 3.0 %combine.1 = bf16[96,2048]{1,0:T(8,128)(2,1)} custom-call(bf16[2048,256]{1,0:T(8,128)(2,1)} %bitcast.57, bf16[96,2048]{1,0:T(8,128)(2,1)} %get-tuple-element.12.stream_ref, f32[96,5]{1,0:T(8,128)} %bitcast.73), custom_call_target="tpu_custom_call" | custom-call | tf_op jit(solution)/shard_map/combine/pallas_call | solution.py:392
  187.8 2.0 %copy.47 = bf16[4,24,2048]{2,0,1:T(4,128)(2,1)} copy(bf16[4,24,2048]{2,1,0:T(8,128)(2,1)} %bitcast.67) | data formatting | bytes 786432 | tf_op jit(solution)/shard_map/reshape | solution.py:401
  (73 shorter events, 7.9 us)
Async XLA Ops:
  0.0 2.3 %copy-start = (bf16[512,128]{1,0:T(8,128)(2,1)S(1)}, bf16[512,128]{1,0:T(8,128)(2,1)}, u32[]{:S(2)}) copy-start(bf16[512,128]{1,0:T(8,128)(2,1)} %param.21) | copy-start | bytes 393220
  0.0 2.3 %copy-start.16 = (f32[512]{0:T(512)S(1)}, f32[512]{0:T(512)}, u32[]{:S(2)}) copy-start(f32[512]{0:T(512)} %param.19) | copy-start | bytes 6148
  3.2 14.9 %copy-start.4 = (bf16[128,2048]{1,0:T(8,128)(2,1)S(1)}, bf16[128,2048]{1,0:T(8,128)(2,1)}, u32[]{:S(2)}) copy-start(bf16[128,2048]{1,0:T(8,128)(2,1)} %w0.1) | copy-start | bytes 1572868
  3.2 20.3 %copy-start.8 = (bf16[192,4,192]{2,1,0:T(4,128)(2,1)S(1)}, bf16[192,4,192]{2,1,0:T(4,128)(2,1)}, u32[]{:S(2)}) copy-start(bf16[192,4,192]{2,1,0:T(4,128)(2,1)} %param.16) | copy-start | bytes 884740
  4.4 31.0 %all-to-all-start = ((bf16[8,480,128]{2,1,0:T(8,128)(2,1)}), bf16[8,480,128]{2,1,0:T(8,128)(2,1)S(1)}, u32[]{:S(2)}, u32[]{:S(2)}) async-start(bf16[8,480,128]{2,1,0:T(8,128)(2,1)} %maximum_maximum_fusion), calls=%async_computation | async-start | bytes 1966080 | tf_op jit(solution)/shard_map/all_to_all | solution.py:325
  18.1 28.9 %collective-permute-start.5 = (bf16[128,2048]{1,0:T(8,128)(2,1)S(1)}, bf16[128,2048]{1,0:T(8,128)(2,1)S(1)}, u32[]{:S(2)}, u32[]{:S(2)}) collective-permute-start(bf16[128,2048]{1,0:T(8,128)(2,1)S(1)} %copy-done.4), channel_id=1, source_target_pairs={{0,2},{8,14},{1,3},{9,15},{2,4},{10,8},{3,5},{11,9},{4,6},{12,10},... | collective-permute-start | bytes 1572872 | tf_op jit(solution)/shard_map/ppermute | solution.py:60
  22.5 38.3 %collective-permute-start.4 = (bf16[128,2048]{1,0:T(8,128)(2,1)S(1)}, bf16[128,2048]{1,0:T(8,128)(2,1)}, u32[]{:S(2)}, u32[]{:S(2)}) collective-permute-start(bf16[128,2048]{1,0:T(8,128)(2,1)S(1)} %copy-done.4), channel_id=1, source_target_pairs={{0,1},{8,15},{1,2},{9,8},{2,3},{10,9},{3,4},{11,10},{4,5},{12,11},... | collective-permute-start | bytes 1572872 | tf_op jit(solution)/shard_map/ppermute | solution.py:60
  35.4 15.3 %copy-start.1 = (bf16[8,480,128]{2,1,0:T(8,128)(2,1)}, bf16[8,480,128]{2,1,0:T(8,128)(2,1)S(1)}, u32[]{:S(2)}) copy-start(bf16[8,480,128]{2,1,0:T(8,128)(2,1)S(1)} %all-to-all-done.a_ref) | copy-start | bytes 2949124
  35.4 32.8 %collective-permute-start.3 = (bf16[8,480,128]{2,1,0:T(8,128)(2,1)S(1)}, bf16[8,480,128]{2,1,0:T(8,128)(2,1)}, u32[]{:S(2)}, u32[]{:S(2)}) collective-permute-start(bf16[8,480,128]{2,1,0:T(8,128)(2,1)S(1)} %all-to-all-done.a_ref), channel_id=1, source_target_pairs={{0,8},{8,0},{1,9},{9,1},{2,10},{10,2},{3,11},{11,3},{4,12},{12,4},... | collective-permute-start | bytes 2949128 | tf_op jit(solution)/shard_map/ppermute | solution.py:52
  47.0 21.2 %copy-start.2 = (bf16[128,2048]{1,0:T(8,128)(2,1)}, bf16[128,2048]{1,0:T(8,128)(2,1)S(1)}, u32[]{:S(2)}) copy-start(bf16[128,2048]{1,0:T(8,128)(2,1)S(1)} %collective-permute-done.5.w2) | copy-start | bytes 1572868
  47.0 14.3 %collective-permute-start.6 = (bf16[128,2048]{1,0:T(8,128)(2,1)S(1)}, bf16[128,2048]{1,0:T(8,128)(2,1)}, u32[]{:S(2)}, u32[]{:S(2)}) collective-permute-start(bf16[128,2048]{1,0:T(8,128)(2,1)S(1)} %collective-permute-done.5.w2), channel_id=1, source_target_pairs={{0,1},{8,15},{1,2},{9,8},{2,3},{10,9},{3,4},{11,10},{4,5},{12,11},... | collective-permute-start | bytes 1572872 | tf_op jit(solution)/shard_map/ppermute | solution.py:60
  50.7 5.4 %collective-permute-start = (bf16[288,128]{1,0:T(8,128)(2,1)S(1)}, bf16[288,128]{1,0:T(8,128)(2,1)S(1)}, u32[]{:S(2)}, u32[]{:S(2)}) collective-permute-start(bf16[288,128]{1,0:T(8,128)(2,1)S(1)} %get-tuple-element.20), channel_id=1, source_target_pairs={{0,16},{16,32},{32,48},{48,0},{1,17},{17,33},{33,49},{49,1},{2,18}... | collective-permute-start | bytes 221192 | tf_op jit(solution)/shard_map/ppermute | solution.py:48
  51.1 7.4 %collective-permute-start.1 = (bf16[288,128]{1,0:T(8,128)(2,1)S(1)}, bf16[288,128]{1,0:T(8,128)(2,1)}, u32[]{:S(2)}, u32[]{:S(2)}) collective-permute-start(bf16[288,128]{1,0:T(8,128)(2,1)S(1)} %get-tuple-element.19), channel_id=1, source_target_pairs={{0,32},{16,48},{32,0},{48,16},{1,33},{17,49},{33,1},{49,17},{2,34}... | collective-permute-start | bytes 221192 | tf_op jit(solution)/shard_map/ppermute | solution.py:48
  56.1 4.7 %collective-permute-start.2 = (bf16[288,128]{1,0:T(8,128)(2,1)S(1)}, bf16[288,128]{1,0:T(8,128)(2,1)S(1)}, u32[]{:S(2)}, u32[]{:S(2)}) collective-permute-start(bf16[288,128]{1,0:T(8,128)(2,1)S(1)} %get-tuple-element.18), channel_id=1, source_target_pairs={{0,48},{16,0},{32,16},{48,32},{1,49},{17,1},{33,17},{49,33},{2,50}... | collective-permute-start | bytes 221192 | tf_op jit(solution)/shard_map/ppermute | solution.py:48
  58.5 22.3 %collective-permute-start.10 = (bf16[64,2048]{1,0:T(8,128)(2,1)}, bf16[64,2048]{1,0:T(8,128)(2,1)S(1)}, u32[]{:S(2)}, u32[]{:S(2)}) collective-permute-start(bf16[64,2048]{1,0:T(8,128)(2,1)} %constant_dynamic-slice_fusion), channel_id=1, source_target_pairs={{0,2},{8,14},{1,3},{9,15},{2,4},{10,8},{3,5},{11,9},{4,6},{12,10},... | collective-permute-start | bytes 786440 | tf_op jit(solution)/shard_map/ppermute | solution.py:60
  60.8 29.7 %collective-permute-start.8 = (bf16[128,2048]{1,0:T(8,128)(2,1)S(1)}, bf16[128,2048]{1,0:T(8,128)(2,1)S(1)}, u32[]{:S(2)}, u32[]{:S(2)}) collective-permute-start(bf16[128,2048]{1,0:T(8,128)(2,1)S(1)} %collective-permute-done.5.w2), channel_id=1, source_target_pairs={{0,8},{8,0},{1,9},{9,1},{2,10},{10,2},{3,11},{11,3},{4,12},{12,4},... | collective-permute-start | bytes 1572872 | tf_op jit(solution)/shard_map/ppermute | solution.py:52
  60.8 29.8 %collective-permute-start.7 = (bf16[128,2048]{1,0:T(8,128)(2,1)}, bf16[128,2048]{1,0:T(8,128)(2,1)S(1)}, u32[]{:S(2)}, u32[]{:S(2)}) collective-permute-start(bf16[128,2048]{1,0:T(8,128)(2,1)} %collective-permute-done.4.w1), channel_id=1, source_target_pairs={{0,8},{8,0},{1,9},{9,1},{2,10},{10,2},{3,11},{11,3},{4,12},{12,4},... | collective-permute-start | bytes 1572872 | tf_op jit(solution)/shard_map/ppermute | solution.py:52
  61.3 29.3 %collective-permute-start.9 = (bf16[128,2048]{1,0:T(8,128)(2,1)}, bf16[128,2048]{1,0:T(8,128)(2,1)S(1)}, u32[]{:S(2)}, u32[]{:S(2)}) collective-permute-start(bf16[128,2048]{1,0:T(8,128)(2,1)} %collective-permute-done.6.w3), channel_id=1, source_target_pairs={{0,8},{8,0},{1,9},{9,1},{2,10},{10,2},{3,11},{11,3},{4,12},{12,4},... | collective-permute-start | bytes 1572872 | tf_op jit(solution)/shard_map/ppermute | solution.py:52
  63.3 18.3 %copy-start.12 = (s32[24,4,2]{0,2,1:T(2,128)S(1)}, s32[24,4,2]{0,2,1:T(2,128)}, u32[]{:S(2)}) copy-start(s32[24,4,2]{0,2,1:T(2,128)} %param.26) | copy-start | bytes 2308
  63.3 18.3 %copy-start.13 = (f32[24,4,2]{0,2,1:T(2,128)S(1)}, f32[24,4,2]{0,2,1:T(2,128)}, u32[]{:S(2)}) copy-start(f32[24,4,2]{0,2,1:T(2,128)} %param.25) | copy-start | bytes 2308
  63.3 18.3 %copy-start.14 = (f32[24,4]{0,1:T(4,128)S(1)}, f32[24,4]{0,1:T(4,128)}, u32[]{:S(2)}) copy-start(f32[24,4]{0,1:T(4,128)} %param.24) | copy-start | bytes 1156
  73.3 16.5 %all-to-all-start.1 = ((bf16[32,24,128]{2,1,0:T(8,128)(2,1)}), bf16[32,24,128]{2,1,0:T(8,128)(2,1)S(1)}, u32[]{:S(2)}, u32[]{:S(2)}) async-start(bf16[32,24,128]{2,1,0:T(8,128)(2,1)} %bitcast.70), calls=%async_computation.1 | async-start | bytes 393216 | tf_op jit(solution)/shard_map/all_to_all | solution.py:347
  80.8 9.8 %copy-start.9 = (bf16[64,2048]{1,0:T(8,128)(2,1)}, bf16[64,2048]{1,0:T(8,128)(2,1)S(1)}, u32[]{:S(2)}) copy-start(bf16[64,2048]{1,0:T(8,128)(2,1)S(1)} %collective-permute-done.10.w4) | copy-start | bytes 786436
  80.9 9.7 %collective-permute-start.11 = (bf16[64,2048]{1,0:T(8,128)(2,1)S(1)}, bf16[64,2048]{1,0:T(8,128)(2,1)S(1)}, u32[]{:S(2)}, u32[]{:S(2)}) collective-permute-start(bf16[64,2048]{1,0:T(8,128)(2,1)S(1)} %collective-permute-done.10.w4), channel_id=1, source_target_pairs={{0,8},{8,0},{1,9},{9,1},{2,10},{10,2},{3,11},{11,3},{4,12},{12,4},... | collective-permute-start | bytes 786440 | tf_op jit(solution)/shard_map/ppermute | solution.py:52
  (7 other events, 7.5 us)

commit v2 on v1

--- a/solution.py
+++ b/solution.py
@@ -206,31 +206,19 @@
     pack_rows(rows, out_ref, packing(False))
 
 
-def expert_body(in_ref, gate_ref, up_ref, down_ref, out_ref, rows, acc):
-    step = pl.program_id(0)
-
-    @pl.when(step == 0)
-    def _():
-        unpack_rows(in_ref, rows, packing(True))
-
+def expert_body(in_ref, gate_ref, up_ref, down_ref, out_ref, rows):
+    unpack_rows(in_ref, rows, packing(True))
     x = rows[...]
-    gate = dot(x, gate_ref[...])
-    up = dot(x, up_ref[...])
-    hidden = (gate / (1.0 + jnp.exp(-gate)) * up).astype(jnp.bfloat16)
-    part = dot(hidden, down_ref[...])
-
-    @pl.when(step == 0)
-    def _():
-        acc[...] = part
-
-    @pl.when(step > 0)
-    def _():
-        acc[...] += part
-
-    @pl.when(step == pl.num_programs(0) - 1)
-    def _():
-        rows[...] = acc[...].astype(jnp.bfloat16)
-        pack_rows(rows, out_ref, packing(False))
+    hid = []
+    for n in range(0, gate_ref.shape[1], 256):
+        gate = dot(x, gate_ref[:, n : n + 256])
+        up = dot(x, up_ref[:, n : n + 256])
+        hidden = (gate / (1.0 + jnp.exp(-gate)) * up).astype(jnp.bfloat16)
+        hid.append(hidden)
+    hidden = jnp.concatenate(hid, axis=1)
+    for n in range(0, D, 512):
+        rows[:, n : n + 512] = dot(hidden, down_ref[:, n : n + 512]).astype(jnp.bfloat16)
+    pack_rows(rows, out_ref, packing(False))
 
 
 def combine_body(in_ref, stream_ref, meta_ref, out_ref, rows):
@@ -255,12 +243,12 @@
     return pltpu.VMEM(shape, jnp.bfloat16)
 
 
-def params():
-    return pltpu.CompilerParams(vmem_limit_bytes=56 * 1024 * 1024)
-
-
-def kernel_call(body, **options):
-    return pl.pallas_call(body, compiler_params=params(), **options)
+def params(mib):
+    return pltpu.CompilerParams(vmem_limit_bytes=mib * 1024 * 1024)
+
+
+def kernel_call(body, limit, **options):
+    return pl.pallas_call(body, compiler_params=params(limit), **options)
 
 
 VM = pl.BlockSpec(memory_space=pltpu.VMEM)
@@ -314,6 +302,7 @@
     rot = jnp.concatenate([rot[:, : block // 2], rot[:, block // 2 :]], axis=-1)
     kv = jnp.concatenate([keys, vals, rot], axis=1).astype(jnp.bfloat16)
     kv = jnp.concatenate([kv, kv], axis=0)
+    kv, at = lax.optimization_barrier((kv, at))
     half_rows = out_weight.shape[0] // 2
     one, two = spread(out_weight, 1, tp_size), spread(out_weight, 2, tp_size)
     three = spread(two, 1, tp_size)
@@ -328,6 +317,7 @@
     scratch = [vmem(8 * block, 256), vmem(8 * block, VDIM)]
     partial, stats = kernel_call(
         attention_near_body,
+        limit=12,
         out_shape=(
             jax.ShapeDtypeStruct((4, block, VDIM), jnp.float32),
             jax.ShapeDtypeStruct((4, block, 2 * VDIM), jnp.float32),
@@ -338,6 +328,7 @@
     )(queries, near)
     attended = kernel_call(
         attention_far_body,
+        limit=12,
         out_shape=jax.ShapeDtypeStruct((4, block, VDIM), jnp.bfloat16),
         in_specs=[SM] + [VM] * 4,
         out_specs=VM,
@@ -353,8 +344,9 @@
         [routes.astype(jnp.float32), pair_logits, group_prob[..., None]], axis=-1
     )
     meta = jnp.swapaxes(meta, 0, 1).reshape(rows, 5)
-    stream, outgoing = pl.pallas_call(
+    stream, outgoing = kernel_call(
         project_body,
+        limit=10,
         out_shape=(
             jax.ShapeDtypeStruct((rows, D), jnp.bfloat16),
             jax.ShapeDtypeStruct((2048, LANE), jnp.bfloat16),
@@ -362,8 +354,6 @@
         in_specs=[SM] + [VM] * 13,
         out_specs=(VM, VM),
         scratch_shapes=[vmem(256, D)],
-        compiler_params=params(),
-        name="project",
     )(at, attended, *weights, res, norm_gain.reshape(1, D), meta)
 
     def exchange(x):
@@ -371,32 +361,22 @@
         return lax.all_to_all(x, ALL, split_axis=0, concat_axis=0, tiled=True).reshape(2048, LANE)
 
     arrived = exchange(outgoing)
-    hidden = w_gate.shape[2]
-    step = 256
-    served = pl.pallas_call(
+    served = kernel_call(
         expert_body,
+        limit=10,
         out_shape=jax.ShapeDtypeStruct((2048, LANE), jnp.bfloat16),
-        grid=(hidden // step,),
-        in_specs=[
-            pl.BlockSpec((2048, LANE), lambda i: (0, 0)),
-            pl.BlockSpec((D, step), lambda i: (0, i)),
-            pl.BlockSpec((D, step), lambda i: (0, i)),
-            pl.BlockSpec((step, D), lambda i: (i, 0)),
-        ],
-        out_specs=pl.BlockSpec((2048, LANE), lambda i: (0, 0)),
-        scratch_shapes=[vmem(256, D), pltpu.VMEM((256, D), jnp.float32)],
-        compiler_params=params(),
-        name="experts",
+        in_specs=[VM] * 4,
+        out_specs=VM,
+        scratch_shapes=[vmem(256, D)],
     )(arrived, w_gate[0], w_up[0], w_down[0])
     returned = exchange(served)
-    combined = pl.pallas_call(
+    combined = kernel_call(
         combine_body,
+        limit=8,
         out_shape=jax.ShapeDtypeStruct((rows, D), jnp.bfloat16),
         in_specs=[VM] * 3,
         out_specs=VM,
         scratch_shapes=[vmem(256, D)],
-        compiler_params=params(),
-        name="combine",
     )(returned, stream, meta)
     return jnp.swapaxes(combined.reshape(SEQS, rows // SEQS, D), 0, 1)
 

time: 190 us -> 178 us (0.937)
  Pallas kernels: 26.9 us -> 15 us
  local copies, waits for them, and re-layouts: 8.65 us -> 11.9 us
  blocking collectives: 79 us -> 77.1 us
    pallas_call x5, Pallas kernels: 26.9 us -> 15 us  [the longest x1 4.03 us: layer(): kernel_call(attention_far_body, limit=12, out_shape=jax.ShapeDtypeStruct(...]
    unnamed x35 -> x39, local copies, waits for them, and re-layouts: 1.3 us -> 5 us
  transfers between devices with their start and end apart: 14 -> 14, of which waited for: 4 -> 4; matrix products, arithmetic and copies ran while one was open for 4% -> 3% of each run, Pallas kernels for 5% -> 4%
where the time goes in v2:
time: 178 us
  blocking collectives  77.1 us (43%)
  starting transfers between devices  45.6 us (26%)
  waiting for transfers between devices  22.9 us (13%)
  Pallas kernels  15 us (8%)
  local copies, waits for them, and re-layouts  11.9 us (7%)
  other arithmetic  3.65 us (2%)
    all_to_all x2, blocking collectives, exchange(): lax.all_to_all(x, ALL, split_axis=0, concat_axis=0, tiled=True)  77.1 us
    all_to_all x1, starting transfers between devices, layer(): near = lax.all_to_all(kv, Y, split_axis=0, concat_axis=0, tiled=True)  13.7 us
    ppermute x5, starting transfers between devices, swap(): return lax.ppermute(x, 'core', [(0, 1), (1, 0)])  12.7 us
    ppermute x4, starting transfers between devices, spread(): return lax.ppermute(x, ('core', 'tp'), pairs)  11.2 us
    all_to_all x1, waiting for transfers between devices, layer(): near = lax.all_to_all(kv, Y, split_axis=0, concat_axis=0, tiled=True)  11.1 us
    all_to_all x1, starting transfers between devices, layer(): lax.all_to_all(attended, ('quad', 'tp'), split_axis=0, concat_axis=0, til...  7.6 us
    all_to_all x1, waiting for transfers between devices, layer(): lax.all_to_all(attended, ('quad', 'tp'), split_axis=0, concat_axis=0, til...  6.18 us
    ppermute x3, waiting for transfers between devices, shift(): return lax.ppermute(x, axis, [(i, (i + by) % size) for i in range(size)])  5.64 us
  transfers between devices with their start and end apart: 14, of which 4 were waited for; matrix products, arithmetic and copies ran while one was open for 3% of the time, Pallas kernels for 4%

profile of v2, /device:TPU:513, one launch (start us, length us, event | category | flops | bytes accessed | tf_op | source)
XLA Modules:
  0.0 177.6 jit_solution(17871587469399015007)
XLA Ops:
  0.1 1.1 copy.34
  3.3 1.1 maximum_maximum_fusion
  4.5 13.7 %all-to-all-start = ((bf16[8,480,128]{2,1,0:T(8,128)(2,1)}), bf16[8,480,128]{2,1,0:T(8,128)(2,1)S(1)}, u32[]{:S(2)}, u32[]{:S(2)}) async-start(bf16[8,480,128]{2,1,0:T(8,128)(2,1)} %maximum_maximum_fusion), calls=%async_computation | async-start | bytes 1966080 | tf_op jit(solution)/shard_map/all_to_all | solution.py:314
  18.2 4.4 %collective-permute-start.5 = (bf16[128,2048]{1,0:T(8,128)(2,1)S(1)}, bf16[128,2048]{1,0:T(8,128)(2,1)}, u32[]{:S(2)}, u32[]{:S(2)}) collective-permute-start(bf16[128,2048]{1,0:T(8,128)(2,1)S(1)} %copy-done.7), channel_id=1, source_target_pairs={{0,2},{8,14},{1,3},{9,15},{2,4},{10,8},{3,5},{11,9},{4,6},{12,10},... | collective-permute-start | bytes 1572872 | tf_op jit(solution)/shard_map/ppermute | solution.py:60
  22.5 1.0 collective-permute-start.4
  24.4 11.1 %all-to-all-done.a_ref = bf16[8,480,128]{2,1,0:T(8,128)(2,1)S(1)} async-done(((bf16[8,480,128]{2,1,0:T(8,128)(2,1)}), bf16[8,480,128]{2,1,0:T(8,128)(2,1)S(1)}, u32[]{:S(2)}, u32[]{:S(2)}) %all-to-all-start) | async-done | bytes 983072 | tf_op jit(solution)/shard_map/all_to_all | solution.py:314
  35.4 11.2 %collective-permute-start.3 = (bf16[8,480,128]{2,1,0:T(8,128)(2,1)S(1)}, bf16[8,480,128]{2,1,0:T(8,128)(2,1)S(1)}, u32[]{:S(2)}, u32[]{:S(2)}) collective-permute-start(bf16[8,480,128]{2,1,0:T(8,128)(2,1)S(1)} %all-to-all-done.a_ref), channel_id=1, source_target_pairs={{0,8},{8,0},{1,9},{9,1},{2,10},{10,2},{3,11},{11,3},{4,12},{12,4},... | collective-permute-start | bytes 2949128 | tf_op jit(solution)/shard_map/ppermute | solution.py:52
  46.6 1.1 subtract_convert_fusion
  48.8 3.5 %collective-permute-start.6 = (bf16[128,2048]{1,0:T(8,128)(2,1)}, bf16[128,2048]{1,0:T(8,128)(2,1)}, u32[]{:S(2)}, u32[]{:S(2)}) collective-permute-start(bf16[128,2048]{1,0:T(8,128)(2,1)} %collective-permute-done.5.w2), channel_id=1, source_target_pairs={{0,1},{8,15},{1,2},{9,8},{2,3},{10,9},{3,4},{11,10},{4,5},{12,11},... | collective-permute-start | bytes 1572872 | tf_op jit(solution)/shard_map/ppermute | solution.py:60
  52.9 5.0 %collective-permute-done = bf16[288,128]{1,0:T(8,128)(2,1)S(1)} collective-permute-done((bf16[288,128]{1,0:T(8,128)(2,1)S(1)}, bf16[288,128]{1,0:T(8,128)(2,1)S(1)}, u32[]{:S(2)}, u32[]{:S(2)}) %collective-permute-start) | collective-permute-done | bytes 73760 | tf_op jit(solution)/shard_map/ppermute | solution.py:48
  57.9 1.7 constant_dynamic-slice_fusion
  60.2 2.3 %collective-permute-start.10 = (bf16[64,2048]{1,0:T(8,128)(2,1)}, bf16[64,2048]{1,0:T(8,128)(2,1)}, u32[]{:S(2)}, u32[]{:S(2)}) collective-permute-start(bf16[64,2048]{1,0:T(8,128)(2,1)} %constant_dynamic-slice_fusion), channel_id=1, source_target_pairs={{0,2},{8,14},{1,3},{9,15},{2,4},{10,8},{3,5},{11,9},{4,6},{12,10},... | collective-permute-start | bytes 786440 | tf_op jit(solution)/shard_map/ppermute | solution.py:60
  63.4 2.7 %shard_map.145 = (f32[4,192,128]{2,1,0:T(8,128)S(1)}, f32[4,192,256]{2,1,0:T(8,128)S(1)}) custom-call(bf16[1152,128]{1,0:T(8,128)(2,1)S(1)} %pad_maximum_fusion.q_ref, bf16[8,480,128]{2,1,0:T(8,128)(2,1)S(1)} %all-to-all-done.a_ref), custom_call_target="tpu_custom_call" | custom-call | tf_op jit(solution)/shard_map/pallas_call | solution.py:318
  67.1 1.2 copy-done.6
  68.3 4.0 %shard_map.146 = bf16[4,192,128]{2,1,0:T(8,128)(2,1)} custom-call(s32[3]{0:T(128)S(1)} %pad_add_fusion.at_ref, bf16[1152,128]{1,0:T(8,128)(2,1)S(1)} %pad_maximum_fusion.q_ref, bf16[8,480,128]{2,1,0:T(8,128)(2,1)S(1)} %copy-done.6, f32[4,192,128]{2,1,0:T(8,128)S(1)} %get-tuple-element.13.acc_ref, f32[4,192,256]{2,1,0:T(8,128)S(1)} %get-tuple-element.14.stat_ref), custom_call_target="tpu_custom_call" | custom-call | tf_op jit(solution)/shard_map/pallas_call | solution.py:329
  72.4 7.6 %all-to-all-start.1 = ((bf16[32,24,128]{2,1,0:T(8,128)(2,1)}), bf16[32,24,128]{2,1,0:T(8,128)(2,1)S(1)}, u32[]{:S(2)}, u32[]{:S(2)}) async-start(bf16[32,24,128]{2,1,0:T(8,128)(2,1)} %bitcast.12), calls=%async_computation.1 | async-start | bytes 393216 | tf_op jit(solution)/shard_map/all_to_all | solution.py:338
  80.8 2.0 %copy.37 = bf16[4,24,2048]{2,1,0:T(8,128)(2,1)} copy(bf16[4,24,2048]{2,0,1:T(4,128)(2,1)} %bitcast.74) | data formatting | bytes 786432 | tf_op jit(solution)/shard_map/transpose | solution.py:342
  82.8 6.2 %all-to-all-done.1 = bf16[32,24,128]{2,1,0:T(8,128)(2,1)S(1)} async-done(((bf16[32,24,128]{2,1,0:T(8,128)(2,1)}), bf16[32,24,128]{2,1,0:T(8,128)(2,1)S(1)}, u32[]{:S(2)}, u32[]{:S(2)}) %all-to-all-start.1) | async-done | bytes 196640 | tf_op jit(solution)/shard_map/all_to_all | solution.py:338
  90.1 1.0 copy-done.8
  91.1 3.9 %shard_map.147 = (bf16[96,2048]{1,0:T(8,128)(2,1)S(1)}, bf16[2048,256]{1,0:T(8,128)(2,1)S(1)}) custom-call(s32[3]{0:T(128)S(1)} %pad_add_fusion.at_ref, bf16[8,96,128]{2,1,0:T(8,128)(2,1)S(1)} %bitcast.66, bf16[128,2048]{1,0:T(8,128)(2,1)S(1)} %copy-done.8, bf16[128,2048]{1,0:T(8,128)(2,1)} %collective-permute-done.4.w1, ...), custom_call_target="tpu_custom_call" | custom-call | tf_op jit(solution)/shard_map/pallas_call | solution.py:347
  95.0 38.8 %all_to_all.20 = bf16[128,16,256]{2,1,0:T(8,128)(2,1)S(1)} all-to-all(bf16[128,16,256]{2,1,0:T(8,128)(2,1)S(1)} %bitcast.65), channel_id=1, replica_groups=mesh['grp'=2,'half'=2,'quad'=4,'core'=2,'tp'=8] {'half','quad','core','tp'}, dimensions={0} | all-to-all | bytes 2097152 | tf_op jit(solution)/shard_map/all_to_all | solution.py:361
  133.8 3.4 %shard_map.148 = bf16[2048,256]{1,0:T(8,128)(2,1)S(1)} custom-call(bf16[2048,256]{1,0:T(8,128)(2,1)S(1)} %bitcast.58, bf16[2048,768]{1,0:T(8,128)(2,1)S(1)} %bitcast.60, bf16[2048,768]{1,0:T(8,128)(2,1)S(1)} %bitcast.61, bf16[768,2048]{1,0:T(8,128)(2,1)S(1)} %bitcast.62), custom_call_target="tpu_custom_call" | custom-call | tf_op jit(solution)/shard_map/pallas_call | solution.py:364
  137.2 38.4 %all_to_all.21 = bf16[128,16,256]{2,1,0:T(8,128)(2,1)S(1)} all-to-all(bf16[128,16,256]{2,1,0:T(8,128)(2,1)S(1)} %bitcast.59), channel_id=1, replica_groups=mesh['grp'=2,'half'=2,'quad'=4,'core'=2,'tp'=8] {'half','quad','core','tp'}, dimensions={0} | all-to-all | bytes 2097152 | tf_op jit(solution)/shard_map/all_to_all | solution.py:361
  176.5 1.1 copy.47
  (77 shorter events, 9.7 us)
Async XLA Ops:
  0.0 2.3 %copy-start.18 = (f32[512]{0:T(512)S(1)}, f32[512]{0:T(512)}, u32[]{:S(2)}) copy-start(f32[512]{0:T(512)} %param.19) | copy-start | bytes 6148
  3.2 14.9 %copy-start.7 = (bf16[128,2048]{1,0:T(8,128)(2,1)S(1)}, bf16[128,2048]{1,0:T(8,128)(2,1)}, u32[]{:S(2)}) copy-start(bf16[128,2048]{1,0:T(8,128)(2,1)} %w0.1) | copy-start | bytes 1572868
  3.2 20.3 %copy-start.13 = (bf16[192,4,192]{2,1,0:T(4,128)(2,1)S(1)}, bf16[192,4,192]{2,1,0:T(4,128)(2,1)}, u32[]{:S(2)}) copy-start(bf16[192,4,192]{2,1,0:T(4,128)(2,1)} %param.16) | copy-start | bytes 884740
  4.5 31.0 %all-to-all-start = ((bf16[8,480,128]{2,1,0:T(8,128)(2,1)}), bf16[8,480,128]{2,1,0:T(8,128)(2,1)S(1)}, u32[]{:S(2)}, u32[]{:S(2)}) async-start(bf16[8,480,128]{2,1,0:T(8,128)(2,1)} %maximum_maximum_fusion), calls=%async_computation | async-start | bytes 1966080 | tf_op jit(solution)/shard_map/all_to_all | solution.py:314
  18.2 30.7 %collective-permute-start.5 = (bf16[128,2048]{1,0:T(8,128)(2,1)S(1)}, bf16[128,2048]{1,0:T(8,128)(2,1)}, u32[]{:S(2)}, u32[]{:S(2)}) collective-permute-start(bf16[128,2048]{1,0:T(8,128)(2,1)S(1)} %copy-done.7), channel_id=1, source_target_pairs={{0,2},{8,14},{1,3},{9,15},{2,4},{10,8},{3,5},{11,9},{4,6},{12,10},... | collective-permute-start | bytes 1572872 | tf_op jit(solution)/shard_map/ppermute | solution.py:60
  22.5 40.0 %collective-permute-start.4 = (bf16[128,2048]{1,0:T(8,128)(2,1)S(1)}, bf16[128,2048]{1,0:T(8,128)(2,1)}, u32[]{:S(2)}, u32[]{:S(2)}) collective-permute-start(bf16[128,2048]{1,0:T(8,128)(2,1)S(1)} %copy-done.7), channel_id=1, source_target_pairs={{0,1},{8,15},{1,2},{9,8},{2,3},{10,9},{3,4},{11,10},{4,5},{12,11},... | collective-permute-start | bytes 1572872 | tf_op jit(solution)/shard_map/ppermute | solution.py:60
  35.4 30.7 %collective-permute-start.3 = (bf16[8,480,128]{2,1,0:T(8,128)(2,1)S(1)}, bf16[8,480,128]{2,1,0:T(8,128)(2,1)S(1)}, u32[]{:S(2)}, u32[]{:S(2)}) collective-permute-start(bf16[8,480,128]{2,1,0:T(8,128)(2,1)S(1)} %all-to-all-done.a_ref), channel_id=1, source_target_pairs={{0,8},{8,0},{1,9},{9,1},{2,10},{10,2},{3,11},{11,3},{4,12},{12,4},... | collective-permute-start | bytes 2949128 | tf_op jit(solution)/shard_map/ppermute | solution.py:52
  48.8 14.2 %collective-permute-start.6 = (bf16[128,2048]{1,0:T(8,128)(2,1)}, bf16[128,2048]{1,0:T(8,128)(2,1)}, u32[]{:S(2)}, u32[]{:S(2)}) collective-permute-start(bf16[128,2048]{1,0:T(8,128)(2,1)} %collective-permute-done.5.w2), channel_id=1, source_target_pairs={{0,1},{8,15},{1,2},{9,8},{2,3},{10,9},{3,4},{11,10},{4,5},{12,11},... | collective-permute-start | bytes 1572872 | tf_op jit(solution)/shard_map/ppermute | solution.py:60
  52.5 5.4 %collective-permute-start = (bf16[288,128]{1,0:T(8,128)(2,1)S(1)}, bf16[288,128]{1,0:T(8,128)(2,1)S(1)}, u32[]{:S(2)}, u32[]{:S(2)}) collective-permute-start(bf16[288,128]{1,0:T(8,128)(2,1)S(1)} %get-tuple-element.24), channel_id=1, source_target_pairs={{0,16},{16,32},{32,48},{48,0},{1,17},{17,33},{33,49},{49,1},{2,18}... | collective-permute-start | bytes 221192 | tf_op jit(solution)/shard_map/ppermute | solution.py:48
  52.9 7.3 %collective-permute-start.1 = (bf16[288,128]{1,0:T(8,128)(2,1)S(1)}, bf16[288,128]{1,0:T(8,128)(2,1)S(1)}, u32[]{:S(2)}, u32[]{:S(2)}) collective-permute-start(bf16[288,128]{1,0:T(8,128)(2,1)S(1)} %get-tuple-element.23), channel_id=1, source_target_pairs={{0,32},{16,48},{32,0},{48,16},{1,33},{17,49},{33,1},{49,17},{2,34}... | collective-permute-start | bytes 221192 | tf_op jit(solution)/shard_map/ppermute | solution.py:48
  57.9 4.6 %collective-permute-start.2 = (bf16[288,128]{1,0:T(8,128)(2,1)S(1)}, bf16[288,128]{1,0:T(8,128)(2,1)S(1)}, u32[]{:S(2)}, u32[]{:S(2)}) collective-permute-start(bf16[288,128]{1,0:T(8,128)(2,1)S(1)} %get-tuple-element.22), channel_id=1, source_target_pairs={{0,48},{16,0},{32,16},{48,32},{1,49},{17,1},{33,17},{49,33},{2,50}... | collective-permute-start | bytes 221192 | tf_op jit(solution)/shard_map/ppermute | solution.py:48
  60.2 19.8 %collective-permute-start.10 = (bf16[64,2048]{1,0:T(8,128)(2,1)}, bf16[64,2048]{1,0:T(8,128)(2,1)}, u32[]{:S(2)}, u32[]{:S(2)}) collective-permute-start(bf16[64,2048]{1,0:T(8,128)(2,1)} %constant_dynamic-slice_fusion), channel_id=1, source_target_pairs={{0,2},{8,14},{1,3},{9,15},{2,4},{10,8},{3,5},{11,9},{4,6},{12,10},... | collective-permute-start | bytes 786440 | tf_op jit(solution)/shard_map/ppermute | solution.py:60
  62.5 26.5 %collective-permute-start.8 = (bf16[128,2048]{1,0:T(8,128)(2,1)}, bf16[128,2048]{1,0:T(8,128)(2,1)}, u32[]{:S(2)}, u32[]{:S(2)}) collective-permute-start(bf16[128,2048]{1,0:T(8,128)(2,1)} %collective-permute-done.5.w2), channel_id=1, source_target_pairs={{0,8},{8,0},{1,9},{9,1},{2,10},{10,2},{3,11},{11,3},{4,12},{12,4},... | collective-permute-start | bytes 1572872 | tf_op jit(solution)/shard_map/ppermute | solution.py:52
  62.5 26.5 %collective-permute-start.7 = (bf16[128,2048]{1,0:T(8,128)(2,1)}, bf16[128,2048]{1,0:T(8,128)(2,1)}, u32[]{:S(2)}, u32[]{:S(2)}) collective-permute-start(bf16[128,2048]{1,0:T(8,128)(2,1)} %collective-permute-done.4.w1), channel_id=1, source_target_pairs={{0,8},{8,0},{1,9},{9,1},{2,10},{10,2},{3,11},{11,3},{4,12},{12,4},... | collective-permute-start | bytes 1572872 | tf_op jit(solution)/shard_map/ppermute | solution.py:52
  63.0 26.0 %collective-permute-start.9 = (bf16[128,2048]{1,0:T(8,128)(2,1)}, bf16[128,2048]{1,0:T(8,128)(2,1)}, u32[]{:S(2)}, u32[]{:S(2)}) collective-permute-start(bf16[128,2048]{1,0:T(8,128)(2,1)} %collective-permute-done.6.w3), channel_id=1, source_target_pairs={{0,8},{8,0},{1,9},{9,1},{2,10},{10,2},{3,11},{11,3},{4,12},{12,4},... | collective-permute-start | bytes 1572872 | tf_op jit(solution)/shard_map/ppermute | solution.py:52
  63.4 17.3 %copy-start.14 = (s32[24,4,2]{0,2,1:T(2,128)S(1)}, s32[24,4,2]{0,2,1:T(2,128)}, u32[]{:S(2)}) copy-start(s32[24,4,2]{0,2,1:T(2,128)} %param.26) | copy-start | bytes 2308
  63.4 17.3 %copy-start.15 = (f32[24,4,2]{0,2,1:T(2,128)S(1)}, f32[24,4,2]{0,2,1:T(2,128)}, u32[]{:S(2)}) copy-start(f32[24,4,2]{0,2,1:T(2,128)} %param.25) | copy-start | bytes 2308
  63.4 17.3 %copy-start.16 = (f32[24,4]{0,1:T(4,128)S(1)}, f32[24,4]{0,1:T(4,128)}, u32[]{:S(2)}) copy-start(f32[24,4]{0,1:T(4,128)} %param.24) | copy-start | bytes 1156
  68.3 20.7 %copy-start.9 = (f32[2048]{0:T(1024)S(1)}, f32[2048]{0:T(1024)}, u32[]{:S(2)}) copy-start(f32[2048]{0:T(1024)} %param.23) | copy-start | bytes 24580
  68.3 65.4 %copy-start.3 = (bf16[1,768,2048]{2,1,0:T(8,128)(2,1)S(1)}, bf16[1,768,2048]{2,1,0:T(8,128)(2,1)}, u32[]{:S(2)}) copy-start(bf16[1,768,2048]{2,1,0:T(8,128)(2,1)} %param.29) | copy-start | bytes 9437188
  72.4 16.6 %all-to-all-start.1 = ((bf16[32,24,128]{2,1,0:T(8,128)(2,1)}), bf16[32,24,128]{2,1,0:T(8,128)(2,1)S(1)}, u32[]{:S(2)}, u32[]{:S(2)}) async-start(bf16[32,24,128]{2,1,0:T(8,128)(2,1)} %bitcast.12), calls=%async_computation.1 | async-start | bytes 393216 | tf_op jit(solution)/shard_map/all_to_all | solution.py:338
  80.0 9.0 %collective-permute-start.11 = (bf16[64,2048]{1,0:T(8,128)(2,1)}, bf16[64,2048]{1,0:T(8,128)(2,1)}, u32[]{:S(2)}, u32[]{:S(2)}) collective-permute-start(bf16[64,2048]{1,0:T(8,128)(2,1)} %collective-permute-done.10.w4), channel_id=1, source_target_pairs={{0,8},{8,0},{1,9},{9,1},{2,10},{10,2},{3,11},{11,3},{4,12},{12,4},... | collective-permute-start | bytes 786440 | tf_op jit(solution)/shard_map/ppermute | solution.py:52
  91.1 42.7 %copy-start.1 = (bf16[1,2048,768]{2,1,0:T(8,128)(2,1)S(1)}, bf16[1,2048,768]{2,1,0:T(8,128)(2,1)}, u32[]{:S(2)}) copy-start(bf16[1,2048,768]{2,1,0:T(8,128)(2,1)} %param.27) | copy-start | bytes 9437188
  91.1 42.7 %copy-start.2 = (bf16[1,2048,768]{2,1,0:T(8,128)(2,1)S(1)}, bf16[1,2048,768]{2,1,0:T(8,128)(2,1)}, u32[]{:S(2)}) copy-start(bf16[1,2048,768]{2,1,0:T(8,128)(2,1)} %param.28) | copy-start | bytes 9437188
  (9 other events, 11.4 us)

commit v3 on v2

--- a/solution.py
+++ b/solution.py
@@ -140,10 +140,12 @@
     return highest, totals, dot(weights.astype(jnp.bfloat16), values[...])
 
 
-def attention_near_body(q_ref, a_ref, acc_ref, stat_ref, keys, values):
+def attention_near_body(q_ref, a_ref, acc_ref, stat_ref, padded_ref, keys, values):
     load_keys(a_ref, keys, values)
     for n in range(4):
-        highest, totals, out = attend(load_query(q_ref, n), keys, values)
+        q = load_query(q_ref, n)
+        padded_ref[n] = q
+        highest, totals, out = attend(q, keys, values)
         acc_ref[n] = out
         stat_ref[n] = jnp.concatenate([highest + jnp.zeros_like(out), totals + jnp.zeros_like(out)], axis=1)
 
@@ -152,7 +154,7 @@
     quad = at_ref[2]
     load_keys(b_ref, keys, values)
     for n in range(4):
-        highest, totals, out = attend(load_query(q_ref, n), keys, values)
+        highest, totals, out = attend(q_ref[n], keys, values)
         before, sums = stat_ref[n, :, 0:128], stat_ref[n, :, 128:256]
         top = jnp.maximum(highest, before)
         old = jnp.exp2((before - top) * score_scale)
@@ -182,16 +184,27 @@
 ):
     tp, core = at_ref[0], at_ref[1]
     turn = 1 - 2 * core
-    last = att_ref[(tp + 4) % 8]
-    turned = pltpu.roll(last.astype(jnp.float32), 64, 1).astype(jnp.bfloat16)
-    last = jnp.where(core == 0, last, turned)
-    near = jnp.concatenate([att_ref[tp], last], axis=1)
-    projected = dot(near, jnp.concatenate([w0[...], w4[...], s4[...]], axis=0))
-    for k, w_ref, s_ref in ((1, w1, s1), (2, w2, s2), (3, w3, s3)):
-        pair = jnp.concatenate(
-            [att_ref[(tp + 8 - turn * k) % 8], att_ref[(tp + 8 + turn * k) % 8]], axis=1
-        )
-        projected += dot(pair, jnp.concatenate([w_ref[...], s_ref[...]], axis=0))
+
+    def head(k):
+        spot = (tp + 8 + k) % 8
+        parts = [att_ref[8 * seq + spot].astype(jnp.float32) for seq in range(SEQS)]
+        return jnp.concatenate(parts, axis=0)
+
+    last = head(4)
+    last = jnp.where(core == 0, last, pltpu.roll(last, 64, 1))
+    lhs = [head(0), last]
+    for k in (1, 2, 3):
+        lhs += [head(-turn * k), head(turn * k)]
+    lhs = jnp.concatenate(lhs, axis=1).astype(jnp.bfloat16)
+    count = lhs.shape[0]
+    row = lax.broadcasted_iota(jnp.int32, (count, count), 0)
+    col = lax.broadcasted_iota(jnp.int32, (count, count), 1)
+    turned = (col == row % SEQS * (count // SEQS) + row // SEQS).astype(jnp.bfloat16)
+    lhs = dot(turned, lhs).astype(jnp.bfloat16)
+    projected = dot(lhs[:, 0:256], jnp.concatenate([w0[...], w4[...], s4[...]], axis=0))
+    for n, w_ref, s_ref in ((1, w1, s1), (2, w2, s2), (3, w3, s3)):
+        both = jnp.concatenate([w_ref[...], s_ref[...]], axis=0)
+        projected += dot(lhs[:, n * 256 : (n + 1) * 256], both)
     stream = (res_ref[...].astype(jnp.float32) + projected).astype(jnp.bfloat16)
     stream_ref[...] = stream
     wide = stream.astype(jnp.float32)
@@ -236,7 +249,9 @@
         pick = jnp.concatenate([hot * slots[0], hot * slots[1]], axis=-1).astype(jnp.bfloat16)
         term = dot(pick, r) * mixing[:, k : k + 1]
         added = term if added is None else added + term
-    out_ref[...] = (total + added).astype(jnp.bfloat16)
+    total = (total + added).astype(jnp.bfloat16)
+    for p in range(out_ref.shape[0]):
+        out_ref[p] = total[SEQS * p : SEQS * (p + 1), :]
 
 
 def vmem(*shape):
@@ -286,6 +301,12 @@
     q_rot = rotate(q[..., NOPE:].astype(jnp.float32), positions).astype(jnp.bfloat16)
     q_rot = jnp.concatenate([q_rot[:, : block // 2], q_rot[:, block // 2 :]], axis=-1)
     q = jnp.concatenate([q[..., :NOPE], q_rot], axis=1)
+    res = residual.reshape(rows, D)
+    meta = jnp.concatenate(
+        [routes.astype(jnp.float32), pair_logits, group_prob[..., None]], axis=-1
+    )
+    meta = meta.reshape(rows, 5)
+    q, res, meta = lax.optimization_barrier((q, res, meta))
     queries = []
     for k in range(4):
         piece = lax.dynamic_index_in_dim(q, (quad + k) % 4, 0, keepdims=False)
@@ -315,15 +336,16 @@
     far = swap(near)
 
     scratch = [vmem(8 * block, 256), vmem(8 * block, VDIM)]
-    partial, stats = kernel_call(
+    partial, stats, padded = kernel_call(
         attention_near_body,
         limit=12,
         out_shape=(
             jax.ShapeDtypeStruct((4, block, VDIM), jnp.float32),
             jax.ShapeDtypeStruct((4, block, 2 * VDIM), jnp.float32),
+            jax.ShapeDtypeStruct((4, block, 256), jnp.bfloat16),
         ),
         in_specs=[VM] * 2,
-        out_specs=(VM, VM),
+        out_specs=(VM, VM, VM),
         scratch_shapes=scratch,
     )(queries, near)
     attended = kernel_call(
@@ -333,17 +355,10 @@
         in_specs=[SM] + [VM] * 4,
         out_specs=VM,
         scratch_shapes=scratch,
-    )(at, queries, far, partial, stats)
+    )(at, padded, far, partial, stats)
     attended = attended.reshape(4 * tp_size, block // tp_size, VDIM)
     attended = lax.all_to_all(attended, ("quad", "tp"), split_axis=0, concat_axis=0, tiled=True)
-    attended = attended.reshape(SEQS, tp_size, block // tp_size, VDIM)
-    attended = jnp.swapaxes(attended, 0, 1).reshape(tp_size, rows, VDIM)
-
-    res = jnp.swapaxes(residual, 0, 1).reshape(rows, D)
-    meta = jnp.concatenate(
-        [routes.astype(jnp.float32), pair_logits, group_prob[..., None]], axis=-1
-    )
-    meta = jnp.swapaxes(meta, 0, 1).reshape(rows, 5)
+
     stream, outgoing = kernel_call(
         project_body,
         limit=10,
@@ -373,12 +388,12 @@
     combined = kernel_call(
         combine_body,
         limit=8,
-        out_shape=jax.ShapeDtypeStruct((rows, D), jnp.bfloat16),
+        out_shape=jax.ShapeDtypeStruct(residual.shape, jnp.bfloat16),
         in_specs=[VM] * 3,
         out_specs=VM,
         scratch_shapes=[vmem(256, D)],
     )(returned, stream, meta)
-    return jnp.swapaxes(combined.reshape(SEQS, rows // SEQS, D), 0, 1)
+    return combined
 
 
 def solution(mesh):

time: 178 us -> 177 us (level)
  local copies, waits for them, and re-layouts: 11.9 us -> 10 us
    transpose x3 -> x0, local copies, waits for them, and re-layouts: 2.09 us -> none  [the longest x1 1.96 us: layer(): res = jnp.swapaxes(residual, 0, 1).reshape(rows, D)]
    unnamed x39 -> x41, local copies, waits for them, and re-layouts: 5 us -> 5.14 us
  transfers between devices with their start and end apart: 14 -> 14, of which waited for: 4 -> 5; matrix products, arithmetic and copies ran while one was open for 3% -> 3% of each run, Pallas kernels for 4% -> 3%
where the time goes in v3:
time: 177 us; the launch traced here: 176 us
  blocking collectives  77.1 us (44%)
  starting transfers between devices  45.8 us (26%)
  waiting for transfers between devices  23.2 us (13%)
  Pallas kernels  15 us (8%)
  local copies, waits for them, and re-layouts  10 us (6%)
  other arithmetic  3.69 us (2%)
    all_to_all x2, blocking collectives, exchange(): lax.all_to_all(x, ALL, split_axis=0, concat_axis=0, tiled=True)  77.1 us
    all_to_all x1, starting transfers between devices, layer(): near = lax.all_to_all(kv, Y, split_axis=0, concat_axis=0, tiled=True)  13.8 us
    ppermute x5, starting transfers between devices, swap(): return lax.ppermute(x, 'core', [(0, 1), (1, 0)])  12.7 us
    ppermute x4, starting transfers between devices, spread(): return lax.ppermute(x, ('core', 'tp'), pairs)  11.2 us
    all_to_all x1, waiting for transfers between devices, layer(): near = lax.all_to_all(kv, Y, split_axis=0, concat_axis=0, tiled=True)  9.38 us
    all_to_all x1, starting transfers between devices, layer(): lax.all_to_all(attended, ('quad', 'tp'), split_axis=0, concat_axis=0, til...  7.6 us
    all_to_all x1, waiting for transfers between devices, layer(): lax.all_to_all(attended, ('quad', 'tp'), split_axis=0, concat_axis=0, til...  6.78 us
    ppermute x3, waiting for transfers between devices, shift(): return lax.ppermute(x, axis, [(i, (i + by) % size) for i in range(size)])  5.63 us
  transfers between devices with their start and end apart: 14, of which 5 were waited for; matrix products, arithmetic and copies ran while one was open for 3% of the time, Pallas kernels for 3%

profile of v3, /device:TPU:513, one launch (start us, length us, event | category | flops | bytes accessed | tf_op | source)
XLA Modules:
  0.0 176.1 jit_solution(344169710470178078)
XLA Ops:
  0.1 1.1 copy.51
  3.3 1.1 maximum_maximum_fusion
  4.4 13.8 %all-to-all-start = ((bf16[8,480,128]{2,1,0:T(8,128)(2,1)}), bf16[8,480,128]{2,1,0:T(8,128)(2,1)S(1)}, u32[]{:S(2)}, u32[]{:S(2)}) async-start(bf16[8,480,128]{2,1,0:T(8,128)(2,1)} %maximum_maximum_fusion), calls=%async_computation | async-start | bytes 1966080 | tf_op jit(solution)/shard_map/all_to_all | solution.py:335
  18.3 4.4 %collective-permute-start.5 = (bf16[128,2048]{1,0:T(8,128)(2,1)S(1)}, bf16[128,2048]{1,0:T(8,128)(2,1)}, u32[]{:S(2)}, u32[]{:S(2)}) collective-permute-start(bf16[128,2048]{1,0:T(8,128)(2,1)S(1)} %copy-done.8), channel_id=1, source_target_pairs={{0,2},{8,14},{1,3},{9,15},{2,4},{10,8},{3,5},{11,9},{4,6},{12,10},... | collective-permute-start | bytes 1572872 | tf_op jit(solution)/shard_map/ppermute | solution.py:60
  22.7 1.0 collective-permute-start.4
  26.2 9.4 %all-to-all-done.a_ref = bf16[8,480,128]{2,1,0:T(8,128)(2,1)S(1)} async-done(((bf16[8,480,128]{2,1,0:T(8,128)(2,1)}), bf16[8,480,128]{2,1,0:T(8,128)(2,1)S(1)}, u32[]{:S(2)}, u32[]{:S(2)}) %all-to-all-start) | async-done | bytes 983072 | tf_op jit(solution)/shard_map/all_to_all | solution.py:335
  35.6 11.2 %collective-permute-start.3 = (bf16[8,480,128]{2,1,0:T(8,128)(2,1)S(1)}, bf16[8,480,128]{2,1,0:T(8,128)(2,1)S(1)}, u32[]{:S(2)}, u32[]{:S(2)}) collective-permute-start(bf16[8,480,128]{2,1,0:T(8,128)(2,1)S(1)} %all-to-all-done.a_ref), channel_id=1, source_target_pairs={{0,8},{8,0},{1,9},{9,1},{2,10},{10,2},{3,11},{11,3},{4,12},{12,4},... | collective-permute-start | bytes 2949128 | tf_op jit(solution)/shard_map/ppermute | solution.py:52
  46.9 1.1 fusion.12
  47.9 3.5 %collective-permute-start.6 = (bf16[128,2048]{1,0:T(8,128)(2,1)}, bf16[128,2048]{1,0:T(8,128)(2,1)}, u32[]{:S(2)}, u32[]{:S(2)}) collective-permute-start(bf16[128,2048]{1,0:T(8,128)(2,1)} %collective-permute-done.5.w2), channel_id=1, source_target_pairs={{0,1},{8,15},{1,2},{9,8},{2,3},{10,9},{3,4},{11,10},{4,5},{12,11},... | collective-permute-start | bytes 1572872 | tf_op jit(solution)/shard_map/ppermute | solution.py:60
  51.9 5.0 %collective-permute-done = bf16[288,128]{1,0:T(8,128)(2,1)S(1)} collective-permute-done((bf16[288,128]{1,0:T(8,128)(2,1)S(1)}, bf16[288,128]{1,0:T(8,128)(2,1)S(1)}, u32[]{:S(2)}, u32[]{:S(2)}) %collective-permute-start) | collective-permute-done | bytes 73760 | tf_op jit(solution)/shard_map/ppermute | solution.py:48
  56.9 1.7 constant_dynamic-slice_fusion
  59.2 2.3 %collective-permute-start.10 = (bf16[64,2048]{1,0:T(8,128)(2,1)}, bf16[64,2048]{1,0:T(8,128)(2,1)}, u32[]{:S(2)}, u32[]{:S(2)}) collective-permute-start(bf16[64,2048]{1,0:T(8,128)(2,1)} %constant_dynamic-slice_fusion), channel_id=1, source_target_pairs={{0,2},{8,14},{1,3},{9,15},{2,4},{10,8},{3,5},{11,9},{4,6},{12,10},... | collective-permute-start | bytes 786440 | tf_op jit(solution)/shard_map/ppermute | solution.py:60
  62.4 2.7 %shard_map.145 = (f32[4,192,128]{2,1,0:T(8,128)S(1)}, f32[4,192,256]{2,1,0:T(8,128)S(1)}, bf16[4,192,256]{2,1,0:T(8,128)(2,1)S(1)}) custom-call(bf16[1152,128]{1,0:T(8,128)(2,1)S(1)} %pad_maximum_fusion.q_ref, bf16[8,480,128]{2,1,0:T(8,128)(2,1)S(1)} %all-to-all-done.a_ref), custom_call_target="tpu_custom_call" | custom-call | tf_op jit(solution)/shard_map/pallas_call | solution.py:339
  66.1 1.2 copy-done.6
  67.3 3.3 %shard_map.146 = bf16[4,192,128]{2,1,0:T(8,128)(2,1)S(1)} custom-call(s32[3]{0:T(128)S(1)} %pad_add_fusion.at_ref, bf16[4,192,256]{2,1,0:T(8,128)(2,1)S(1)} %get-tuple-element.18.q_ref, bf16[8,480,128]{2,1,0:T(8,128)(2,1)S(1)} %copy-done.6, f32[4,192,128]{2,1,0:T(8,128)S(1)} %get-tuple-element.19.acc_ref, f32[4,192,256]{2,1,0:T(8,128)S(1)} %get-tuple-element.20.stat_ref), custom_call_target="tpu_custom_call" | custom-call | tf_op jit(solution)/shard_map/pallas_call | solution.py:351
  71.3 7.6 %all-to-all-start.1 = ((bf16[32,24,128]{2,1,0:T(8,128)(2,1)}), bf16[32,24,128]{2,1,0:T(8,128)(2,1)S(1)}, u32[]{:S(2)}, u32[]{:S(2)}) async-start(bf16[32,24,128]{2,1,0:T(8,128)(2,1)} %bitcast.52), calls=%async_computation.1 | async-start | bytes 393216 | tf_op jit(solution)/shard_map/all_to_all | solution.py:360
  79.7 1.4 collective-permute-done.11.s4
  81.2 6.8 %all-to-all-done.1.att_ref = bf16[32,24,128]{2,1,0:T(8,128)(2,1)S(1)} async-done(((bf16[32,24,128]{2,1,0:T(8,128)(2,1)}), bf16[32,24,128]{2,1,0:T(8,128)(2,1)S(1)}, u32[]{:S(2)}, u32[]{:S(2)}) %all-to-all-start.1) | async-done | bytes 196640 | tf_op jit(solution)/shard_map/all_to_all | solution.py:360
  88.9 1.0 copy-done.9
  90.0 3.9 %shard_map.147 = (bf16[96,2048]{1,0:T(8,128)(2,1)S(1)}, bf16[2048,256]{1,0:T(8,128)(2,1)S(1)}) custom-call(s32[3]{0:T(128)S(1)} %pad_add_fusion.at_ref, bf16[32,24,128]{2,1,0:T(8,128)(2,1)S(1)} %all-to-all-done.1.att_ref, bf16[128,2048]{1,0:T(8,128)(2,1)S(1)} %copy-done.9, bf16[128,2048]{1,0:T(8,128)(2,1)} %collective-permute-done.4.w1, ...), custom_call_target="tpu_custom_call" | custom-call | tf_op jit(solution)/shard_map/pallas_call | solution.py:362
  93.9 38.7 %all_to_all.20 = bf16[128,16,256]{2,1,0:T(8,128)(2,1)S(1)} all-to-all(bf16[128,16,256]{2,1,0:T(8,128)(2,1)S(1)} %bitcast.51), channel_id=1, replica_groups=mesh['grp'=2,'half'=2,'quad'=4,'core'=2,'tp'=8] {'half','quad','core','tp'}, dimensions={0} | all-to-all | bytes 2097152 | tf_op jit(solution)/shard_map/all_to_all | solution.py:376
  132.7 3.3 %shard_map.148 = bf16[2048,256]{1,0:T(8,128)(2,1)S(1)} custom-call(bf16[2048,256]{1,0:T(8,128)(2,1)S(1)} %bitcast.46, bf16[2048,768]{1,0:T(8,128)(2,1)S(1)} %bitcast.48, bf16[2048,768]{1,0:T(8,128)(2,1)S(1)} %bitcast.49, bf16[768,2048]{1,0:T(8,128)(2,1)S(1)} %bitcast.50), custom_call_target="tpu_custom_call" | custom-call | tf_op jit(solution)/shard_map/pallas_call | solution.py:379
  136.0 38.4 %all_to_all.21 = bf16[128,16,256]{2,1,0:T(8,128)(2,1)S(1)} all-to-all(bf16[128,16,256]{2,1,0:T(8,128)(2,1)S(1)} %bitcast.47), channel_id=1, replica_groups=mesh['grp'=2,'half'=2,'quad'=4,'core'=2,'tp'=8] {'half','quad','core','tp'}, dimensions={0} | all-to-all | bytes 2097152 | tf_op jit(solution)/shard_map/all_to_all | solution.py:376
  174.4 1.7 shard_map.149
  (81 shorter events, 10.0 us)
Async XLA Ops:
  3.2 15.1 %copy-start.8 = (bf16[128,2048]{1,0:T(8,128)(2,1)S(1)}, bf16[128,2048]{1,0:T(8,128)(2,1)}, u32[]{:S(2)}) copy-start(bf16[128,2048]{1,0:T(8,128)(2,1)} %w0.1) | copy-start | bytes 1572868
  3.2 20.5 %copy-start.12 = (bf16[192,4,192]{2,1,0:T(4,128)(2,1)S(1)}, bf16[192,4,192]{2,1,0:T(4,128)(2,1)}, u32[]{:S(2)}) copy-start(bf16[192,4,192]{2,1,0:T(4,128)(2,1)} %param.16) | copy-start | bytes 884740
  4.4 20.1 %copy-start.13 = (bf16[24,4,2048]{2,1,0:T(4,128)(2,1)S(1)}, bf16[24,4,2048]{2,1,0:T(4,128)(2,1)}, u32[]{:S(2)}) copy-start(bf16[24,4,2048]{2,1,0:T(4,128)(2,1)} %param.15) | copy-start | bytes 1179652
  4.4 21.0 %copy-start.15 = (s32[24,4,2]{0,2,1:T(2,128)S(1)}, s32[24,4,2]{0,2,1:T(2,128)}, u32[]{:S(2)}) copy-start(s32[24,4,2]{0,2,1:T(2,128)} %param.26) | copy-start | bytes 2308
  4.4 21.2 %copy-start.14 = (f32[24,4,2]{0,2,1:T(2,128)S(1)}, f32[24,4,2]{0,2,1:T(2,128)}, u32[]{:S(2)}) copy-start(f32[24,4,2]{0,2,1:T(2,128)} %param.25) | copy-start | bytes 2308
  4.4 21.4 %copy-start.16 = (f32[24,4]{0,1:T(4,128)S(1)}, f32[24,4]{0,1:T(4,128)}, u32[]{:S(2)}) copy-start(f32[24,4]{0,1:T(4,128)} %param.24) | copy-start | bytes 1156
  4.4 31.1 %all-to-all-start = ((bf16[8,480,128]{2,1,0:T(8,128)(2,1)}), bf16[8,480,128]{2,1,0:T(8,128)(2,1)S(1)}, u32[]{:S(2)}, u32[]{:S(2)}) async-start(bf16[8,480,128]{2,1,0:T(8,128)(2,1)} %maximum_maximum_fusion), calls=%async_computation | async-start | bytes 1966080 | tf_op jit(solution)/shard_map/all_to_all | solution.py:335
  18.3 29.6 %collective-permute-start.5 = (bf16[128,2048]{1,0:T(8,128)(2,1)S(1)}, bf16[128,2048]{1,0:T(8,128)(2,1)}, u32[]{:S(2)}, u32[]{:S(2)}) collective-permute-start(bf16[128,2048]{1,0:T(8,128)(2,1)S(1)} %copy-done.8), channel_id=1, source_target_pairs={{0,2},{8,14},{1,3},{9,15},{2,4},{10,8},{3,5},{11,9},{4,6},{12,10},... | collective-permute-start | bytes 1572872 | tf_op jit(solution)/shard_map/ppermute | solution.py:60
  22.7 38.8 %collective-permute-start.4 = (bf16[128,2048]{1,0:T(8,128)(2,1)S(1)}, bf16[128,2048]{1,0:T(8,128)(2,1)}, u32[]{:S(2)}, u32[]{:S(2)}) collective-permute-start(bf16[128,2048]{1,0:T(8,128)(2,1)S(1)} %copy-done.8), channel_id=1, source_target_pairs={{0,1},{8,15},{1,2},{9,8},{2,3},{10,9},{3,4},{11,10},{4,5},{12,11},... | collective-permute-start | bytes 1572872 | tf_op jit(solution)/shard_map/ppermute | solution.py:60
  35.6 29.5 %collective-permute-start.3 = (bf16[8,480,128]{2,1,0:T(8,128)(2,1)S(1)}, bf16[8,480,128]{2,1,0:T(8,128)(2,1)S(1)}, u32[]{:S(2)}, u32[]{:S(2)}) collective-permute-start(bf16[8,480,128]{2,1,0:T(8,128)(2,1)S(1)} %all-to-all-done.a_ref), channel_id=1, source_target_pairs={{0,8},{8,0},{1,9},{9,1},{2,10},{10,2},{3,11},{11,3},{4,12},{12,4},... | collective-permute-start | bytes 2949128 | tf_op jit(solution)/shard_map/ppermute | solution.py:52
  47.9 14.1 %collective-permute-start.6 = (bf16[128,2048]{1,0:T(8,128)(2,1)}, bf16[128,2048]{1,0:T(8,128)(2,1)}, u32[]{:S(2)}, u32[]{:S(2)}) collective-permute-start(bf16[128,2048]{1,0:T(8,128)(2,1)} %collective-permute-done.5.w2), channel_id=1, source_target_pairs={{0,1},{8,15},{1,2},{9,8},{2,3},{10,9},{3,4},{11,10},{4,5},{12,11},... | collective-permute-start | bytes 1572872 | tf_op jit(solution)/shard_map/ppermute | solution.py:60
  51.5 5.4 %collective-permute-start = (bf16[288,128]{1,0:T(8,128)(2,1)S(1)}, bf16[288,128]{1,0:T(8,128)(2,1)S(1)}, u32[]{:S(2)}, u32[]{:S(2)}) collective-permute-start(bf16[288,128]{1,0:T(8,128)(2,1)S(1)} %get-tuple-element.32), channel_id=1, source_target_pairs={{0,16},{16,32},{32,48},{48,0},{1,17},{17,33},{33,49},{49,1},{2,18}... | collective-permute-start | bytes 221192 | tf_op jit(solution)/shard_map/ppermute | solution.py:48
  51.9 7.3 %collective-permute-start.1 = (bf16[288,128]{1,0:T(8,128)(2,1)S(1)}, bf16[288,128]{1,0:T(8,128)(2,1)S(1)}, u32[]{:S(2)}, u32[]{:S(2)}) collective-permute-start(bf16[288,128]{1,0:T(8,128)(2,1)S(1)} %get-tuple-element.31), channel_id=1, source_target_pairs={{0,32},{16,48},{32,0},{48,16},{1,33},{17,49},{33,1},{49,17},{2,34}... | collective-permute-start | bytes 221192 | tf_op jit(solution)/shard_map/ppermute | solution.py:48
  56.9 4.6 %collective-permute-start.2 = (bf16[288,128]{1,0:T(8,128)(2,1)S(1)}, bf16[288,128]{1,0:T(8,128)(2,1)S(1)}, u32[]{:S(2)}, u32[]{:S(2)}) collective-permute-start(bf16[288,128]{1,0:T(8,128)(2,1)S(1)} %get-tuple-element.30), channel_id=1, source_target_pairs={{0,48},{16,0},{32,16},{48,32},{1,49},{17,1},{33,17},{49,33},{2,50}... | collective-permute-start | bytes 221192 | tf_op jit(solution)/shard_map/ppermute | solution.py:48
  59.2 19.7 %collective-permute-start.10 = (bf16[64,2048]{1,0:T(8,128)(2,1)}, bf16[64,2048]{1,0:T(8,128)(2,1)}, u32[]{:S(2)}, u32[]{:S(2)}) collective-permute-start(bf16[64,2048]{1,0:T(8,128)(2,1)} %constant_dynamic-slice_fusion), channel_id=1, source_target_pairs={{0,2},{8,14},{1,3},{9,15},{2,4},{10,8},{3,5},{11,9},{4,6},{12,10},... | collective-permute-start | bytes 786440 | tf_op jit(solution)/shard_map/ppermute | solution.py:60
  61.5 19.6 %collective-permute-start.8 = (bf16[128,2048]{1,0:T(8,128)(2,1)}, bf16[128,2048]{1,0:T(8,128)(2,1)}, u32[]{:S(2)}, u32[]{:S(2)}) collective-permute-start(bf16[128,2048]{1,0:T(8,128)(2,1)} %collective-permute-done.5.w2), channel_id=1, source_target_pairs={{0,8},{8,0},{1,9},{9,1},{2,10},{10,2},{3,11},{11,3},{4,12},{12,4},... | collective-permute-start | bytes 1572872 | tf_op jit(solution)/shard_map/ppermute | solution.py:52
  61.5 19.6 %collective-permute-start.7 = (bf16[128,2048]{1,0:T(8,128)(2,1)}, bf16[128,2048]{1,0:T(8,128)(2,1)}, u32[]{:S(2)}, u32[]{:S(2)}) collective-permute-start(bf16[128,2048]{1,0:T(8,128)(2,1)} %collective-permute-done.4.w1), channel_id=1, source_target_pairs={{0,8},{8,0},{1,9},{9,1},{2,10},{10,2},{3,11},{11,3},{4,12},{12,4},... | collective-permute-start | bytes 1572872 | tf_op jit(solution)/shard_map/ppermute | solution.py:52
  62.0 19.1 %collective-permute-start.9 = (bf16[128,2048]{1,0:T(8,128)(2,1)}, bf16[128,2048]{1,0:T(8,128)(2,1)}, u32[]{:S(2)}, u32[]{:S(2)}) collective-permute-start(bf16[128,2048]{1,0:T(8,128)(2,1)} %collective-permute-done.6.w3), channel_id=1, source_target_pairs={{0,8},{8,0},{1,9},{9,1},{2,10},{10,2},{3,11},{11,3},{4,12},{12,4},... | collective-permute-start | bytes 1572872 | tf_op jit(solution)/shard_map/ppermute | solution.py:52
  62.4 25.6 %copy-start.10 = (f32[2048]{0:T(1024)S(1)}, f32[2048]{0:T(1024)}, u32[]{:S(2)}) copy-start(f32[2048]{0:T(1024)} %param.23) | copy-start | bytes 24580
  67.3 65.4 %copy-start.3 = (bf16[1,768,2048]{2,1,0:T(8,128)(2,1)S(1)}, bf16[1,768,2048]{2,1,0:T(8,128)(2,1)}, u32[]{:S(2)}) copy-start(bf16[1,768,2048]{2,1,0:T(8,128)(2,1)} %param.29) | copy-start | bytes 9437188
  71.3 16.6 %all-to-all-start.1 = ((bf16[32,24,128]{2,1,0:T(8,128)(2,1)}), bf16[32,24,128]{2,1,0:T(8,128)(2,1)S(1)}, u32[]{:S(2)}, u32[]{:S(2)}) async-start(bf16[32,24,128]{2,1,0:T(8,128)(2,1)} %bitcast.52), calls=%async_computation.1 | async-start | bytes 393216 | tf_op jit(solution)/shard_map/all_to_all | solution.py:360
  78.9 2.2 %collective-permute-start.11 = (bf16[64,2048]{1,0:T(8,128)(2,1)}, bf16[64,2048]{1,0:T(8,128)(2,1)}, u32[]{:S(2)}, u32[]{:S(2)}) collective-permute-start(bf16[64,2048]{1,0:T(8,128)(2,1)} %collective-permute-done.10.w4), channel_id=1, source_target_pairs={{0,8},{8,0},{1,9},{9,1},{2,10},{10,2},{3,11},{11,3},{4,12},{12,4},... | collective-permute-start | bytes 786440 | tf_op jit(solution)/shard_map/ppermute | solution.py:52
  90.0 42.7 %copy-start.1 = (bf16[1,2048,768]{2,1,0:T(8,128)(2,1)S(1)}, bf16[1,2048,768]{2,1,0:T(8,128)(2,1)}, u32[]{:S(2)}) copy-start(bf16[1,2048,768]{2,1,0:T(8,128)(2,1)} %param.27) | copy-start | bytes 9437188
  90.0 42.7 %copy-start.2 = (bf16[1,2048,768]{2,1,0:T(8,128)(2,1)S(1)}, bf16[1,2048,768]{2,1,0:T(8,128)(2,1)}, u32[]{:S(2)}) copy-start(bf16[1,2048,768]{2,1,0:T(8,128)(2,1)} %param.28) | copy-start | bytes 9437188
  (9 other events, 12.4 us)

commit v4 on v3

--- a/solution.py
+++ b/solution.py
@@ -166,7 +166,7 @@
 def project_body(
     at_ref,
     att_ref,
-    w0,
+    w0_far,
     w1,
     w2,
     w3,
@@ -174,14 +174,22 @@
     s2,
     s3,
     w4,
-    s4,
-    res_ref,
+    s4_far,
+    res_far,
     gain_ref,
     meta_ref,
     stream_ref,
     out_ref,
     rows,
+    w0,
+    s4,
+    res_ref,
+    sems,
 ):
+    pairs = ((w0_far, w0), (s4_far, s4), (res_far, res_ref))
+    fetches = [pltpu.make_async_copy(a, b, sems.at[n]) for n, (a, b) in enumerate(pairs)]
+    for fetch in fetches:
+        fetch.start()
     tp, core = at_ref[0], at_ref[1]
     turn = 1 - 2 * core
 
@@ -201,10 +209,14 @@
     col = lax.broadcasted_iota(jnp.int32, (count, count), 1)
     turned = (col == row % SEQS * (count // SEQS) + row // SEQS).astype(jnp.bfloat16)
     lhs = dot(turned, lhs).astype(jnp.bfloat16)
-    projected = dot(lhs[:, 0:256], jnp.concatenate([w0[...], w4[...], s4[...]], axis=0))
+    projected = None
     for n, w_ref, s_ref in ((1, w1, s1), (2, w2, s2), (3, w3, s3)):
         both = jnp.concatenate([w_ref[...], s_ref[...]], axis=0)
-        projected += dot(lhs[:, n * 256 : (n + 1) * 256], both)
+        part = dot(lhs[:, n * 256 : (n + 1) * 256], both)
+        projected = part if projected is None else projected + part
+    for fetch in fetches:
+        fetch.wait()
+    projected += dot(lhs[:, 0:256], jnp.concatenate([w0[...], w4[...], s4[...]], axis=0))
     stream = (res_ref[...].astype(jnp.float32) + projected).astype(jnp.bfloat16)
     stream_ref[...] = stream
     wide = stream.astype(jnp.float32)
@@ -254,6 +266,33 @@
         out_ref[p] = total[SEQS * p : SEQS * (p + 1), :]
 
 
+def meta_body(route_ref, logit_ref, prob_ref, out_ref):
+    rows = out_ref.shape[0]
+    count = rows // SEQS
+    row = lax.broadcasted_iota(jnp.int32, (rows, count), 0)
+    col = lax.broadcasted_iota(jnp.int32, (rows, count), 1)
+    total = None
+    for seq in range(SEQS):
+        block = jnp.concatenate(
+            [
+                route_ref[seq].astype(jnp.float32),
+                logit_ref[seq],
+                prob_ref[seq : seq + 1, :],
+                jnp.zeros((3, count), jnp.float32),
+            ],
+            axis=0,
+        )
+        part = lax.dot_general(
+            (row == col * SEQS + seq).astype(jnp.float32),
+            block,
+            (((1,), (1,)), ((), ())),
+            precision=lax.Precision.HIGHEST,
+            preferred_element_type=jnp.float32,
+        )
+        total = part if total is None else total + part
+    out_ref[...] = total
+
+
 def vmem(*shape):
     return pltpu.VMEM(shape, jnp.bfloat16)
 
@@ -268,6 +307,7 @@
 
 VM = pl.BlockSpec(memory_space=pltpu.VMEM)
 SM = pl.BlockSpec(memory_space=pltpu.SMEM)
+HB = pl.BlockSpec(memory_space=pltpu.HBM)
 
 
 def layer(
@@ -302,11 +342,14 @@
     q_rot = jnp.concatenate([q_rot[:, : block // 2], q_rot[:, block // 2 :]], axis=-1)
     q = jnp.concatenate([q[..., :NOPE], q_rot], axis=1)
     res = residual.reshape(rows, D)
-    meta = jnp.concatenate(
-        [routes.astype(jnp.float32), pair_logits, group_prob[..., None]], axis=-1
-    )
-    meta = meta.reshape(rows, 5)
-    q, res, meta = lax.optimization_barrier((q, res, meta))
+    meta = kernel_call(
+        meta_body,
+        limit=2,
+        out_shape=jax.ShapeDtypeStruct((rows, 8), jnp.float32),
+        in_specs=[VM] * 3,
+        out_specs=VM,
+    )(jnp.transpose(routes, (1, 2, 0)), jnp.transpose(pair_logits, (1, 2, 0)), group_prob.T)
+    q, res = lax.optimization_barrier((q, res))
     queries = []
     for k in range(4):
         piece = lax.dynamic_index_in_dim(q, (quad + k) % 4, 0, keepdims=False)
@@ -366,9 +409,15 @@
             jax.ShapeDtypeStruct((rows, D), jnp.bfloat16),
             jax.ShapeDtypeStruct((2048, LANE), jnp.bfloat16),
         ),
-        in_specs=[SM] + [VM] * 13,
+        in_specs=[SM, VM, HB] + [VM] * 7 + [HB, HB, VM, VM],
         out_specs=(VM, VM),
-        scratch_shapes=[vmem(256, D)],
+        scratch_shapes=[
+            vmem(256, D),
+            vmem(*out_weight.shape),
+            vmem(half_rows, D),
+            vmem(rows, D),
+            pltpu.SemaphoreType.DMA((3,)),
+        ],
     )(at, attended, *weights, res, norm_gain.reshape(1, D), meta)
 
     def exchange(x):

time: 177 us -> 183 us (1.034)
  local copies, waits for them, and re-layouts: 10 us -> 12.9 us
    all_to_all x1, waiting for transfers between devices: 9.38 us -> 11.8 us  [layer(): near = lax.all_to_all(kv, Y, split_axis=0, concat_axis=0, tiled=True)]
    unnamed x41 -> x45, local copies, waits for them, and re-layouts: 5.14 us -> 6.61 us
  transfers between devices with their start and end apart: 14 -> 14, of which waited for: 5 -> 5; matrix products, arithmetic and copies ran while one was open for 3% -> 4% of each run, Pallas kernels for 3% -> 3%
where the time goes in v4:
time: 183 us; the launch traced here: 182 us
  blocking collectives  77.1 us (42%)
  starting transfers between devices  45.6 us (25%)
  waiting for transfers between devices  24.7 us (13%)
  Pallas kernels  15.8 us (9%)
  local copies, waits for them, and re-layouts  12.9 us (7%)
  other arithmetic  4.53 us (2%)
    all_to_all x2, blocking collectives, exchange(): lax.all_to_all(x, ALL, split_axis=0, concat_axis=0, tiled=True)  77.1 us
    all_to_all x1, starting transfers between devices, layer(): near = lax.all_to_all(kv, Y, split_axis=0, concat_axis=0, tiled=True)  13.7 us
    ppermute x5, starting transfers between devices, swap(): return lax.ppermute(x, 'core', [(0, 1), (1, 0)])  12.7 us
    all_to_all x1, waiting for transfers between devices, layer(): near = lax.all_to_all(kv, Y, split_axis=0, concat_axis=0, tiled=True)  11.8 us
    ppermute x4, starting transfers between devices, spread(): return lax.ppermute(x, ('core', 'tp'), pairs)  11.2 us
    all_to_all x1, starting transfers between devices, layer(): lax.all_to_all(attended, ('quad', 'tp'), split_axis=0, concat_axis=0, til...  7.61 us
    unnamed x45, local copies, waits for them, and re-layouts  6.61 us
    all_to_all x1, waiting for transfers between devices, layer(): lax.all_to_all(attended, ('quad', 'tp'), split_axis=0, concat_axis=0, til...  6.22 us
  transfers between devices with their start and end apart: 14, of which 5 were waited for; matrix products, arithmetic and copies ran while one was open for 4% of the time, Pallas kernels for 3%

profile of v4, /device:TPU:513, one launch (start us, length us, event | category | flops | bytes accessed | tf_op | source)
XLA Modules:
  0.0 181.9 jit_solution(13372722111662950790)
XLA Ops:
  0.1 1.1 copy.21
  3.3 1.1 maximum_maximum_fusion
  4.4 13.7 %all-to-all-start = ((bf16[8,480,128]{2,1,0:T(8,128)(2,1)}), bf16[8,480,128]{2,1,0:T(8,128)(2,1)S(1)}, u32[]{:S(2)}, u32[]{:S(2)}) async-start(bf16[8,480,128]{2,1,0:T(8,128)(2,1)} %maximum_maximum_fusion), calls=%async_computation | async-start | bytes 1966080 | tf_op jit(solution)/shard_map/all_to_all | solution.py:378
  18.1 4.4 %collective-permute-start.5 = (bf16[128,2048]{1,0:T(8,128)(2,1)S(1)}, bf16[128,2048]{1,0:T(8,128)(2,1)}, u32[]{:S(2)}, u32[]{:S(2)}) collective-permute-start(bf16[128,2048]{1,0:T(8,128)(2,1)S(1)} %copy-done.8), channel_id=1, source_target_pairs={{0,2},{8,14},{1,3},{9,15},{2,4},{10,8},{3,5},{11,9},{4,6},{12,10},... | collective-permute-start | bytes 1572872 | tf_op jit(solution)/shard_map/ppermute | solution.py:60
  23.6 11.8 %all-to-all-done.a_ref = bf16[8,480,128]{2,1,0:T(8,128)(2,1)S(1)} async-done(((bf16[8,480,128]{2,1,0:T(8,128)(2,1)}), bf16[8,480,128]{2,1,0:T(8,128)(2,1)S(1)}, u32[]{:S(2)}, u32[]{:S(2)}) %all-to-all-start) | async-done | bytes 983072 | tf_op jit(solution)/shard_map/all_to_all | solution.py:378
  35.4 11.2 %collective-permute-start.3 = (bf16[8,480,128]{2,1,0:T(8,128)(2,1)S(1)}, bf16[8,480,128]{2,1,0:T(8,128)(2,1)S(1)}, u32[]{:S(2)}, u32[]{:S(2)}) collective-permute-start(bf16[8,480,128]{2,1,0:T(8,128)(2,1)S(1)} %all-to-all-done.a_ref), channel_id=1, source_target_pairs={{0,8},{8,0},{1,9},{9,1},{2,10},{10,2},{3,11},{11,3},{4,12},{12,4},... | collective-permute-start | bytes 2949128 | tf_op jit(solution)/shard_map/ppermute | solution.py:52
  46.6 1.1 subtract_convert_fusion
  47.7 1.6 slice.46
  49.3 1.8 %reshape.100.res_far = bf16[96,2048]{1,0:T(8,128)(2,1)} reshape(bf16[24,4,2048]{2,1,0:T(4,128)(2,1)} %param.15) | data formatting | bytes 786432 | tf_op jit(solution)/shard_map/reshape | solution.py:344
  51.3 3.5 %collective-permute-start.6 = (bf16[128,2048]{1,0:T(8,128)(2,1)}, bf16[128,2048]{1,0:T(8,128)(2,1)}, u32[]{:S(2)}, u32[]{:S(2)}) collective-permute-start(bf16[128,2048]{1,0:T(8,128)(2,1)} %collective-permute-done.5.w2), channel_id=1, source_target_pairs={{0,1},{8,15},{1,2},{9,8},{2,3},{10,9},{3,4},{11,10},{4,5},{12,11},... | collective-permute-start | bytes 1572872 | tf_op jit(solution)/shard_map/ppermute | solution.py:60
  56.3 5.0 %collective-permute-done = bf16[288,128]{1,0:T(8,128)(2,1)S(1)} collective-permute-done((bf16[288,128]{1,0:T(8,128)(2,1)S(1)}, bf16[288,128]{1,0:T(8,128)(2,1)S(1)}, u32[]{:S(2)}, u32[]{:S(2)}) %collective-permute-start) | collective-permute-done | bytes 73760 | tf_op jit(solution)/shard_map/ppermute | solution.py:48
  61.3 1.7 constant_dynamic-slice_fusion
  63.6 2.3 %collective-permute-start.10 = (bf16[64,2048]{1,0:T(8,128)(2,1)}, bf16[64,2048]{1,0:T(8,128)(2,1)}, u32[]{:S(2)}, u32[]{:S(2)}) collective-permute-start(bf16[64,2048]{1,0:T(8,128)(2,1)} %constant_dynamic-slice_fusion), channel_id=1, source_target_pairs={{0,2},{8,14},{1,3},{9,15},{2,4},{10,8},{3,5},{11,9},{4,6},{12,10},... | collective-permute-start | bytes 786440 | tf_op jit(solution)/shard_map/ppermute | solution.py:60
  66.8 2.7 %shard_map.145 = (f32[4,192,128]{2,1,0:T(8,128)S(1)}, f32[4,192,256]{2,1,0:T(8,128)S(1)}, bf16[4,192,256]{2,1,0:T(8,128)(2,1)S(1)}) custom-call(bf16[1152,128]{1,0:T(8,128)(2,1)S(1)} %pad_maximum_fusion.q_ref, bf16[8,480,128]{2,1,0:T(8,128)(2,1)S(1)} %all-to-all-done.a_ref), custom_call_target="tpu_custom_call" | custom-call | tf_op jit(solution)/shard_map/pallas_call | solution.py:382
  70.5 1.2 copy-done.6
  71.7 3.3 %shard_map.146 = bf16[4,192,128]{2,1,0:T(8,128)(2,1)S(1)} custom-call(s32[3]{0:T(128)S(1)} %pad_add_fusion.at_ref, bf16[4,192,256]{2,1,0:T(8,128)(2,1)S(1)} %get-tuple-element.17.q_ref, bf16[8,480,128]{2,1,0:T(8,128)(2,1)S(1)} %copy-done.6, f32[4,192,128]{2,1,0:T(8,128)S(1)} %get-tuple-element.18.acc_ref, f32[4,192,256]{2,1,0:T(8,128)S(1)} %get-tuple-element.19.stat_ref), custom_call_target="tpu_custom_call" | custom-call | tf_op jit(solution)/shard_map/pallas_call | solution.py:394
  75.7 7.6 %all-to-all-start.1 = ((bf16[32,24,128]{2,1,0:T(8,128)(2,1)}), bf16[32,24,128]{2,1,0:T(8,128)(2,1)S(1)}, u32[]{:S(2)}, u32[]{:S(2)}) async-start(bf16[32,24,128]{2,1,0:T(8,128)(2,1)} %bitcast.51), calls=%async_computation.1 | async-start | bytes 393216 | tf_op jit(solution)/shard_map/all_to_all | solution.py:403
  84.4 1.1 collective-permute-done.11.s4_far
  86.1 6.2 %all-to-all-done.1.att_ref = bf16[32,24,128]{2,1,0:T(8,128)(2,1)S(1)} async-done(((bf16[32,24,128]{2,1,0:T(8,128)(2,1)}), bf16[32,24,128]{2,1,0:T(8,128)(2,1)S(1)}, u32[]{:S(2)}, u32[]{:S(2)}) %all-to-all-start.1) | async-done | bytes 196640 | tf_op jit(solution)/shard_map/all_to_all | solution.py:403
  95.4 4.4 %shard_map.148 = (bf16[96,2048]{1,0:T(8,128)(2,1)S(1)}, bf16[2048,256]{1,0:T(8,128)(2,1)S(1)}) custom-call(s32[3]{0:T(128)S(1)} %pad_add_fusion.at_ref, bf16[32,24,128]{2,1,0:T(8,128)(2,1)S(1)} %all-to-all-done.1.att_ref, bf16[128,2048]{1,0:T(8,128)(2,1)S(1)} %copy-done.9, bf16[128,2048]{1,0:T(8,128)(2,1)} %collective-permute-done.4.w1, ...), custom_call_target="tpu_custom_call" | custom-call | tf_op jit(solution)/shard_map/pallas_call | solution.py:405
  99.7 38.7 %all_to_all.20 = bf16[128,16,256]{2,1,0:T(8,128)(2,1)S(1)} all-to-all(bf16[128,16,256]{2,1,0:T(8,128)(2,1)S(1)} %bitcast.50), channel_id=1, replica_groups=mesh['grp'=2,'half'=2,'quad'=4,'core'=2,'tp'=8] {'half','quad','core','tp'}, dimensions={0} | all-to-all | bytes 2097152 | tf_op jit(solution)/shard_map/all_to_all | solution.py:425
  138.5 3.3 %shard_map.149 = bf16[2048,256]{1,0:T(8,128)(2,1)S(1)} custom-call(bf16[2048,256]{1,0:T(8,128)(2,1)S(1)} %bitcast.45, bf16[2048,768]{1,0:T(8,128)(2,1)S(1)} %bitcast.47, bf16[2048,768]{1,0:T(8,128)(2,1)S(1)} %bitcast.48, bf16[768,2048]{1,0:T(8,128)(2,1)S(1)} %bitcast.49), custom_call_target="tpu_custom_call" | custom-call | tf_op jit(solution)/shard_map/pallas_call | solution.py:428
  141.8 38.4 %all_to_all.21 = bf16[128,16,256]{2,1,0:T(8,128)(2,1)S(1)} all-to-all(bf16[128,16,256]{2,1,0:T(8,128)(2,1)S(1)} %bitcast.46), channel_id=1, replica_groups=mesh['grp'=2,'half'=2,'quad'=4,'core'=2,'tp'=8] {'half','quad','core','tp'}, dimensions={0} | all-to-all | bytes 2097152 | tf_op jit(solution)/shard_map/all_to_all | solution.py:425
  180.2 1.7 shard_map.150
  (79 shorter events, 12.6 us)
Async XLA Ops:
  3.2 14.9 %copy-start.8 = (bf16[128,2048]{1,0:T(8,128)(2,1)S(1)}, bf16[128,2048]{1,0:T(8,128)(2,1)}, u32[]{:S(2)}) copy-start(bf16[128,2048]{1,0:T(8,128)(2,1)} %w0_far.1) | copy-start | bytes 1572868
  3.2 20.3 %copy-start.19 = (bf16[192,4,192]{2,1,0:T(4,128)(2,1)S(1)}, bf16[192,4,192]{2,1,0:T(4,128)(2,1)}, u32[]{:S(2)}) copy-start(bf16[192,4,192]{2,1,0:T(4,128)(2,1)} %param.16) | copy-start | bytes 884740
  4.4 31.0 %all-to-all-start = ((bf16[8,480,128]{2,1,0:T(8,128)(2,1)}), bf16[8,480,128]{2,1,0:T(8,128)(2,1)S(1)}, u32[]{:S(2)}, u32[]{:S(2)}) async-start(bf16[8,480,128]{2,1,0:T(8,128)(2,1)} %maximum_maximum_fusion), calls=%async_computation | async-start | bytes 1966080 | tf_op jit(solution)/shard_map/all_to_all | solution.py:378
  18.1 33.1 %collective-permute-start.5 = (bf16[128,2048]{1,0:T(8,128)(2,1)S(1)}, bf16[128,2048]{1,0:T(8,128)(2,1)}, u32[]{:S(2)}, u32[]{:S(2)}) collective-permute-start(bf16[128,2048]{1,0:T(8,128)(2,1)S(1)} %copy-done.8), channel_id=1, source_target_pairs={{0,2},{8,14},{1,3},{9,15},{2,4},{10,8},{3,5},{11,9},{4,6},{12,10},... | collective-permute-start | bytes 1572872 | tf_op jit(solution)/shard_map/ppermute | solution.py:60
  22.5 43.4 %collective-permute-start.4 = (bf16[128,2048]{1,0:T(8,128)(2,1)S(1)}, bf16[128,2048]{1,0:T(8,128)(2,1)}, u32[]{:S(2)}, u32[]{:S(2)}) collective-permute-start(bf16[128,2048]{1,0:T(8,128)(2,1)S(1)} %copy-done.8), channel_id=1, source_target_pairs={{0,1},{8,15},{1,2},{9,8},{2,3},{10,9},{3,4},{11,10},{4,5},{12,11},... | collective-permute-start | bytes 1572872 | tf_op jit(solution)/shard_map/ppermute | solution.py:60
  23.6 11.8 %copy-start.16 = (bf16[192,4,192]{2,0,1:T(8,128)(2,1)}, bf16[192,4,192]{2,0,1:T(8,128)(2,1)S(1)}, u32[]{:S(2)}) copy-start(bf16[192,4,192]{2,0,1:T(8,128)(2,1)S(1)} %copy.28) | copy-start | bytes 884740
  35.4 34.1 %collective-permute-start.3 = (bf16[8,480,128]{2,1,0:T(8,128)(2,1)S(1)}, bf16[8,480,128]{2,1,0:T(8,128)(2,1)S(1)}, u32[]{:S(2)}, u32[]{:S(2)}) collective-permute-start(bf16[8,480,128]{2,1,0:T(8,128)(2,1)S(1)} %all-to-all-done.a_ref), channel_id=1, source_target_pairs={{0,8},{8,0},{1,9},{9,1},{2,10},{10,2},{3,11},{11,3},{4,12},{12,4},... | collective-permute-start | bytes 2949128 | tf_op jit(solution)/shard_map/ppermute | solution.py:52
  51.3 15.2 %collective-permute-start.6 = (bf16[128,2048]{1,0:T(8,128)(2,1)}, bf16[128,2048]{1,0:T(8,128)(2,1)}, u32[]{:S(2)}, u32[]{:S(2)}) collective-permute-start(bf16[128,2048]{1,0:T(8,128)(2,1)} %collective-permute-done.5.w2), channel_id=1, source_target_pairs={{0,1},{8,15},{1,2},{9,8},{2,3},{10,9},{3,4},{11,10},{4,5},{12,11},... | collective-permute-start | bytes 1572872 | tf_op jit(solution)/shard_map/ppermute | solution.py:60
  55.9 5.4 %collective-permute-start = (bf16[288,128]{1,0:T(8,128)(2,1)S(1)}, bf16[288,128]{1,0:T(8,128)(2,1)S(1)}, u32[]{:S(2)}, u32[]{:S(2)}) collective-permute-start(bf16[288,128]{1,0:T(8,128)(2,1)S(1)} %get-tuple-element.30), channel_id=1, source_target_pairs={{0,16},{16,32},{32,48},{48,0},{1,17},{17,33},{33,49},{49,1},{2,18}... | collective-permute-start | bytes 221192 | tf_op jit(solution)/shard_map/ppermute | solution.py:48
  56.3 7.3 %collective-permute-start.1 = (bf16[288,128]{1,0:T(8,128)(2,1)S(1)}, bf16[288,128]{1,0:T(8,128)(2,1)S(1)}, u32[]{:S(2)}, u32[]{:S(2)}) collective-permute-start(bf16[288,128]{1,0:T(8,128)(2,1)S(1)} %get-tuple-element.29), channel_id=1, source_target_pairs={{0,32},{16,48},{32,0},{48,16},{1,33},{17,49},{33,1},{49,17},{2,34}... | collective-permute-start | bytes 221192 | tf_op jit(solution)/shard_map/ppermute | solution.py:48
  61.3 4.6 %collective-permute-start.2 = (bf16[288,128]{1,0:T(8,128)(2,1)S(1)}, bf16[288,128]{1,0:T(8,128)(2,1)S(1)}, u32[]{:S(2)}, u32[]{:S(2)}) collective-permute-start(bf16[288,128]{1,0:T(8,128)(2,1)S(1)} %get-tuple-element.28), channel_id=1, source_target_pairs={{0,48},{16,0},{32,16},{48,32},{1,49},{17,1},{33,17},{49,33},{2,50}... | collective-permute-start | bytes 221192 | tf_op jit(solution)/shard_map/ppermute | solution.py:48
  63.6 19.7 %collective-permute-start.10 = (bf16[64,2048]{1,0:T(8,128)(2,1)}, bf16[64,2048]{1,0:T(8,128)(2,1)}, u32[]{:S(2)}, u32[]{:S(2)}) collective-permute-start(bf16[64,2048]{1,0:T(8,128)(2,1)} %constant_dynamic-slice_fusion), channel_id=1, source_target_pairs={{0,2},{8,14},{1,3},{9,15},{2,4},{10,8},{3,5},{11,9},{4,6},{12,10},... | collective-permute-start | bytes 786440 | tf_op jit(solution)/shard_map/ppermute | solution.py:60
  65.9 20.2 %collective-permute-start.8 = (bf16[128,2048]{1,0:T(8,128)(2,1)}, bf16[128,2048]{1,0:T(8,128)(2,1)}, u32[]{:S(2)}, u32[]{:S(2)}) collective-permute-start(bf16[128,2048]{1,0:T(8,128)(2,1)} %collective-permute-done.5.w2), channel_id=1, source_target_pairs={{0,8},{8,0},{1,9},{9,1},{2,10},{10,2},{3,11},{11,3},{4,12},{12,4},... | collective-permute-start | bytes 1572872 | tf_op jit(solution)/shard_map/ppermute | solution.py:52
  65.9 20.2 %collective-permute-start.7 = (bf16[128,2048]{1,0:T(8,128)(2,1)}, bf16[128,2048]{1,0:T(8,128)(2,1)}, u32[]{:S(2)}, u32[]{:S(2)}) collective-permute-start(bf16[128,2048]{1,0:T(8,128)(2,1)} %collective-permute-done.4.w1), channel_id=1, source_target_pairs={{0,8},{8,0},{1,9},{9,1},{2,10},{10,2},{3,11},{11,3},{4,12},{12,4},... | collective-permute-start | bytes 1572872 | tf_op jit(solution)/shard_map/ppermute | solution.py:52
  66.4 19.7 %collective-permute-start.9 = (bf16[128,2048]{1,0:T(8,128)(2,1)}, bf16[128,2048]{1,0:T(8,128)(2,1)}, u32[]{:S(2)}, u32[]{:S(2)}) collective-permute-start(bf16[128,2048]{1,0:T(8,128)(2,1)} %collective-permute-done.6.w3), channel_id=1, source_target_pairs={{0,8},{8,0},{1,9},{9,1},{2,10},{10,2},{3,11},{11,3},{4,12},{12,4},... | collective-permute-start | bytes 1572872 | tf_op jit(solution)/shard_map/ppermute | solution.py:52
  66.8 17.3 %copy-start.13 = (s32[24,4,2]{0,2,1:T(2,128)S(1)}, s32[24,4,2]{0,2,1:T(2,128)}, u32[]{:S(2)}) copy-start(s32[24,4,2]{0,2,1:T(2,128)} %param.26) | copy-start | bytes 2308
  66.8 17.3 %copy-start.14 = (f32[24,4,2]{0,2,1:T(2,128)S(1)}, f32[24,4,2]{0,2,1:T(2,128)}, u32[]{:S(2)}) copy-start(f32[24,4,2]{0,2,1:T(2,128)} %param.25) | copy-start | bytes 2308
  66.8 17.3 %copy-start.15 = (f32[24,4]{0,1:T(4,128)S(1)}, f32[24,4]{0,1:T(4,128)}, u32[]{:S(2)}) copy-start(f32[24,4]{0,1:T(4,128)} %param.24) | copy-start | bytes 1156
  66.8 25.6 %copy-start.12 = (f32[2048]{0:T(1024)S(1)}, f32[2048]{0:T(1024)}, u32[]{:S(2)}) copy-start(f32[2048]{0:T(1024)} %param.23) | copy-start | bytes 24580
  71.7 66.8 %copy-start.3 = (bf16[1,768,2048]{2,1,0:T(8,128)(2,1)S(1)}, bf16[1,768,2048]{2,1,0:T(8,128)(2,1)}, u32[]{:S(2)}) copy-start(bf16[1,768,2048]{2,1,0:T(8,128)(2,1)} %param.29) | copy-start | bytes 9437188
  75.7 16.6 %all-to-all-start.1 = ((bf16[32,24,128]{2,1,0:T(8,128)(2,1)}), bf16[32,24,128]{2,1,0:T(8,128)(2,1)S(1)}, u32[]{:S(2)}, u32[]{:S(2)}) async-start(bf16[32,24,128]{2,1,0:T(8,128)(2,1)} %bitcast.51), calls=%async_computation.1 | async-start | bytes 393216 | tf_op jit(solution)/shard_map/all_to_all | solution.py:403
  83.4 2.1 %collective-permute-start.11 = (bf16[64,2048]{1,0:T(8,128)(2,1)}, bf16[64,2048]{1,0:T(8,128)(2,1)S(1)}, u32[]{:S(2)}, u32[]{:S(2)}) collective-permute-start(bf16[64,2048]{1,0:T(8,128)(2,1)} %collective-permute-done.10.w4), channel_id=1, source_target_pairs={{0,8},{8,0},{1,9},{9,1},{2,10},{10,2},{3,11},{11,3},{4,12},{12,4},... | collective-permute-start | bytes 786440 | tf_op jit(solution)/shard_map/ppermute | solution.py:52
  95.4 43.1 %copy-start.1 = (bf16[1,2048,768]{2,1,0:T(8,128)(2,1)S(1)}, bf16[1,2048,768]{2,1,0:T(8,128)(2,1)}, u32[]{:S(2)}) copy-start(bf16[1,2048,768]{2,1,0:T(8,128)(2,1)} %param.27) | copy-start | bytes 9437188
  95.4 43.1 %copy-start.2 = (bf16[1,2048,768]{2,1,0:T(8,128)(2,1)S(1)}, bf16[1,2048,768]{2,1,0:T(8,128)(2,1)}, u32[]{:S(2)}) copy-start(bf16[1,2048,768]{2,1,0:T(8,128)(2,1)} %param.28) | copy-start | bytes 9437188
  (12 other events, 16.9 us)

commit v5 on v4

--- a/solution.py
+++ b/solution.py
@@ -21,7 +21,7 @@
 score_scale = QK ** (-0.5) * 1.4426950408889634
 
 Y = ("half", "quad")
-ALL = ("half", "quad", "core", "tp")
+PLANE = ("half", "quad", "tp")
 
 
 def rotate(values, positions):
@@ -71,26 +71,35 @@
     return (k == (r // 2) * 32 + (r % 2) * 16 + d).astype(jnp.bfloat16)
 
 
-def pack_rows(rows_ref, out_ref, perm):
+def pack_block(rows_ref, b, perm):
+    stack = []
+    for j in range(BANDS):
+        for slot in range(2):
+            lo = slot * 128 + b * 16
+            stack.append(rows_ref[lo : lo + 16, j * LANE : (j + 1) * LANE])
+    return dot(perm, jnp.concatenate(stack, axis=0)).astype(jnp.bfloat16)
+
+
+def half_of(core):
+    return pl.ds(pl.multiple_of(core * 16, 16), 16)
+
+
+def unpack_rows(own_ref, got_ref, core, rows_ref, perm):
     for b in range(8):
-        stack = []
-        for j in range(BANDS):
-            for slot in range(2):
-                lo = slot * 128 + b * 16
-                stack.append(rows_ref[lo : lo + 16, j * LANE : (j + 1) * LANE])
-        out_ref[b * 256 : (b + 1) * 256, :] = dot(perm, jnp.concatenate(stack, axis=0)).astype(
-            jnp.bfloat16
-        )
-
-
-def unpack_rows(in_ref, rows_ref, perm):
-    for b in range(8):
-        block = dot(perm, in_ref[b * 256 : (b + 1) * 256, :]).astype(jnp.bfloat16)
+        if b < 4:
+            block = own_ref[b * 16 : (b + 1) * 16, half_of(core), :]
+        else:
+            block = got_ref[(b - 4) * 16 : (b - 3) * 16, :, :]
+        block = dot(perm, block.reshape(256, LANE)).astype(jnp.bfloat16)
         for j in range(BANDS):
             for slot in range(2):
                 lo = slot * 128 + b * 16
                 at = j * 32 + slot * 16
                 rows_ref[lo : lo + 16, j * LANE : (j + 1) * LANE] = block[at : at + 16, :]
+
+
+def pick_body(at_ref, in_ref, out_ref):
+    out_ref[...] = in_ref[:, half_of(1 - at_ref[1]), :]
 
 
 def places(meta):
@@ -166,7 +175,7 @@
 def project_body(
     at_ref,
     att_ref,
-    w0_far,
+    w0,
     w1,
     w2,
     w3,
@@ -174,22 +183,14 @@
     s2,
     s3,
     w4,
-    s4_far,
-    res_far,
+    s4,
+    res_ref,
     gain_ref,
     meta_ref,
     stream_ref,
     out_ref,
     rows,
-    w0,
-    s4,
-    res_ref,
-    sems,
 ):
-    pairs = ((w0_far, w0), (s4_far, s4), (res_far, res_ref))
-    fetches = [pltpu.make_async_copy(a, b, sems.at[n]) for n, (a, b) in enumerate(pairs)]
-    for fetch in fetches:
-        fetch.start()
     tp, core = at_ref[0], at_ref[1]
     turn = 1 - 2 * core
 
@@ -209,14 +210,10 @@
     col = lax.broadcasted_iota(jnp.int32, (count, count), 1)
     turned = (col == row % SEQS * (count // SEQS) + row // SEQS).astype(jnp.bfloat16)
     lhs = dot(turned, lhs).astype(jnp.bfloat16)
-    projected = None
+    projected = dot(lhs[:, 0:256], jnp.concatenate([w0[...], w4[...], s4[...]], axis=0))
     for n, w_ref, s_ref in ((1, w1, s1), (2, w2, s2), (3, w3, s3)):
         both = jnp.concatenate([w_ref[...], s_ref[...]], axis=0)
-        part = dot(lhs[:, n * 256 : (n + 1) * 256], both)
-        projected = part if projected is None else projected + part
-    for fetch in fetches:
-        fetch.wait()
-    projected += dot(lhs[:, 0:256], jnp.concatenate([w0[...], w4[...], s4[...]], axis=0))
+        projected += dot(lhs[:, n * 256 : (n + 1) * 256], both)
     stream = (res_ref[...].astype(jnp.float32) + projected).astype(jnp.bfloat16)
     stream_ref[...] = stream
     wide = stream.astype(jnp.float32)
@@ -228,11 +225,14 @@
     for slot in range(2):
         pick = (both * (before == slot).astype(jnp.float32)).T.astype(jnp.bfloat16)
         rows[slot * 128 : (slot + 1) * 128, :] = dot(pick, normed).astype(jnp.bfloat16)
-    pack_rows(rows, out_ref, packing(False))
-
-
-def expert_body(in_ref, gate_ref, up_ref, down_ref, out_ref, rows):
-    unpack_rows(in_ref, rows, packing(True))
+    perm = packing(False)
+    for b in range(8):
+        out_ref[b * 256 : (b + 1) * 256, :] = pack_block(rows, b, perm)
+
+
+def expert_body(at_ref, own_ref, got_ref, gate_ref, up_ref, down_ref, out_ref, rows):
+    core = at_ref[1]
+    unpack_rows(own_ref, got_ref, core, rows, packing(True))
     x = rows[...]
     hid = []
     for n in range(0, gate_ref.shape[1], 256):
@@ -243,13 +243,20 @@
     hidden = jnp.concatenate(hid, axis=1)
     for n in range(0, D, 512):
         rows[:, n : n + 512] = dot(hidden, down_ref[:, n : n + 512]).astype(jnp.bfloat16)
-    pack_rows(rows, out_ref, packing(False))
-
-
-def combine_body(in_ref, stream_ref, meta_ref, out_ref, rows):
-    unpack_rows(in_ref, rows, packing(True))
+    perm = packing(False)
+    for b in range(8):
+        side = core if b < 4 else 1 - core
+        block = pack_block(rows, b, perm).reshape(16, 16, LANE)
+        out_ref[b % 4 * 16 : (b % 4 + 1) * 16, half_of(side), :] = block
+
+
+def combine_body(at_ref, own_ref, got_ref, stream_ref, meta_ref, out_ref, rows):
+    core = at_ref[1]
+    unpack_rows(own_ref, got_ref, core, rows, packing(True))
     meta = meta_ref[...]
-    first, second, before = places(meta)
+    spot = meta[:, 0:2].astype(jnp.int32)
+    spot = (spot >> 1) + 64 * ((spot & 1) ^ core)
+    first, second, before = places(spot.astype(jnp.float32))
     logits = meta[:, 2:4]
     weights = jnp.exp(logits - jnp.max(logits, axis=-1, keepdims=True))
     mixing = weights / jnp.sum(weights, axis=-1, keepdims=True) * meta[:, 4:5]
@@ -273,9 +280,11 @@
     col = lax.broadcasted_iota(jnp.int32, (rows, count), 1)
     total = None
     for seq in range(SEQS):
+        e = route_ref[seq]
+        e = (e >> 4) * 16 + (e & 7) * 2 + ((e >> 3) & 1)
         block = jnp.concatenate(
             [
-                route_ref[seq].astype(jnp.float32),
+                e.astype(jnp.float32),
                 logit_ref[seq],
                 prob_ref[seq : seq + 1, :],
                 jnp.zeros((3, count), jnp.float32),
@@ -307,7 +316,6 @@
 
 VM = pl.BlockSpec(memory_space=pltpu.VMEM)
 SM = pl.BlockSpec(memory_space=pltpu.SMEM)
-HB = pl.BlockSpec(memory_space=pltpu.HBM)
 
 
 def layer(
@@ -409,39 +417,40 @@
             jax.ShapeDtypeStruct((rows, D), jnp.bfloat16),
             jax.ShapeDtypeStruct((2048, LANE), jnp.bfloat16),
         ),
-        in_specs=[SM, VM, HB] + [VM] * 7 + [HB, HB, VM, VM],
+        in_specs=[SM] + [VM] * 13,
         out_specs=(VM, VM),
-        scratch_shapes=[
-            vmem(256, D),
-            vmem(*out_weight.shape),
-            vmem(half_rows, D),
-            vmem(rows, D),
-            pltpu.SemaphoreType.DMA((3,)),
-        ],
+        scratch_shapes=[vmem(256, D)],
     )(at, attended, *weights, res, norm_gain.reshape(1, D), meta)
 
     def exchange(x):
-        x = x.reshape(128, 16, LANE)
-        return lax.all_to_all(x, ALL, split_axis=0, concat_axis=0, tiled=True).reshape(2048, LANE)
-
-    arrived = exchange(outgoing)
+        own = lax.all_to_all(
+            x.reshape(64, 32, LANE), PLANE, split_axis=0, concat_axis=0, tiled=True
+        )
+        other = kernel_call(
+            pick_body,
+            limit=2,
+            out_shape=jax.ShapeDtypeStruct((64, 16, LANE), jnp.bfloat16),
+            in_specs=[SM, VM],
+            out_specs=VM,
+        )(at, own)
+        return own, swap(other)
+
     served = kernel_call(
         expert_body,
         limit=10,
-        out_shape=jax.ShapeDtypeStruct((2048, LANE), jnp.bfloat16),
-        in_specs=[VM] * 4,
+        out_shape=jax.ShapeDtypeStruct((64, 32, LANE), jnp.bfloat16),
+        in_specs=[SM] + [VM] * 5,
         out_specs=VM,
         scratch_shapes=[vmem(256, D)],
-    )(arrived, w_gate[0], w_up[0], w_down[0])
-    returned = exchange(served)
+    )(at, *exchange(outgoing), w_gate[0], w_up[0], w_down[0])
     combined = kernel_call(
         combine_body,
         limit=8,
         out_shape=jax.ShapeDtypeStruct(residual.shape, jnp.bfloat16),
-        in_specs=[VM] * 3,
+        in_specs=[SM] + [VM] * 4,
         out_specs=VM,
         scratch_shapes=[vmem(256, D)],
-    )(returned, stream, meta)
+    )(at, *exchange(served), stream, meta)
     return combined
 
 

time: 183 us -> 184 us (level)
  blocking collectives: 77.1 us -> 67 us
  starting transfers between devices: 45.6 us -> 52.9 us
  waiting for transfers between devices: 24.7 us -> 27.8 us
    all_to_all x2, blocking collectives: 77.1 us -> 67 us  [exchange(): lax.all_to_all(x.reshape(64, 32, LANE), PLANE, split_axis=0, concat_axis=...]
    ppermute x5 -> x7, starting transfers between devices: 12.7 us -> 19.9 us  [swap(): return lax.ppermute(x, 'core', [(0, 1), (1, 0)])]
    ppermute x5 -> x7, waiting for transfers between devices: 1.07 us -> 4.14 us  [swap(): return lax.ppermute(x, 'core', [(0, 1), (1, 0)])]
    pallas_call x1 -> x3, Pallas kernels: 3.35 us -> 5.04 us  [the longest x1 3.88 us: layer(): kernel_call(expert_body, limit=10, out_shape=jax.ShapeDtypeStruct((64, 32...]
  transfers between devices with their start and end apart: 14 -> 16, of which waited for: 5 -> 7; matrix products, arithmetic and copies ran while one was open for 4% -> 4% of each run, Pallas kernels for 3% -> 3%
where the time goes in v5:
time: 184 us
  blocking collectives  67 us (36%)
  starting transfers between devices  52.9 us (29%)
  waiting for transfers between devices  27.8 us (15%)
  Pallas kernels  17.5 us (10%)
  local copies, waits for them, and re-layouts  12.9 us (7%)
  other arithmetic  4.54 us (2%)
    all_to_all x2, blocking collectives, exchange(): lax.all_to_all(x.reshape(64, 32, LANE), PLANE, split_axis=0, concat_axis=...  67 us
    ppermute x7, starting transfers between devices, swap(): return lax.ppermute(x, 'core', [(0, 1), (1, 0)])  19.9 us
    all_to_all x1, starting transfers between devices, layer(): near = lax.all_to_all(kv, Y, split_axis=0, concat_axis=0, tiled=True)  13.7 us
    all_to_all x1, waiting for transfers between devices, layer(): near = lax.all_to_all(kv, Y, split_axis=0, concat_axis=0, tiled=True)  11.8 us
    ppermute x4, starting transfers between devices, spread(): return lax.ppermute(x, ('core', 'tp'), pairs)  11.2 us
    all_to_all x1, starting transfers between devices, layer(): lax.all_to_all(attended, ('quad', 'tp'), split_axis=0, concat_axis=0, til...  7.6 us
    unnamed x45, local copies, waits for them, and re-layouts  6.62 us
    all_to_all x1, waiting for transfers between devices, layer(): lax.all_to_all(attended, ('quad', 'tp'), split_axis=0, concat_axis=0, til...  6.21 us
  transfers between devices with their start and end apart: 16, of which 7 were waited for; matrix products, arithmetic and copies ran while one was open for 4% of the time, Pallas kernels for 3%

profile of v5, /device:TPU:513, one launch (start us, length us, event | category | flops | bytes accessed | tf_op | source)
XLA Modules:
  0.0 183.8 jit_solution(16578658307226474914)
XLA Ops:
  4.4 13.7 %all-to-all-start = ((bf16[8,480,128]{2,1,0:T(8,128)(2,1)}), bf16[8,480,128]{2,1,0:T(8,128)(2,1)S(1)}, u32[]{:S(2)}, u32[]{:S(2)}) async-start(bf16[8,480,128]{2,1,0:T(8,128)(2,1)} %maximum_maximum_fusion), calls=%async_computation | async-start | bytes 1966080 | tf_op jit(solution)/shard_map/all_to_all | solution.py:386
  18.1 4.4 %collective-permute-start.5 = (bf16[128,2048]{1,0:T(8,128)(2,1)S(1)}, bf16[128,2048]{1,0:T(8,128)(2,1)}, u32[]{:S(2)}, u32[]{:S(2)}) collective-permute-start(bf16[128,2048]{1,0:T(8,128)(2,1)S(1)} %copy-done.8), channel_id=1, source_target_pairs={{0,2},{8,14},{1,3},{9,15},{2,4},{10,8},{3,5},{11,9},{4,6},{12,10},... | collective-permute-start | bytes 1572872 | tf_op jit(solution)/shard_map/ppermute | solution.py:60
  23.6 11.8 %all-to-all-done.a_ref = bf16[8,480,128]{2,1,0:T(8,128)(2,1)S(1)} async-done(((bf16[8,480,128]{2,1,0:T(8,128)(2,1)}), bf16[8,480,128]{2,1,0:T(8,128)(2,1)S(1)}, u32[]{:S(2)}, u32[]{:S(2)}) %all-to-all-start) | async-done | bytes 983072 | tf_op jit(solution)/shard_map/all_to_all | solution.py:386
  35.4 11.2 %collective-permute-start.3 = (bf16[8,480,128]{2,1,0:T(8,128)(2,1)S(1)}, bf16[8,480,128]{2,1,0:T(8,128)(2,1)S(1)}, u32[]{:S(2)}, u32[]{:S(2)}) collective-permute-start(bf16[8,480,128]{2,1,0:T(8,128)(2,1)S(1)} %all-to-all-done.a_ref), channel_id=1, source_target_pairs={{0,8},{8,0},{1,9},{9,1},{2,10},{10,2},{3,11},{11,3},{4,12},{12,4},... | collective-permute-start | bytes 2949128 | tf_op jit(solution)/shard_map/ppermute | solution.py:52
  47.7 1.6 slice.46
  49.4 1.8 reshape.91.res_ref
  51.3 3.5 %collective-permute-start.6 = (bf16[128,2048]{1,0:T(8,128)(2,1)}, bf16[128,2048]{1,0:T(8,128)(2,1)}, u32[]{:S(2)}, u32[]{:S(2)}) collective-permute-start(bf16[128,2048]{1,0:T(8,128)(2,1)} %collective-permute-done.5.w2), channel_id=1, source_target_pairs={{0,1},{8,15},{1,2},{9,8},{2,3},{10,9},{3,4},{11,10},{4,5},{12,11},... | collective-permute-start | bytes 1572872 | tf_op jit(solution)/shard_map/ppermute | solution.py:60
  56.3 5.0 %collective-permute-done = bf16[288,128]{1,0:T(8,128)(2,1)S(1)} collective-permute-done((bf16[288,128]{1,0:T(8,128)(2,1)S(1)}, bf16[288,128]{1,0:T(8,128)(2,1)S(1)}, u32[]{:S(2)}, u32[]{:S(2)}) %collective-permute-start) | collective-permute-done | bytes 73760 | tf_op jit(solution)/shard_map/ppermute | solution.py:48
  61.3 1.7 constant_dynamic-slice_fusion
  63.6 2.3 %collective-permute-start.10 = (bf16[64,2048]{1,0:T(8,128)(2,1)}, bf16[64,2048]{1,0:T(8,128)(2,1)}, u32[]{:S(2)}, u32[]{:S(2)}) collective-permute-start(bf16[64,2048]{1,0:T(8,128)(2,1)} %constant_dynamic-slice_fusion), channel_id=1, source_target_pairs={{0,2},{8,14},{1,3},{9,15},{2,4},{10,8},{3,5},{11,9},{4,6},{12,10},... | collective-permute-start | bytes 786440 | tf_op jit(solution)/shard_map/ppermute | solution.py:60
  66.8 2.7 %shard_map.145 = (f32[4,192,128]{2,1,0:T(8,128)S(1)}, f32[4,192,256]{2,1,0:T(8,128)S(1)}, bf16[4,192,256]{2,1,0:T(8,128)(2,1)S(1)}) custom-call(bf16[1152,128]{1,0:T(8,128)(2,1)S(1)} %pad_maximum_fusion.q_ref, bf16[8,480,128]{2,1,0:T(8,128)(2,1)S(1)} %all-to-all-done.a_ref), custom_call_target="tpu_custom_call" | custom-call | tf_op jit(solution)/shard_map/pallas_call | solution.py:390
  70.5 1.2 copy-done.6
  71.7 3.3 %shard_map.146 = bf16[4,192,128]{2,1,0:T(8,128)(2,1)S(1)} custom-call(s32[3]{0:T(128)S(1)} %pad_add_fusion.at_ref, bf16[4,192,256]{2,1,0:T(8,128)(2,1)S(1)} %get-tuple-element.17.q_ref, bf16[8,480,128]{2,1,0:T(8,128)(2,1)S(1)} %copy-done.6, f32[4,192,128]{2,1,0:T(8,128)S(1)} %get-tuple-element.18.acc_ref, f32[4,192,256]{2,1,0:T(8,128)S(1)} %get-tuple-element.19.stat_ref), custom_call_target="tpu_custom_call" | custom-call | tf_op jit(solution)/shard_map/pallas_call | solution.py:402
  75.8 7.6 %all-to-all-start.1 = ((bf16[32,24,128]{2,1,0:T(8,128)(2,1)}), bf16[32,24,128]{2,1,0:T(8,128)(2,1)S(1)}, u32[]{:S(2)}, u32[]{:S(2)}) async-start(bf16[32,24,128]{2,1,0:T(8,128)(2,1)} %bitcast.45), calls=%async_computation.1 | async-start | bytes 393216 | tf_op jit(solution)/shard_map/all_to_all | solution.py:411
  86.2 6.2 %all-to-all-done.1.att_ref = bf16[32,24,128]{2,1,0:T(8,128)(2,1)S(1)} async-done(((bf16[32,24,128]{2,1,0:T(8,128)(2,1)}), bf16[32,24,128]{2,1,0:T(8,128)(2,1)S(1)}, u32[]{:S(2)}, u32[]{:S(2)}) %all-to-all-start.1) | async-done | bytes 196640 | tf_op jit(solution)/shard_map/all_to_all | solution.py:411
  95.4 3.8 %shard_map.148 = (bf16[96,2048]{1,0:T(8,128)(2,1)S(1)}, bf16[2048,256]{1,0:T(8,128)(2,1)S(1)}) custom-call(s32[3]{0:T(128)S(1)} %pad_add_fusion.at_ref, bf16[32,24,128]{2,1,0:T(8,128)(2,1)S(1)} %all-to-all-done.1.att_ref, bf16[128,2048]{1,0:T(8,128)(2,1)S(1)} %copy-done.9, bf16[128,2048]{1,0:T(8,128)(2,1)} %collective-permute-done.4.w1, ...), custom_call_target="tpu_custom_call" | custom-call | tf_op jit(solution)/shard_map/pallas_call | solution.py:413
  99.2 32.8 %all_to_all.20.in_ref.own_ref = bf16[64,32,256]{2,1,0:T(8,128)(2,1)S(1)} all-to-all(bf16[64,32,256]{2,1,0:T(8,128)(2,1)S(1)} %bitcast.44), channel_id=1, replica_groups=mesh['grp'=2,'half'=2,'quad'=4,'core'=2,'tp'=8] {'half','quad','tp'}, dimensions={0} | all-to-all | bytes 2097152 | tf_op jit(solution)/shard_map/all_to_all | solution.py:426
  132.6 4.4 %collective-permute-start.12 = (bf16[64,16,256]{2,1,0:T(8,128)(2,1)S(1)}, bf16[64,16,256]{2,1,0:T(8,128)(2,1)S(1)}, u32[]{:S(2)}, u32[]{:S(2)}) collective-permute-start(bf16[64,16,256]{2,1,0:T(8,128)(2,1)S(1)} %shard_map.149), channel_id=1, source_target_pairs={{0,8},{8,0},{1,9},{9,1},{2,10},{10,2},{3,11},{11,3},{4,12},{12,4},... | collective-permute-start | bytes 1572872 | tf_op jit(solution)/shard_map/ppermute | solution.py:52
  136.9 1.5 collective-permute-done.12.got_ref
  138.5 3.9 %shard_map.150 = bf16[64,32,256]{2,1,0:T(8,128)(2,1)S(1)} custom-call(s32[3]{0:T(128)S(1)} %pad_add_fusion.at_ref, bf16[64,32,256]{2,1,0:T(8,128)(2,1)S(1)} %all_to_all.20.in_ref.own_ref, bf16[64,16,256]{2,1,0:T(8,128)(2,1)S(1)} %collective-permute-done.12.got_ref, bf16[2048,768]{1,0:T(8,128)(2,1)S(1)} %bitcast.41, bf16[2048,768]{1,0:T(8,128)(2,1)S(1)} %bitcast.42, ...), custom_call_target="tpu_custom_call" | custom-call | tf_op jit(solution)/shard_map/pallas_call | solution.py:438
  142.4 34.2 %all_to_all.21.in_ref.own_ref = bf16[64,32,256]{2,1,0:T(8,128)(2,1)S(1)} all-to-all(bf16[64,32,256]{2,1,0:T(8,128)(2,1)S(1)} %shard_map.150), channel_id=1, replica_groups=mesh['grp'=2,'half'=2,'quad'=4,'core'=2,'tp'=8] {'half','quad','tp'}, dimensions={0} | all-to-all | bytes 2097152 | tf_op jit(solution)/shard_map/all_to_all | solution.py:426
  177.2 2.8 %collective-permute-start.13 = (bf16[64,16,256]{2,1,0:T(8,128)(2,1)S(1)}, bf16[64,16,256]{2,1,0:T(8,128)(2,1)S(1)}, u32[]{:S(2)}, u32[]{:S(2)}) collective-permute-start(bf16[64,16,256]{2,1,0:T(8,128)(2,1)S(1)} %shard_map.151), channel_id=1, source_target_pairs={{0,8},{8,0},{1,9},{9,1},{2,10},{10,2},{3,11},{11,3},{4,12},{12,4},... | collective-permute-start | bytes 1572872 | tf_op jit(solution)/shard_map/ppermute | solution.py:52
  180.0 1.5 collective-permute-done.13.got_ref
  181.6 2.3 %shard_map.152 = bf16[24,4,2048]{2,1,0:T(4,128)(2,1)} custom-call(s32[3]{0:T(128)S(1)} %pad_add_fusion.at_ref, bf16[64,32,256]{2,1,0:T(8,128)(2,1)S(1)} %all_to_all.21.in_ref.own_ref, bf16[64,16,256]{2,1,0:T(8,128)(2,1)S(1)} %collective-permute-done.13.got_ref, bf16[96,2048]{1,0:T(8,128)(2,1)S(1)} %get-tuple-element.22.stream_ref, ...), custom_call_target="tpu_custom_call" | custom-call | tf_op jit(solution)/shard_map/pallas_call | solution.py:446
  (85 shorter events, 18.1 us)
Async XLA Ops:
  3.2 20.3 %copy-start.19 = (bf16[192,4,192]{2,1,0:T(4,128)(2,1)S(1)}, bf16[192,4,192]{2,1,0:T(4,128)(2,1)}, u32[]{:S(2)}) copy-start(bf16[192,4,192]{2,1,0:T(4,128)(2,1)} %param.16) | copy-start | bytes 884740
  4.4 31.0 %all-to-all-start = ((bf16[8,480,128]{2,1,0:T(8,128)(2,1)}), bf16[8,480,128]{2,1,0:T(8,128)(2,1)S(1)}, u32[]{:S(2)}, u32[]{:S(2)}) async-start(bf16[8,480,128]{2,1,0:T(8,128)(2,1)} %maximum_maximum_fusion), calls=%async_computation | async-start | bytes 1966080 | tf_op jit(solution)/shard_map/all_to_all | solution.py:386
  18.1 33.1 %collective-permute-start.5 = (bf16[128,2048]{1,0:T(8,128)(2,1)S(1)}, bf16[128,2048]{1,0:T(8,128)(2,1)}, u32[]{:S(2)}, u32[]{:S(2)}) collective-permute-start(bf16[128,2048]{1,0:T(8,128)(2,1)S(1)} %copy-done.8), channel_id=1, source_target_pairs={{0,2},{8,14},{1,3},{9,15},{2,4},{10,8},{3,5},{11,9},{4,6},{12,10},... | collective-permute-start | bytes 1572872 | tf_op jit(solution)/shard_map/ppermute | solution.py:60
  22.5 43.4 %collective-permute-start.4 = (bf16[128,2048]{1,0:T(8,128)(2,1)S(1)}, bf16[128,2048]{1,0:T(8,128)(2,1)}, u32[]{:S(2)}, u32[]{:S(2)}) collective-permute-start(bf16[128,2048]{1,0:T(8,128)(2,1)S(1)} %copy-done.8), channel_id=1, source_target_pairs={{0,1},{8,15},{1,2},{9,8},{2,3},{10,9},{3,4},{11,10},{4,5},{12,11},... | collective-permute-start | bytes 1572872 | tf_op jit(solution)/shard_map/ppermute | solution.py:60
  35.4 34.2 %collective-permute-start.3 = (bf16[8,480,128]{2,1,0:T(8,128)(2,1)S(1)}, bf16[8,480,128]{2,1,0:T(8,128)(2,1)S(1)}, u32[]{:S(2)}, u32[]{:S(2)}) collective-permute-start(bf16[8,480,128]{2,1,0:T(8,128)(2,1)S(1)} %all-to-all-done.a_ref), channel_id=1, source_target_pairs={{0,8},{8,0},{1,9},{9,1},{2,10},{10,2},{3,11},{11,3},{4,12},{12,4},... | collective-permute-start | bytes 2949128 | tf_op jit(solution)/shard_map/ppermute | solution.py:52
  51.3 15.2 %collective-permute-start.6 = (bf16[128,2048]{1,0:T(8,128)(2,1)}, bf16[128,2048]{1,0:T(8,128)(2,1)}, u32[]{:S(2)}, u32[]{:S(2)}) collective-permute-start(bf16[128,2048]{1,0:T(8,128)(2,1)} %collective-permute-done.5.w2), channel_id=1, source_target_pairs={{0,1},{8,15},{1,2},{9,8},{2,3},{10,9},{3,4},{11,10},{4,5},{12,11},... | collective-permute-start | bytes 1572872 | tf_op jit(solution)/shard_map/ppermute | solution.py:60
  55.9 5.4 %collective-permute-start = (bf16[288,128]{1,0:T(8,128)(2,1)S(1)}, bf16[288,128]{1,0:T(8,128)(2,1)S(1)}, u32[]{:S(2)}, u32[]{:S(2)}) collective-permute-start(bf16[288,128]{1,0:T(8,128)(2,1)S(1)} %get-tuple-element.30), channel_id=1, source_target_pairs={{0,16},{16,32},{32,48},{48,0},{1,17},{17,33},{33,49},{49,1},{2,18}... | collective-permute-start | bytes 221192 | tf_op jit(solution)/shard_map/ppermute | solution.py:48
  56.3 7.3 %collective-permute-start.1 = (bf16[288,128]{1,0:T(8,128)(2,1)S(1)}, bf16[288,128]{1,0:T(8,128)(2,1)S(1)}, u32[]{:S(2)}, u32[]{:S(2)}) collective-permute-start(bf16[288,128]{1,0:T(8,128)(2,1)S(1)} %get-tuple-element.29), channel_id=1, source_target_pairs={{0,32},{16,48},{32,0},{48,16},{1,33},{17,49},{33,1},{49,17},{2,34}... | collective-permute-start | bytes 221192 | tf_op jit(solution)/shard_map/ppermute | solution.py:48
  61.3 4.6 %collective-permute-start.2 = (bf16[288,128]{1,0:T(8,128)(2,1)S(1)}, bf16[288,128]{1,0:T(8,128)(2,1)S(1)}, u32[]{:S(2)}, u32[]{:S(2)}) collective-permute-start(bf16[288,128]{1,0:T(8,128)(2,1)S(1)} %get-tuple-element.28), channel_id=1, source_target_pairs={{0,48},{16,0},{32,16},{48,32},{1,49},{17,1},{33,17},{49,33},{2,50}... | collective-permute-start | bytes 221192 | tf_op jit(solution)/shard_map/ppermute | solution.py:48
  63.6 19.7 %collective-permute-start.10 = (bf16[64,2048]{1,0:T(8,128)(2,1)}, bf16[64,2048]{1,0:T(8,128)(2,1)}, u32[]{:S(2)}, u32[]{:S(2)}) collective-permute-start(bf16[64,2048]{1,0:T(8,128)(2,1)} %constant_dynamic-slice_fusion), channel_id=1, source_target_pairs={{0,2},{8,14},{1,3},{9,15},{2,4},{10,8},{3,5},{11,9},{4,6},{12,10},... | collective-permute-start | bytes 786440 | tf_op jit(solution)/shard_map/ppermute | solution.py:60
  65.9 20.2 %collective-permute-start.8 = (bf16[128,2048]{1,0:T(8,128)(2,1)}, bf16[128,2048]{1,0:T(8,128)(2,1)}, u32[]{:S(2)}, u32[]{:S(2)}) collective-permute-start(bf16[128,2048]{1,0:T(8,128)(2,1)} %collective-permute-done.5.w2), channel_id=1, source_target_pairs={{0,8},{8,0},{1,9},{9,1},{2,10},{10,2},{3,11},{11,3},{4,12},{12,4},... | collective-permute-start | bytes 1572872 | tf_op jit(solution)/shard_map/ppermute | solution.py:52
  65.9 20.2 %collective-permute-start.7 = (bf16[128,2048]{1,0:T(8,128)(2,1)}, bf16[128,2048]{1,0:T(8,128)(2,1)}, u32[]{:S(2)}, u32[]{:S(2)}) collective-permute-start(bf16[128,2048]{1,0:T(8,128)(2,1)} %collective-permute-done.4.w1), channel_id=1, source_target_pairs={{0,8},{8,0},{1,9},{9,1},{2,10},{10,2},{3,11},{11,3},{4,12},{12,4},... | collective-permute-start | bytes 1572872 | tf_op jit(solution)/shard_map/ppermute | solution.py:52
  66.5 19.7 %collective-permute-start.9 = (bf16[128,2048]{1,0:T(8,128)(2,1)}, bf16[128,2048]{1,0:T(8,128)(2,1)}, u32[]{:S(2)}, u32[]{:S(2)}) collective-permute-start(bf16[128,2048]{1,0:T(8,128)(2,1)} %collective-permute-done.6.w3), channel_id=1, source_target_pairs={{0,8},{8,0},{1,9},{9,1},{2,10},{10,2},{3,11},{11,3},{4,12},{12,4},... | collective-permute-start | bytes 1572872 | tf_op jit(solution)/shard_map/ppermute | solution.py:52
  66.8 17.3 %copy-start.13 = (s32[24,4,2]{0,2,1:T(2,128)S(1)}, s32[24,4,2]{0,2,1:T(2,128)}, u32[]{:S(2)}) copy-start(s32[24,4,2]{0,2,1:T(2,128)} %param.26) | copy-start | bytes 2308
  66.8 17.3 %copy-start.14 = (f32[24,4,2]{0,2,1:T(2,128)S(1)}, f32[24,4,2]{0,2,1:T(2,128)}, u32[]{:S(2)}) copy-start(f32[24,4,2]{0,2,1:T(2,128)} %param.25) | copy-start | bytes 2308
  66.8 17.3 %copy-start.15 = (f32[24,4]{0,1:T(4,128)S(1)}, f32[24,4]{0,1:T(4,128)}, u32[]{:S(2)}) copy-start(f32[24,4]{0,1:T(4,128)} %param.24) | copy-start | bytes 1156
  66.8 25.6 %copy-start.12 = (f32[2048]{0:T(1024)S(1)}, f32[2048]{0:T(1024)}, u32[]{:S(2)}) copy-start(f32[2048]{0:T(1024)} %param.23) | copy-start | bytes 24580
  71.7 66.7 %copy-start.3 = (bf16[1,768,2048]{2,1,0:T(8,128)(2,1)S(1)}, bf16[1,768,2048]{2,1,0:T(8,128)(2,1)}, u32[]{:S(2)}) copy-start(bf16[1,768,2048]{2,1,0:T(8,128)(2,1)} %param.29) | copy-start | bytes 9437188
  75.8 16.6 %all-to-all-start.1 = ((bf16[32,24,128]{2,1,0:T(8,128)(2,1)}), bf16[32,24,128]{2,1,0:T(8,128)(2,1)S(1)}, u32[]{:S(2)}, u32[]{:S(2)}) async-start(bf16[32,24,128]{2,1,0:T(8,128)(2,1)} %bitcast.45), calls=%async_computation.1 | async-start | bytes 393216 | tf_op jit(solution)/shard_map/all_to_all | solution.py:411
  83.4 2.1 %collective-permute-start.11 = (bf16[64,2048]{1,0:T(8,128)(2,1)}, bf16[64,2048]{1,0:T(8,128)(2,1)S(1)}, u32[]{:S(2)}, u32[]{:S(2)}) collective-permute-start(bf16[64,2048]{1,0:T(8,128)(2,1)} %collective-permute-done.10.w4), channel_id=1, source_target_pairs={{0,8},{8,0},{1,9},{9,1},{2,10},{10,2},{3,11},{11,3},{4,12},{12,4},... | collective-permute-start | bytes 786440 | tf_op jit(solution)/shard_map/ppermute | solution.py:52
  95.4 43.1 %copy-start.2 = (bf16[1,2048,768]{2,1,0:T(8,128)(2,1)S(1)}, bf16[1,2048,768]{2,1,0:T(8,128)(2,1)}, u32[]{:S(2)}) copy-start(bf16[1,2048,768]{2,1,0:T(8,128)(2,1)} %param.28) | copy-start | bytes 9437188
  99.2 39.3 %copy-start.1 = (bf16[1,2048,768]{2,1,0:T(8,128)(2,1)S(1)}, bf16[1,2048,768]{2,1,0:T(8,128)(2,1)}, u32[]{:S(2)}) copy-start(bf16[1,2048,768]{2,1,0:T(8,128)(2,1)} %param.27) | copy-start | bytes 9437188
  132.6 5.9 %collective-permute-start.12 = (bf16[64,16,256]{2,1,0:T(8,128)(2,1)S(1)}, bf16[64,16,256]{2,1,0:T(8,128)(2,1)S(1)}, u32[]{:S(2)}, u32[]{:S(2)}) collective-permute-start(bf16[64,16,256]{2,1,0:T(8,128)(2,1)S(1)} %shard_map.149), channel_id=1, source_target_pairs={{0,8},{8,0},{1,9},{9,1},{2,10},{10,2},{3,11},{11,3},{4,12},{12,4},... | collective-permute-start | bytes 1572872 | tf_op jit(solution)/shard_map/ppermute | solution.py:52
  177.2 4.4 %collective-permute-start.13 = (bf16[64,16,256]{2,1,0:T(8,128)(2,1)S(1)}, bf16[64,16,256]{2,1,0:T(8,128)(2,1)S(1)}, u32[]{:S(2)}, u32[]{:S(2)}) collective-permute-start(bf16[64,16,256]{2,1,0:T(8,128)(2,1)S(1)} %shard_map.151), channel_id=1, source_target_pairs={{0,8},{8,0},{1,9},{9,1},{2,10},{10,2},{3,11},{11,3},{4,12},{12,4},... | collective-permute-start | bytes 1572872 | tf_op jit(solution)/shard_map/ppermute | solution.py:52
  (14 other events, 43.6 us)

commit v6 on v4

--- a/solution.py
+++ b/solution.py
@@ -13,6 +13,7 @@
 VDIM = 128
 QK = 192
 SEQS = 4
+CHIPS = 8
 LANE = 256
 BANDS = D // LANE
 
@@ -106,6 +107,27 @@
     return first, second, before
 
 
+def expand_body(lat_ref, rope_ref, turn_ref, gain_ref, key_ref, value_ref, out_ref):
+    block = lat_ref.shape[1]
+    half = block // 2
+    turn = turn_ref[...]
+    for s in range(SEQS):
+        lat = lat_ref[s].astype(jnp.float32)
+        scale = lax.rsqrt(jnp.mean(lat * lat, axis=-1, keepdims=True) + epsilon)
+        lat = (lat * scale * gain_ref[...]).astype(jnp.bfloat16)
+        keys = dot(lat, key_ref[...]).astype(jnp.bfloat16)
+        values = dot(lat, value_ref[...]).astype(jnp.bfloat16)
+        rope = rope_ref[s].astype(jnp.float32)
+        rope = jnp.concatenate([rope, rope], axis=1)
+        rot = rope * turn[:, 0:128] + pltpu.roll(rope, 32, 1) * turn[:, 128:256]
+        low = lax.broadcasted_iota(jnp.int32, (half, 128), 1) < ROPE
+        rot = jnp.where(low, rot[0:half], rot[half:]).astype(jnp.bfloat16)
+        for at in (s, SEQS + s):
+            out_ref[at, 0:block, :] = keys
+            out_ref[at, block : 2 * block, :] = values
+            out_ref[at, 2 * block :, :] = rot
+
+
 def load_keys(src, keys, values):
     for j in range(8):
         lo, hi = j * 96, 768 + j * 96
@@ -166,7 +188,7 @@
 def project_body(
     at_ref,
     att_ref,
-    w0_far,
+    w0,
     w1,
     w2,
     w3,
@@ -174,22 +196,14 @@
     s2,
     s3,
     w4,
-    s4_far,
-    res_far,
+    s4,
+    res_ref,
     gain_ref,
     meta_ref,
     stream_ref,
     out_ref,
     rows,
-    w0,
-    s4,
-    res_ref,
-    sems,
 ):
-    pairs = ((w0_far, w0), (s4_far, s4), (res_far, res_ref))
-    fetches = [pltpu.make_async_copy(a, b, sems.at[n]) for n, (a, b) in enumerate(pairs)]
-    for fetch in fetches:
-        fetch.start()
     tp, core = at_ref[0], at_ref[1]
     turn = 1 - 2 * core
 
@@ -209,14 +223,10 @@
     col = lax.broadcasted_iota(jnp.int32, (count, count), 1)
     turned = (col == row % SEQS * (count // SEQS) + row // SEQS).astype(jnp.bfloat16)
     lhs = dot(turned, lhs).astype(jnp.bfloat16)
-    projected = None
+    projected = dot(lhs[:, 0:256], jnp.concatenate([w0[...], w4[...], s4[...]], axis=0))
     for n, w_ref, s_ref in ((1, w1, s1), (2, w2, s2), (3, w3, s3)):
         both = jnp.concatenate([w_ref[...], s_ref[...]], axis=0)
-        part = dot(lhs[:, n * 256 : (n + 1) * 256], both)
-        projected = part if projected is None else projected + part
-    for fetch in fetches:
-        fetch.wait()
-    projected += dot(lhs[:, 0:256], jnp.concatenate([w0[...], w4[...], s4[...]], axis=0))
+        projected += dot(lhs[:, n * 256 : (n + 1) * 256], both)
     stream = (res_ref[...].astype(jnp.float32) + projected).astype(jnp.bfloat16)
     stream_ref[...] = stream
     wide = stream.astype(jnp.float32)
@@ -307,7 +317,6 @@
 
 VM = pl.BlockSpec(memory_space=pltpu.VMEM)
 SM = pl.BlockSpec(memory_space=pltpu.SMEM)
-HB = pl.BlockSpec(memory_space=pltpu.HBM)
 
 
 def layer(
@@ -356,16 +365,25 @@
         queries.append(shift(piece, "quad", k, 4))
     queries = jnp.concatenate(queries, axis=0)
 
-    lat = jnp.swapaxes(latent, 0, 1).astype(jnp.float32)
-    lat = (
-        lat * lax.rsqrt(jnp.mean(lat * lat, axis=-1, keepdims=True) + epsilon) * latent_gain
-    ).astype(jnp.bfloat16)
-    keys = jnp.einsum("spd,dc->spc", lat, key_up, preferred_element_type=jnp.float32)
-    vals = jnp.einsum("spd,dc->spc", lat, value_up, preferred_element_type=jnp.float32)
-    rot = rotate(jnp.swapaxes(rope_key, 0, 1).astype(jnp.float32), positions)
-    rot = jnp.concatenate([rot[:, : block // 2], rot[:, block // 2 :]], axis=-1)
-    kv = jnp.concatenate([keys, vals, rot], axis=1).astype(jnp.bfloat16)
-    kv = jnp.concatenate([kv, kv], axis=0)
+    halfway = ROPE // 2
+    inverse = rotary_base ** (-jnp.arange(halfway, dtype=jnp.float32) / halfway)
+    angles = positions.astype(jnp.float32)[:, None] * jnp.concatenate([inverse] * 4)[None, :]
+    sign = jnp.concatenate([-jnp.ones((halfway,)), jnp.ones((halfway,))] * 2)[None, :]
+    turn = jnp.concatenate([jnp.cos(angles), jnp.sin(angles) * sign], axis=1)
+    kv = kernel_call(
+        expand_body,
+        limit=12,
+        out_shape=jax.ShapeDtypeStruct((CHIPS, 2 * block + block // 2, 128), jnp.bfloat16),
+        in_specs=[VM] * 6,
+        out_specs=VM,
+    )(
+        jnp.swapaxes(latent, 0, 1),
+        jnp.swapaxes(rope_key, 0, 1),
+        turn,
+        latent_gain.reshape(1, -1),
+        key_up,
+        value_up,
+    )
     kv, at = lax.optimization_barrier((kv, at))
     half_rows = out_weight.shape[0] // 2
     one, two = spread(out_weight, 1, tp_size), spread(out_weight, 2, tp_size)
@@ -409,15 +427,9 @@
             jax.ShapeDtypeStruct((rows, D), jnp.bfloat16),
             jax.ShapeDtypeStruct((2048, LANE), jnp.bfloat16),
         ),
-        in_specs=[SM, VM, HB] + [VM] * 7 + [HB, HB, VM, VM],
+        in_specs=[SM] + [VM] * 13,
         out_specs=(VM, VM),
-        scratch_shapes=[
-            vmem(256, D),
-            vmem(*out_weight.shape),
-            vmem(half_rows, D),
-            vmem(rows, D),
-            pltpu.SemaphoreType.DMA((3,)),
-        ],
+        scratch_shapes=[vmem(256, D)],
     )(at, attended, *weights, res, norm_gain.reshape(1, D), meta)
 
     def exchange(x):

time: 183 us -> 186 us (1.016)
  local copies, waits for them, and re-layouts: 12.9 us -> 17.4 us
  waiting for transfers between devices: 24.7 us -> 21.9 us
    unnamed x45, local copies, waits for them, and re-layouts: 6.61 us -> 13.3 us
  transfers between devices with their start and end apart: 14 -> 14, of which waited for: 5 -> 4; matrix products, arithmetic and copies ran while one was open for 4% -> 5% of each run, Pallas kernels for 3% -> 3%
where the time goes in v6:
time: 186 us
  blocking collectives  77.1 us (41%)
  starting transfers between devices  45.5 us (24%)
  waiting for transfers between devices  21.9 us (12%)
  local copies, waits for them, and re-layouts  17.4 us (9%)
  Pallas kernels  17 us (9%)
  other arithmetic  6.37 us (3%)
    all_to_all x2, blocking collectives, exchange(): lax.all_to_all(x, ALL, split_axis=0, concat_axis=0, tiled=True)  77.1 us
    all_to_all x1, starting transfers between devices, layer(): near = lax.all_to_all(kv, Y, split_axis=0, concat_axis=0, tiled=True)  13.7 us
    unnamed x45, local copies, waits for them, and re-layouts  13.3 us
    ppermute x5, starting transfers between devices, swap(): return lax.ppermute(x, 'core', [(0, 1), (1, 0)])  12.7 us
    ppermute x4, starting transfers between devices, spread(): return lax.ppermute(x, ('core', 'tp'), pairs)  11.2 us
    all_to_all x1, waiting for transfers between devices, layer(): near = lax.all_to_all(kv, Y, split_axis=0, concat_axis=0, tiled=True)  10.7 us
    all_to_all x1, starting transfers between devices, layer(): lax.all_to_all(attended, ('quad', 'tp'), split_axis=0, concat_axis=0, til...  7.62 us
    ppermute x3, waiting for transfers between devices, shift(): return lax.ppermute(x, axis, [(i, (i + by) % size) for i in range(size)])  5.86 us
  transfers between devices with their start and end apart: 14, of which 4 were waited for; matrix products, arithmetic and copies ran while one was open for 5% of the time, Pallas kernels for 3%

profile of v6, /device:TPU:513, one launch (start us, length us, event | category | flops | bytes accessed | tf_op | source)
XLA Modules:
  0.0 185.6 jit_solution(2669160570507666757)
XLA Ops:
  0.1 1.4 copy.23
  6.2 1.7 shard_map.145
  7.9 13.7 %all-to-all-start = ((bf16[8,480,128]{2,1,0:T(8,128)(2,1)}), bf16[8,480,128]{2,1,0:T(8,128)(2,1)S(1)}, u32[]{:S(2)}, u32[]{:S(2)}) async-start(bf16[8,480,128]{2,1,0:T(8,128)(2,1)} %shard_map.145), calls=%async_computation | async-start | bytes 1966080 | tf_op jit(solution)/shard_map/all_to_all | solution.py:396
  21.6 4.4 %collective-permute-start.5 = (bf16[128,2048]{1,0:T(8,128)(2,1)S(1)}, bf16[128,2048]{1,0:T(8,128)(2,1)}, u32[]{:S(2)}, u32[]{:S(2)}) collective-permute-start(bf16[128,2048]{1,0:T(8,128)(2,1)S(1)} %copy-done.6), channel_id=1, source_target_pairs={{0,2},{8,14},{1,3},{9,15},{2,4},{10,8},{3,5},{11,9},{4,6},{12,10},... | collective-permute-start | bytes 1572872 | tf_op jit(solution)/shard_map/ppermute | solution.py:61
  27.1 1.1 multiply_cosine_fusion
  28.2 10.7 %all-to-all-done.a_ref = bf16[8,480,128]{2,1,0:T(8,128)(2,1)S(1)} async-done(((bf16[8,480,128]{2,1,0:T(8,128)(2,1)}), bf16[8,480,128]{2,1,0:T(8,128)(2,1)S(1)}, u32[]{:S(2)}, u32[]{:S(2)}) %all-to-all-start) | async-done | bytes 983072 | tf_op jit(solution)/shard_map/all_to_all | solution.py:396
  38.9 11.2 %collective-permute-start.3 = (bf16[8,480,128]{2,1,0:T(8,128)(2,1)S(1)}, bf16[8,480,128]{2,1,0:T(8,128)(2,1)S(1)}, u32[]{:S(2)}, u32[]{:S(2)}) collective-permute-start(bf16[8,480,128]{2,1,0:T(8,128)(2,1)S(1)} %all-to-all-done.a_ref), channel_id=1, source_target_pairs={{0,8},{8,0},{1,9},{9,1},{2,10},{10,2},{3,11},{11,3},{4,12},{12,4},... | collective-permute-start | bytes 2949128 | tf_op jit(solution)/shard_map/ppermute | solution.py:53
  50.1 1.8 subtract_convert_fusion
  52.6 1.1 reshape.95.res_ref
  54.7 3.5 %collective-permute-start.6 = (bf16[128,2048]{1,0:T(8,128)(2,1)}, bf16[128,2048]{1,0:T(8,128)(2,1)}, u32[]{:S(2)}, u32[]{:S(2)}) collective-permute-start(bf16[128,2048]{1,0:T(8,128)(2,1)} %collective-permute-done.5.w2), channel_id=1, source_target_pairs={{0,1},{8,15},{1,2},{9,8},{2,3},{10,9},{3,4},{11,10},{4,5},{12,11},... | collective-permute-start | bytes 1572872 | tf_op jit(solution)/shard_map/ppermute | solution.py:61
  58.2 1.1 fusion.7
  60.3 5.2 %collective-permute-done = bf16[288,128]{1,0:T(8,128)(2,1)S(1)} collective-permute-done((bf16[288,128]{1,0:T(8,128)(2,1)}, bf16[288,128]{1,0:T(8,128)(2,1)S(1)}, u32[]{:S(2)}, u32[]{:S(2)}) %collective-permute-start) | collective-permute-done | bytes 73760 | tf_op jit(solution)/shard_map/ppermute | solution.py:49
  65.6 1.7 constant_dynamic-slice_fusion
  67.9 2.3 %collective-permute-start.10 = (bf16[64,2048]{1,0:T(8,128)(2,1)}, bf16[64,2048]{1,0:T(8,128)(2,1)}, u32[]{:S(2)}, u32[]{:S(2)}) collective-permute-start(bf16[64,2048]{1,0:T(8,128)(2,1)} %constant_dynamic-slice_fusion), channel_id=1, source_target_pairs={{0,2},{8,14},{1,3},{9,15},{2,4},{10,8},{3,5},{11,9},{4,6},{12,10},... | collective-permute-start | bytes 786440 | tf_op jit(solution)/shard_map/ppermute | solution.py:61
  71.0 2.7 %shard_map.146 = (f32[4,192,128]{2,1,0:T(8,128)S(1)}, f32[4,192,256]{2,1,0:T(8,128)S(1)}, bf16[4,192,256]{2,1,0:T(8,128)(2,1)S(1)}) custom-call(bf16[1152,128]{1,0:T(8,128)(2,1)S(1)} %pad_maximum_fusion.q_ref, bf16[8,480,128]{2,1,0:T(8,128)(2,1)S(1)} %all-to-all-done.a_ref), custom_call_target="tpu_custom_call" | custom-call | tf_op jit(solution)/shard_map/pallas_call | solution.py:400
  74.7 1.2 copy-done.4
  75.9 3.3 %shard_map.147 = bf16[4,192,128]{2,1,0:T(8,128)(2,1)S(1)} custom-call(s32[3]{0:T(128)S(1)} %pad_add_fusion.at_ref, bf16[4,192,256]{2,1,0:T(8,128)(2,1)S(1)} %get-tuple-element.17.q_ref, bf16[8,480,128]{2,1,0:T(8,128)(2,1)S(1)} %copy-done.4, f32[4,192,128]{2,1,0:T(8,128)S(1)} %get-tuple-element.18.acc_ref, f32[4,192,256]{2,1,0:T(8,128)S(1)} %get-tuple-element.19.stat_ref), custom_call_target="tpu_custom_call" | custom-call | tf_op jit(solution)/shard_map/pallas_call | solution.py:412
  80.0 7.6 %all-to-all-start.1 = ((bf16[32,24,128]{2,1,0:T(8,128)(2,1)}), bf16[32,24,128]{2,1,0:T(8,128)(2,1)}, u32[]{:S(2)}, u32[]{:S(2)}) async-start(bf16[32,24,128]{2,1,0:T(8,128)(2,1)} %bitcast.39), calls=%async_computation.1 | async-start | bytes 393216 | tf_op jit(solution)/shard_map/all_to_all | solution.py:421
  91.3 5.4 %all-to-all-done.1.att_ref = bf16[32,24,128]{2,1,0:T(8,128)(2,1)} async-done(((bf16[32,24,128]{2,1,0:T(8,128)(2,1)}), bf16[32,24,128]{2,1,0:T(8,128)(2,1)}, u32[]{:S(2)}, u32[]{:S(2)}) %all-to-all-start.1) | async-done | bytes 196640 | tf_op jit(solution)/shard_map/all_to_all | solution.py:421
  99.5 3.9 %shard_map.149 = (bf16[96,2048]{1,0:T(8,128)(2,1)S(1)}, bf16[2048,256]{1,0:T(8,128)(2,1)S(1)}) custom-call(s32[3]{0:T(128)S(1)} %pad_add_fusion.at_ref, bf16[32,24,128]{2,1,0:T(8,128)(2,1)} %all-to-all-done.1.att_ref, bf16[128,2048]{1,0:T(8,128)(2,1)S(1)} %copy-done.7, bf16[128,2048]{1,0:T(8,128)(2,1)} %collective-permute-done.4.w1, ...), custom_call_target="tpu_custom_call" | custom-call | tf_op jit(solution)/shard_map/pallas_call | solution.py:423
  103.4 38.7 %all_to_all.20 = bf16[128,16,256]{2,1,0:T(8,128)(2,1)S(1)} all-to-all(bf16[128,16,256]{2,1,0:T(8,128)(2,1)S(1)} %bitcast.38), channel_id=1, replica_groups=mesh['grp'=2,'half'=2,'quad'=4,'core'=2,'tp'=8] {'half','quad','core','tp'}, dimensions={0} | all-to-all | bytes 2097152 | tf_op jit(solution)/shard_map/all_to_all | solution.py:437
  142.2 3.3 %shard_map.150 = bf16[2048,256]{1,0:T(8,128)(2,1)S(1)} custom-call(bf16[2048,256]{1,0:T(8,128)(2,1)S(1)} %bitcast.32, bf16[2048,768]{1,0:T(8,128)(2,1)S(1)} %bitcast.35, bf16[2048,768]{1,0:T(8,128)(2,1)S(1)} %bitcast.36, bf16[768,2048]{1,0:T(8,128)(2,1)S(1)} %bitcast.37), custom_call_target="tpu_custom_call" | custom-call | tf_op jit(solution)/shard_map/pallas_call | solution.py:440
  145.5 38.4 %all_to_all.21 = bf16[128,16,256]{2,1,0:T(8,128)(2,1)S(1)} all-to-all(bf16[128,16,256]{2,1,0:T(8,128)(2,1)S(1)} %bitcast.33), channel_id=1, replica_groups=mesh['grp'=2,'half'=2,'quad'=4,'core'=2,'tp'=8] {'half','quad','core','tp'}, dimensions={0} | all-to-all | bytes 2097152 | tf_op jit(solution)/shard_map/all_to_all | solution.py:437
  183.9 1.7 shard_map.151
  (74 shorter events, 18.2 us)
Async XLA Ops:
  0.1 21.5 %copy-start.6 = (bf16[128,2048]{1,0:T(8,128)(2,1)S(1)}, bf16[128,2048]{1,0:T(8,128)(2,1)}, u32[]{:S(2)}) copy-start(bf16[128,2048]{1,0:T(8,128)(2,1)} %w0.1) | copy-start | bytes 1572868
  0.1 26.9 %copy-start.20 = (bf16[192,4,192]{2,1,0:T(4,128)(2,1)S(1)}, bf16[192,4,192]{2,1,0:T(4,128)(2,1)}, u32[]{:S(2)}) copy-start(bf16[192,4,192]{2,1,0:T(4,128)(2,1)} %param.16) | copy-start | bytes 884740
  7.9 31.0 %all-to-all-start = ((bf16[8,480,128]{2,1,0:T(8,128)(2,1)}), bf16[8,480,128]{2,1,0:T(8,128)(2,1)S(1)}, u32[]{:S(2)}, u32[]{:S(2)}) async-start(bf16[8,480,128]{2,1,0:T(8,128)(2,1)} %shard_map.145), calls=%async_computation | async-start | bytes 1966080 | tf_op jit(solution)/shard_map/all_to_all | solution.py:396
  21.6 33.0 %collective-permute-start.5 = (bf16[128,2048]{1,0:T(8,128)(2,1)S(1)}, bf16[128,2048]{1,0:T(8,128)(2,1)}, u32[]{:S(2)}, u32[]{:S(2)}) collective-permute-start(bf16[128,2048]{1,0:T(8,128)(2,1)S(1)} %copy-done.6), channel_id=1, source_target_pairs={{0,2},{8,14},{1,3},{9,15},{2,4},{10,8},{3,5},{11,9},{4,6},{12,10},... | collective-permute-start | bytes 1572872 | tf_op jit(solution)/shard_map/ppermute | solution.py:61
  26.0 44.2 %collective-permute-start.4 = (bf16[128,2048]{1,0:T(8,128)(2,1)S(1)}, bf16[128,2048]{1,0:T(8,128)(2,1)}, u32[]{:S(2)}, u32[]{:S(2)}) collective-permute-start(bf16[128,2048]{1,0:T(8,128)(2,1)S(1)} %copy-done.6), channel_id=1, source_target_pairs={{0,1},{8,15},{1,2},{9,8},{2,3},{10,9},{3,4},{11,10},{4,5},{12,11},... | collective-permute-start | bytes 1572872 | tf_op jit(solution)/shard_map/ppermute | solution.py:61
  38.9 34.9 %collective-permute-start.3 = (bf16[8,480,128]{2,1,0:T(8,128)(2,1)S(1)}, bf16[8,480,128]{2,1,0:T(8,128)(2,1)S(1)}, u32[]{:S(2)}, u32[]{:S(2)}) collective-permute-start(bf16[8,480,128]{2,1,0:T(8,128)(2,1)S(1)} %all-to-all-done.a_ref), channel_id=1, source_target_pairs={{0,8},{8,0},{1,9},{9,1},{2,10},{10,2},{3,11},{11,3},{4,12},{12,4},... | collective-permute-start | bytes 2949128 | tf_op jit(solution)/shard_map/ppermute | solution.py:53
  54.7 16.0 %collective-permute-start.6 = (bf16[128,2048]{1,0:T(8,128)(2,1)}, bf16[128,2048]{1,0:T(8,128)(2,1)}, u32[]{:S(2)}, u32[]{:S(2)}) collective-permute-start(bf16[128,2048]{1,0:T(8,128)(2,1)} %collective-permute-done.5.w2), channel_id=1, source_target_pairs={{0,1},{8,15},{1,2},{9,8},{2,3},{10,9},{3,4},{11,10},{4,5},{12,11},... | collective-permute-start | bytes 1572872 | tf_op jit(solution)/shard_map/ppermute | solution.py:61
  59.3 29.0 %copy-start.16 = (s32[24,4,2]{0,2,1:T(2,128)S(1)}, s32[24,4,2]{0,2,1:T(2,128)}, u32[]{:S(2)}) copy-start(s32[24,4,2]{0,2,1:T(2,128)} %param.26) | copy-start | bytes 2308
  59.3 37.4 %copy-start.15 = (f32[2048]{0:T(1024)S(1)}, f32[2048]{0:T(1024)}, u32[]{:S(2)}) copy-start(f32[2048]{0:T(1024)} %param.23) | copy-start | bytes 24580
  60.0 5.5 %collective-permute-start = (bf16[288,128]{1,0:T(8,128)(2,1)}, bf16[288,128]{1,0:T(8,128)(2,1)S(1)}, u32[]{:S(2)}, u32[]{:S(2)}) collective-permute-start(bf16[288,128]{1,0:T(8,128)(2,1)} %get-tuple-element.28), channel_id=1, source_target_pairs={{0,16},{16,32},{32,48},{48,0},{1,17},{17,33},{33,49},{49,1},{2,18}... | collective-permute-start | bytes 221192 | tf_op jit(solution)/shard_map/ppermute | solution.py:49
  60.3 7.5 %collective-permute-start.1 = (bf16[288,128]{1,0:T(8,128)(2,1)}, bf16[288,128]{1,0:T(8,128)(2,1)S(1)}, u32[]{:S(2)}, u32[]{:S(2)}) collective-permute-start(bf16[288,128]{1,0:T(8,128)(2,1)} %get-tuple-element.27), channel_id=1, source_target_pairs={{0,32},{16,48},{32,0},{48,16},{1,33},{17,49},{33,1},{49,17},{2,34}... | collective-permute-start | bytes 221192 | tf_op jit(solution)/shard_map/ppermute | solution.py:49
  65.5 4.6 %collective-permute-start.2 = (bf16[288,128]{1,0:T(8,128)(2,1)S(1)}, bf16[288,128]{1,0:T(8,128)(2,1)S(1)}, u32[]{:S(2)}, u32[]{:S(2)}) collective-permute-start(bf16[288,128]{1,0:T(8,128)(2,1)S(1)} %get-tuple-element.26), channel_id=1, source_target_pairs={{0,48},{16,0},{32,16},{48,32},{1,49},{17,1},{33,17},{49,33},{2,50}... | collective-permute-start | bytes 221192 | tf_op jit(solution)/shard_map/ppermute | solution.py:49
  67.9 19.7 %collective-permute-start.10 = (bf16[64,2048]{1,0:T(8,128)(2,1)}, bf16[64,2048]{1,0:T(8,128)(2,1)}, u32[]{:S(2)}, u32[]{:S(2)}) collective-permute-start(bf16[64,2048]{1,0:T(8,128)(2,1)} %constant_dynamic-slice_fusion), channel_id=1, source_target_pairs={{0,2},{8,14},{1,3},{9,15},{2,4},{10,8},{3,5},{11,9},{4,6},{12,10},... | collective-permute-start | bytes 786440 | tf_op jit(solution)/shard_map/ppermute | solution.py:61
  70.2 21.1 %collective-permute-start.8 = (bf16[128,2048]{1,0:T(8,128)(2,1)}, bf16[128,2048]{1,0:T(8,128)(2,1)}, u32[]{:S(2)}, u32[]{:S(2)}) collective-permute-start(bf16[128,2048]{1,0:T(8,128)(2,1)} %collective-permute-done.5.w2), channel_id=1, source_target_pairs={{0,8},{8,0},{1,9},{9,1},{2,10},{10,2},{3,11},{11,3},{4,12},{12,4},... | collective-permute-start | bytes 1572872 | tf_op jit(solution)/shard_map/ppermute | solution.py:53
  70.2 21.1 %collective-permute-start.7 = (bf16[128,2048]{1,0:T(8,128)(2,1)}, bf16[128,2048]{1,0:T(8,128)(2,1)}, u32[]{:S(2)}, u32[]{:S(2)}) collective-permute-start(bf16[128,2048]{1,0:T(8,128)(2,1)} %collective-permute-done.4.w1), channel_id=1, source_target_pairs={{0,8},{8,0},{1,9},{9,1},{2,10},{10,2},{3,11},{11,3},{4,12},{12,4},... | collective-permute-start | bytes 1572872 | tf_op jit(solution)/shard_map/ppermute | solution.py:53
  70.7 20.6 %collective-permute-start.9 = (bf16[128,2048]{1,0:T(8,128)(2,1)}, bf16[128,2048]{1,0:T(8,128)(2,1)}, u32[]{:S(2)}, u32[]{:S(2)}) collective-permute-start(bf16[128,2048]{1,0:T(8,128)(2,1)} %collective-permute-done.6.w3), channel_id=1, source_target_pairs={{0,8},{8,0},{1,9},{9,1},{2,10},{10,2},{3,11},{11,3},{4,12},{12,4},... | collective-permute-start | bytes 1572872 | tf_op jit(solution)/shard_map/ppermute | solution.py:53
  74.7 1.2 copy-start.4
  75.9 66.2 %copy-start.2 = (bf16[1,768,2048]{2,1,0:T(8,128)(2,1)S(1)}, bf16[1,768,2048]{2,1,0:T(8,128)(2,1)}, u32[]{:S(2)}) copy-start(bf16[1,768,2048]{2,1,0:T(8,128)(2,1)} %param.29) | copy-start | bytes 9437188
  80.0 16.7 %all-to-all-start.1 = ((bf16[32,24,128]{2,1,0:T(8,128)(2,1)}), bf16[32,24,128]{2,1,0:T(8,128)(2,1)}, u32[]{:S(2)}, u32[]{:S(2)}) async-start(bf16[32,24,128]{2,1,0:T(8,128)(2,1)} %bitcast.39), calls=%async_computation.1 | async-start | bytes 393216 | tf_op jit(solution)/shard_map/all_to_all | solution.py:421
  87.6 3.0 %collective-permute-start.11 = (bf16[64,2048]{1,0:T(8,128)(2,1)}, bf16[64,2048]{1,0:T(8,128)(2,1)S(1)}, u32[]{:S(2)}, u32[]{:S(2)}) collective-permute-start(bf16[64,2048]{1,0:T(8,128)(2,1)} %collective-permute-done.10.w4), channel_id=1, source_target_pairs={{0,8},{8,0},{1,9},{9,1},{2,10},{10,2},{3,11},{11,3},{4,12},{12,4},... | collective-permute-start | bytes 786440 | tf_op jit(solution)/shard_map/ppermute | solution.py:53
  96.7 1.0 copy-start.7
  99.5 42.6 %copy-start = (bf16[1,2048,768]{2,1,0:T(8,128)(2,1)S(1)}, bf16[1,2048,768]{2,1,0:T(8,128)(2,1)}, u32[]{:S(2)}) copy-start(bf16[1,2048,768]{2,1,0:T(8,128)(2,1)} %param.27) | copy-start | bytes 9437188
  99.5 42.6 %copy-start.1 = (bf16[1,2048,768]{2,1,0:T(8,128)(2,1)S(1)}, bf16[1,2048,768]{2,1,0:T(8,128)(2,1)}, u32[]{:S(2)}) copy-start(bf16[1,2048,768]{2,1,0:T(8,128)(2,1)} %param.28) | copy-start | bytes 9437188
  142.1 41.7 %copy-start.10 = (f32[96,8]{1,0:T(8,128)S(1)}, f32[96,8]{1,0:T(8,128)}, u32[]{:S(2)}) copy-start(f32[96,8]{1,0:T(8,128)} %copy-done.8) | copy-start | bytes 9220
  (11 other events, 8.6 us)

commit v7 on v3

--- a/solution.py
+++ b/solution.py
@@ -166,7 +166,6 @@
 def project_body(
     at_ref,
     att_ref,
-    w0,
     w1,
     w2,
     w3,
@@ -201,11 +200,12 @@
     col = lax.broadcasted_iota(jnp.int32, (count, count), 1)
     turned = (col == row % SEQS * (count // SEQS) + row // SEQS).astype(jnp.bfloat16)
     lhs = dot(turned, lhs).astype(jnp.bfloat16)
-    projected = dot(lhs[:, 0:256], jnp.concatenate([w0[...], w4[...], s4[...]], axis=0))
+    first = jnp.concatenate([res_ref[count:, :], w4[...], s4[...]], axis=0)
+    projected = dot(lhs[:, 0:256], first)
     for n, w_ref, s_ref in ((1, w1, s1), (2, w2, s2), (3, w3, s3)):
         both = jnp.concatenate([w_ref[...], s_ref[...]], axis=0)
         projected += dot(lhs[:, n * 256 : (n + 1) * 256], both)
-    stream = (res_ref[...].astype(jnp.float32) + projected).astype(jnp.bfloat16)
+    stream = (res_ref[0:count, :].astype(jnp.float32) + projected).astype(jnp.bfloat16)
     stream_ref[...] = stream
     wide = stream.astype(jnp.float32)
     normed = (
@@ -301,7 +301,7 @@
     q_rot = rotate(q[..., NOPE:].astype(jnp.float32), positions).astype(jnp.bfloat16)
     q_rot = jnp.concatenate([q_rot[:, : block // 2], q_rot[:, block // 2 :]], axis=-1)
     q = jnp.concatenate([q[..., :NOPE], q_rot], axis=1)
-    res = residual.reshape(rows, D)
+    res = jnp.concatenate([residual.reshape(rows, D), out_weight], axis=0)
     meta = jnp.concatenate(
         [routes.astype(jnp.float32), pair_logits, group_prob[..., None]], axis=-1
     )
@@ -329,7 +329,7 @@
     three = spread(two, 1, tp_size)
     part = lax.dynamic_slice(two, (core * half_rows, 0), (half_rows, D))
     four = spread(part, 2, tp_size)
-    weights = [out_weight, one, two, three, swap(one), swap(two)]
+    weights = [one, two, three, swap(one), swap(two)]
     weights += [swap(three), four, swap(four)]
 
     near = lax.all_to_all(kv, Y, split_axis=0, concat_axis=0, tiled=True)
@@ -366,7 +366,7 @@
             jax.ShapeDtypeStruct((rows, D), jnp.bfloat16),
             jax.ShapeDtypeStruct((2048, LANE), jnp.bfloat16),
         ),
-        in_specs=[SM] + [VM] * 13,
+        in_specs=[SM] + [VM] * 12,
         out_specs=(VM, VM),
         scratch_shapes=[vmem(256, D)],
     )(at, attended, *weights, res, norm_gain.reshape(1, D), meta)

time: 177 us -> 178 us (level)
  other arithmetic: 3.69 us -> 6.33 us
  local copies, waits for them, and re-layouts: 10 us -> 7.66 us
    unnamed x41 -> x29, local copies, waits for them, and re-layouts: 5.14 us -> 2.17 us
  transfers between devices with their start and end apart: 14 -> 14, of which waited for: 5 -> 5; matrix products, arithmetic and copies ran while one was open for 3% -> 5% of each run, Pallas kernels for 3% -> 4%
where the time goes in v7:
time: 178 us; the launch traced here: 177 us
  blocking collectives  77.1 us (43%)
  starting transfers between devices  45.7 us (26%)
  waiting for transfers between devices  23.6 us (13%)
  Pallas kernels  15.5 us (9%)
  local copies, waits for them, and re-layouts  7.66 us (4%)
  other arithmetic  6.33 us (4%)
    all_to_all x2, blocking collectives, exchange(): lax.all_to_all(x, ALL, split_axis=0, concat_axis=0, tiled=True)  77.1 us
    all_to_all x1, starting transfers between devices, layer(): near = lax.all_to_all(kv, Y, split_axis=0, concat_axis=0, tiled=True)  13.7 us
    ppermute x5, starting transfers between devices, swap(): return lax.ppermute(x, 'core', [(0, 1), (1, 0)])  12.7 us
    ppermute x4, starting transfers between devices, spread(): return lax.ppermute(x, ('core', 'tp'), pairs)  11.2 us
    all_to_all x1, waiting for transfers between devices, layer(): near = lax.all_to_all(kv, Y, split_axis=0, concat_axis=0, tiled=True)  8.47 us
    all_to_all x1, starting transfers between devices, layer(): lax.all_to_all(attended, ('quad', 'tp'), split_axis=0, concat_axis=0, til...  7.81 us
    ppermute x3, waiting for transfers between devices, shift(): return lax.ppermute(x, axis, [(i, (i + by) % size) for i in range(size)])  6.92 us
    all_to_all x1, waiting for transfers between devices, layer(): lax.all_to_all(attended, ('quad', 'tp'), split_axis=0, concat_axis=0, til...  6.9 us
  transfers between devices with their start and end apart: 14, of which 5 were waited for; matrix products, arithmetic and copies ran while one was open for 5% of the time, Pallas kernels for 4%

profile of v7, /device:TPU:513, one launch (start us, length us, event | category | flops | bytes accessed | tf_op | source)
XLA Modules:
  0.0 177.2 jit_solution(8328810322442275047)
XLA Ops:
  0.1 1.1 copy.51
  3.3 1.1 maximum_maximum_fusion
  4.4 13.7 %all-to-all-start = ((bf16[8,480,128]{2,1,0:T(8,128)(2,1)}), bf16[8,480,128]{2,1,0:T(8,128)(2,1)S(1)}, u32[]{:S(2)}, u32[]{:S(2)}) async-start(bf16[8,480,128]{2,1,0:T(8,128)(2,1)} %maximum_maximum_fusion), calls=%async_computation | async-start | bytes 1966080 | tf_op jit(solution)/shard_map/all_to_all | solution.py:335
  18.2 4.4 %collective-permute-start.5 = (bf16[128,2048]{1,0:T(8,128)(2,1)}, bf16[128,2048]{1,0:T(8,128)(2,1)S(1)}, u32[]{:S(2)}, u32[]{:S(2)}) collective-permute-start(bf16[128,2048]{1,0:T(8,128)(2,1)} %param.22), channel_id=1, source_target_pairs={{0,2},{8,14},{1,3},{9,15},{2,4},{10,8},{3,5},{11,9},{4,6},{12,10},... | collective-permute-start | bytes 1572872 | tf_op jit(solution)/shard_map/ppermute | solution.py:60
  22.6 1.0 collective-permute-start.4
  26.9 8.5 %all-to-all-done.a_ref = bf16[8,480,128]{2,1,0:T(8,128)(2,1)S(1)} async-done(((bf16[8,480,128]{2,1,0:T(8,128)(2,1)}), bf16[8,480,128]{2,1,0:T(8,128)(2,1)S(1)}, u32[]{:S(2)}, u32[]{:S(2)}) %all-to-all-start) | async-done | bytes 983072 | tf_op jit(solution)/shard_map/all_to_all | solution.py:335
  35.4 11.2 %collective-permute-start.3 = (bf16[8,480,128]{2,1,0:T(8,128)(2,1)S(1)}, bf16[8,480,128]{2,1,0:T(8,128)(2,1)S(1)}, u32[]{:S(2)}, u32[]{:S(2)}) collective-permute-start(bf16[8,480,128]{2,1,0:T(8,128)(2,1)S(1)} %all-to-all-done.a_ref), channel_id=1, source_target_pairs={{0,8},{8,0},{1,9},{9,1},{2,10},{10,2},{3,11},{11,3},{4,12},{12,4},... | collective-permute-start | bytes 2949128 | tf_op jit(solution)/shard_map/ppermute | solution.py:52
  46.6 1.2 pad_maximum_fusion.res_ref
  47.8 3.5 %collective-permute-start.6 = (bf16[128,2048]{1,0:T(8,128)(2,1)S(1)}, bf16[128,2048]{1,0:T(8,128)(2,1)}, u32[]{:S(2)}, u32[]{:S(2)}) collective-permute-start(bf16[128,2048]{1,0:T(8,128)(2,1)S(1)} %collective-permute-done.5.w2), channel_id=1, source_target_pairs={{0,1},{8,15},{1,2},{9,8},{2,3},{10,9},{3,4},{11,10},{4,5},{12,11},... | collective-permute-start | bytes 1572872 | tf_op jit(solution)/shard_map/ppermute | solution.py:60
  52.0 1.7 dynamic-slice_bitcast_fusion.3
  54.0 5.3 %collective-permute-done = bf16[288,128]{1,0:T(8,128)(2,1)} collective-permute-done((bf16[288,128]{1,0:T(8,128)(2,1)}, bf16[288,128]{1,0:T(8,128)(2,1)}, u32[]{:S(2)}, u32[]{:S(2)}) %collective-permute-start) | collective-permute-done | bytes 73760 | tf_op jit(solution)/shard_map/ppermute | solution.py:48
  60.0 1.6 collective-permute-done.1
  61.6 2.3 %collective-permute-start.10 = (bf16[64,2048]{1,0:T(8,128)(2,1)}, bf16[64,2048]{1,0:T(8,128)(2,1)}, u32[]{:S(2)}, u32[]{:S(2)}) collective-permute-start(bf16[64,2048]{1,0:T(8,128)(2,1)} %constant_dynamic-slice_fusion), channel_id=1, source_target_pairs={{0,2},{8,14},{1,3},{9,15},{2,4},{10,8},{3,5},{11,9},{4,6},{12,10},... | collective-permute-start | bytes 786440 | tf_op jit(solution)/shard_map/ppermute | solution.py:60
  65.7 2.7 %shard_map.145 = (f32[4,192,128]{2,1,0:T(8,128)S(1)}, f32[4,192,256]{2,1,0:T(8,128)S(1)}, bf16[4,192,256]{2,1,0:T(8,128)(2,1)S(1)}) custom-call(bf16[1152,128]{1,0:T(8,128)(2,1)S(1)} %pad_maximum_fusion.1.q_ref, bf16[8,480,128]{2,1,0:T(8,128)(2,1)S(1)} %all-to-all-done.a_ref), custom_call_target="tpu_custom_call" | custom-call | tf_op jit(solution)/shard_map/pallas_call | solution.py:339
  68.5 4.0 %shard_map.146 = bf16[4,192,128]{2,1,0:T(8,128)(2,1)} custom-call(s32[3]{0:T(128)S(1)} %pad_add_fusion.at_ref, bf16[4,192,256]{2,1,0:T(8,128)(2,1)S(1)} %get-tuple-element.18.q_ref, bf16[8,480,128]{2,1,0:T(8,128)(2,1)S(1)} %collective-permute-done.3.b_ref, f32[4,192,128]{2,1,0:T(8,128)S(1)} %get-tuple-element.19.acc_ref, ...), custom_call_target="tpu_custom_call" | custom-call | tf_op jit(solution)/shard_map/pallas_call | solution.py:351
  72.5 7.8 %all-to-all-start.1 = ((bf16[32,24,128]{2,1,0:T(8,128)(2,1)}), bf16[32,24,128]{2,1,0:T(8,128)(2,1)S(1)}, u32[]{:S(2)}, u32[]{:S(2)}) async-start(bf16[32,24,128]{2,1,0:T(8,128)(2,1)} %bitcast.12), calls=%async_computation.1 | async-start | bytes 393216 | tf_op jit(solution)/shard_map/all_to_all | solution.py:360
  81.2 1.3 collective-permute-done.11.s4
  82.4 6.9 %all-to-all-done.1.att_ref = bf16[32,24,128]{2,1,0:T(8,128)(2,1)S(1)} async-done(((bf16[32,24,128]{2,1,0:T(8,128)(2,1)}), bf16[32,24,128]{2,1,0:T(8,128)(2,1)S(1)}, u32[]{:S(2)}, u32[]{:S(2)}) %all-to-all-start.1) | async-done | bytes 196640 | tf_op jit(solution)/shard_map/all_to_all | solution.py:360
  89.4 3.7 %shard_map.147 = (bf16[96,2048]{1,0:T(8,128)(2,1)S(1)}, bf16[2048,256]{1,0:T(8,128)(2,1)S(1)}) custom-call(s32[3]{0:T(128)S(1)} %pad_add_fusion.at_ref, bf16[32,24,128]{2,1,0:T(8,128)(2,1)S(1)} %all-to-all-done.1.att_ref, bf16[128,2048]{1,0:T(8,128)(2,1)} %collective-permute-done.4.w1, bf16[128,2048]{1,0:T(8,128)(2,1)S(1)} %collective-permute-done.5.w2, ...), custom_call_target="tpu_custom_call" | custom-call | tf_op jit(solution)/shard_map/pallas_call | solution.py:362
  93.0 38.8 %all_to_all.20 = bf16[128,16,256]{2,1,0:T(8,128)(2,1)S(1)} all-to-all(bf16[128,16,256]{2,1,0:T(8,128)(2,1)S(1)} %bitcast.51), channel_id=1, replica_groups=mesh['grp'=2,'half'=2,'quad'=4,'core'=2,'tp'=8] {'half','quad','core','tp'}, dimensions={0} | all-to-all | bytes 2097152 | tf_op jit(solution)/shard_map/all_to_all | solution.py:376
  131.8 1.9 %copy-done.3 = bf16[1,768,2048]{2,1,0:T(8,128)(2,1)S(1)} copy-done((bf16[1,768,2048]{2,1,0:T(8,128)(2,1)S(1)}, bf16[1,768,2048]{2,1,0:T(8,128)(2,1)}, u32[]{:S(2)}) %copy-start.3) | copy-done | bytes 3145752
  133.7 3.4 %shard_map.148 = bf16[2048,256]{1,0:T(8,128)(2,1)S(1)} custom-call(bf16[2048,256]{1,0:T(8,128)(2,1)S(1)} %bitcast.46, bf16[2048,768]{1,0:T(8,128)(2,1)S(1)} %bitcast.48, bf16[2048,768]{1,0:T(8,128)(2,1)S(1)} %bitcast.49, bf16[768,2048]{1,0:T(8,128)(2,1)S(1)} %bitcast.50), custom_call_target="tpu_custom_call" | custom-call | tf_op jit(solution)/shard_map/pallas_call | solution.py:379
  137.1 38.4 %all_to_all.21 = bf16[128,16,256]{2,1,0:T(8,128)(2,1)S(1)} all-to-all(bf16[128,16,256]{2,1,0:T(8,128)(2,1)S(1)} %bitcast.47), channel_id=1, replica_groups=mesh['grp'=2,'half'=2,'quad'=4,'core'=2,'tp'=8] {'half','quad','core','tp'}, dimensions={0} | all-to-all | bytes 2097152 | tf_op jit(solution)/shard_map/all_to_all | solution.py:376
  175.5 1.7 shard_map.149
  (70 shorter events, 9.7 us)
Async XLA Ops:
  0.0 2.3 %copy-start = (bf16[512,128]{1,0:T(8,128)(2,1)S(1)}, bf16[512,128]{1,0:T(8,128)(2,1)}, u32[]{:S(2)}) copy-start(bf16[512,128]{1,0:T(8,128)(2,1)} %param.21) | copy-start | bytes 393220
  0.0 2.3 %copy-start.12 = (f32[512]{0:T(512)S(1)}, f32[512]{0:T(512)}, u32[]{:S(2)}) copy-start(f32[512]{0:T(512)} %param.19) | copy-start | bytes 6148
  3.2 20.4 %copy-start.6 = (bf16[192,4,192]{2,1,0:T(4,128)(2,1)S(1)}, bf16[192,4,192]{2,1,0:T(4,128)(2,1)}, u32[]{:S(2)}) copy-start(bf16[192,4,192]{2,1,0:T(4,128)(2,1)} %param.16) | copy-start | bytes 884740
  4.4 31.0 %all-to-all-start = ((bf16[8,480,128]{2,1,0:T(8,128)(2,1)}), bf16[8,480,128]{2,1,0:T(8,128)(2,1)S(1)}, u32[]{:S(2)}, u32[]{:S(2)}) async-start(bf16[8,480,128]{2,1,0:T(8,128)(2,1)} %maximum_maximum_fusion), calls=%async_computation | async-start | bytes 1966080 | tf_op jit(solution)/shard_map/all_to_all | solution.py:335
  18.1 5.8 %copy-start.7 = (bf16[24,4,2048]{2,1,0:T(4,128)(2,1)S(1)}, bf16[24,4,2048]{2,1,0:T(4,128)(2,1)}, u32[]{:S(2)}) copy-start(bf16[24,4,2048]{2,1,0:T(4,128)(2,1)} %param.15) | copy-start | bytes 1179652
  18.1 6.7 %copy-start.9 = (s32[24,4,2]{0,2,1:T(2,128)S(1)}, s32[24,4,2]{0,2,1:T(2,128)}, u32[]{:S(2)}) copy-start(s32[24,4,2]{0,2,1:T(2,128)} %param.26) | copy-start | bytes 2308
  18.1 6.9 %copy-start.8 = (f32[24,4,2]{0,2,1:T(2,128)S(1)}, f32[24,4,2]{0,2,1:T(2,128)}, u32[]{:S(2)}) copy-start(f32[24,4,2]{0,2,1:T(2,128)} %param.25) | copy-start | bytes 2308
  18.2 7.1 %copy-start.10 = (f32[24,4]{0,1:T(4,128)S(1)}, f32[24,4]{0,1:T(4,128)}, u32[]{:S(2)}) copy-start(f32[24,4]{0,1:T(4,128)} %param.24) | copy-start | bytes 1156
  18.2 29.6 %collective-permute-start.5 = (bf16[128,2048]{1,0:T(8,128)(2,1)}, bf16[128,2048]{1,0:T(8,128)(2,1)S(1)}, u32[]{:S(2)}, u32[]{:S(2)}) collective-permute-start(bf16[128,2048]{1,0:T(8,128)(2,1)} %param.22), channel_id=1, source_target_pairs={{0,2},{8,14},{1,3},{9,15},{2,4},{10,8},{3,5},{11,9},{4,6},{12,10},... | collective-permute-start | bytes 1572872 | tf_op jit(solution)/shard_map/ppermute | solution.py:60
  22.6 41.4 %collective-permute-start.4 = (bf16[128,2048]{1,0:T(8,128)(2,1)}, bf16[128,2048]{1,0:T(8,128)(2,1)}, u32[]{:S(2)}, u32[]{:S(2)}) collective-permute-start(bf16[128,2048]{1,0:T(8,128)(2,1)} %param.22), channel_id=1, source_target_pairs={{0,1},{8,15},{1,2},{9,8},{2,3},{10,9},{3,4},{11,10},{4,5},{12,11},... | collective-permute-start | bytes 1572872 | tf_op jit(solution)/shard_map/ppermute | solution.py:60
  35.4 33.1 %collective-permute-start.3 = (bf16[8,480,128]{2,1,0:T(8,128)(2,1)S(1)}, bf16[8,480,128]{2,1,0:T(8,128)(2,1)S(1)}, u32[]{:S(2)}, u32[]{:S(2)}) collective-permute-start(bf16[8,480,128]{2,1,0:T(8,128)(2,1)S(1)} %all-to-all-done.a_ref), channel_id=1, source_target_pairs={{0,8},{8,0},{1,9},{9,1},{2,10},{10,2},{3,11},{11,3},{4,12},{12,4},... | collective-permute-start | bytes 2949128 | tf_op jit(solution)/shard_map/ppermute | solution.py:52
  47.8 16.6 %collective-permute-start.6 = (bf16[128,2048]{1,0:T(8,128)(2,1)S(1)}, bf16[128,2048]{1,0:T(8,128)(2,1)}, u32[]{:S(2)}, u32[]{:S(2)}) collective-permute-start(bf16[128,2048]{1,0:T(8,128)(2,1)S(1)} %collective-permute-done.5.w2), channel_id=1, source_target_pairs={{0,1},{8,15},{1,2},{9,8},{2,3},{10,9},{3,4},{11,10},{4,5},{12,11},... | collective-permute-start | bytes 1572872 | tf_op jit(solution)/shard_map/ppermute | solution.py:60
  53.7 5.6 %collective-permute-start = (bf16[288,128]{1,0:T(8,128)(2,1)}, bf16[288,128]{1,0:T(8,128)(2,1)}, u32[]{:S(2)}, u32[]{:S(2)}) collective-permute-start(bf16[288,128]{1,0:T(8,128)(2,1)} %get-tuple-element.32), channel_id=1, source_target_pairs={{0,16},{16,32},{32,48},{48,0},{1,17},{17,33},{33,49},{49,1},{2,18}... | collective-permute-start | bytes 221192 | tf_op jit(solution)/shard_map/ppermute | solution.py:48
  54.0 7.6 %collective-permute-start.1 = (bf16[288,128]{1,0:T(8,128)(2,1)}, bf16[288,128]{1,0:T(8,128)(2,1)}, u32[]{:S(2)}, u32[]{:S(2)}) collective-permute-start(bf16[288,128]{1,0:T(8,128)(2,1)} %get-tuple-element.31), channel_id=1, source_target_pairs={{0,32},{16,48},{32,0},{48,16},{1,33},{17,49},{33,1},{49,17},{2,34}... | collective-permute-start | bytes 221192 | tf_op jit(solution)/shard_map/ppermute | solution.py:48
  59.2 4.7 %collective-permute-start.2 = (bf16[288,128]{1,0:T(8,128)(2,1)}, bf16[288,128]{1,0:T(8,128)(2,1)S(1)}, u32[]{:S(2)}, u32[]{:S(2)}) collective-permute-start(bf16[288,128]{1,0:T(8,128)(2,1)} %get-tuple-element.30), channel_id=1, source_target_pairs={{0,48},{16,0},{32,16},{48,32},{1,49},{17,1},{33,17},{49,33},{2,50}... | collective-permute-start | bytes 221192 | tf_op jit(solution)/shard_map/ppermute | solution.py:48
  61.6 18.7 %collective-permute-start.10 = (bf16[64,2048]{1,0:T(8,128)(2,1)}, bf16[64,2048]{1,0:T(8,128)(2,1)}, u32[]{:S(2)}, u32[]{:S(2)}) collective-permute-start(bf16[64,2048]{1,0:T(8,128)(2,1)} %constant_dynamic-slice_fusion), channel_id=1, source_target_pairs={{0,2},{8,14},{1,3},{9,15},{2,4},{10,8},{3,5},{11,9},{4,6},{12,10},... | collective-permute-start | bytes 786440 | tf_op jit(solution)/shard_map/ppermute | solution.py:60
  63.9 18.5 %collective-permute-start.8 = (bf16[128,2048]{1,0:T(8,128)(2,1)S(1)}, bf16[128,2048]{1,0:T(8,128)(2,1)}, u32[]{:S(2)}, u32[]{:S(2)}) collective-permute-start(bf16[128,2048]{1,0:T(8,128)(2,1)S(1)} %collective-permute-done.5.w2), channel_id=1, source_target_pairs={{0,8},{8,0},{1,9},{9,1},{2,10},{10,2},{3,11},{11,3},{4,12},{12,4},... | collective-permute-start | bytes 1572872 | tf_op jit(solution)/shard_map/ppermute | solution.py:52
  63.9 18.5 %collective-permute-start.7 = (bf16[128,2048]{1,0:T(8,128)(2,1)}, bf16[128,2048]{1,0:T(8,128)(2,1)}, u32[]{:S(2)}, u32[]{:S(2)}) collective-permute-start(bf16[128,2048]{1,0:T(8,128)(2,1)} %collective-permute-done.4.w1), channel_id=1, source_target_pairs={{0,8},{8,0},{1,9},{9,1},{2,10},{10,2},{3,11},{11,3},{4,12},{12,4},... | collective-permute-start | bytes 1572872 | tf_op jit(solution)/shard_map/ppermute | solution.py:52
  64.4 18.0 %collective-permute-start.9 = (bf16[128,2048]{1,0:T(8,128)(2,1)}, bf16[128,2048]{1,0:T(8,128)(2,1)}, u32[]{:S(2)}, u32[]{:S(2)}) collective-permute-start(bf16[128,2048]{1,0:T(8,128)(2,1)} %collective-permute-done.6.w3), channel_id=1, source_target_pairs={{0,8},{8,0},{1,9},{9,1},{2,10},{10,2},{3,11},{11,3},{4,12},{12,4},... | collective-permute-start | bytes 1572872 | tf_op jit(solution)/shard_map/ppermute | solution.py:52
  65.7 23.6 %copy-start.4 = (f32[2048]{0:T(1024)S(1)}, f32[2048]{0:T(1024)}, u32[]{:S(2)}) copy-start(f32[2048]{0:T(1024)} %param.23) | copy-start | bytes 24580
  72.5 16.8 %all-to-all-start.1 = ((bf16[32,24,128]{2,1,0:T(8,128)(2,1)}), bf16[32,24,128]{2,1,0:T(8,128)(2,1)S(1)}, u32[]{:S(2)}, u32[]{:S(2)}) async-start(bf16[32,24,128]{2,1,0:T(8,128)(2,1)} %bitcast.12), calls=%async_computation.1 | async-start | bytes 393216 | tf_op jit(solution)/shard_map/all_to_all | solution.py:360
  80.3 2.1 %collective-permute-start.11 = (bf16[64,2048]{1,0:T(8,128)(2,1)}, bf16[64,2048]{1,0:T(8,128)(2,1)S(1)}, u32[]{:S(2)}, u32[]{:S(2)}) collective-permute-start(bf16[64,2048]{1,0:T(8,128)(2,1)} %collective-permute-done.10.w4), channel_id=1, source_target_pairs={{0,8},{8,0},{1,9},{9,1},{2,10},{10,2},{3,11},{11,3},{4,12},{12,4},... | collective-permute-start | bytes 786440 | tf_op jit(solution)/shard_map/ppermute | solution.py:52
  89.4 42.4 %copy-start.1 = (bf16[1,2048,768]{2,1,0:T(8,128)(2,1)S(1)}, bf16[1,2048,768]{2,1,0:T(8,128)(2,1)}, u32[]{:S(2)}) copy-start(bf16[1,2048,768]{2,1,0:T(8,128)(2,1)} %param.27) | copy-start | bytes 9437188
  89.4 42.4 %copy-start.2 = (bf16[1,2048,768]{2,1,0:T(8,128)(2,1)S(1)}, bf16[1,2048,768]{2,1,0:T(8,128)(2,1)}, u32[]{:S(2)}) copy-start(bf16[1,2048,768]{2,1,0:T(8,128)(2,1)} %param.28) | copy-start | bytes 9437188
  (3 other events, 4.8 us)
